TPU v7x, 128 devices: a whole 4x4x4 slice. The times are simulated.
128 devices in a mesh: st: 64 (over z, y, x), tp: 2 (over core).
Axes of the slice: x: 4, y: 4, z: 4, core: 2. Of those that a mesh axis runs over, the one named last changes fastest.
Arguments:
- tokens: bfloat16 [65536, 2048], P('st', 'tp'), may hold values from -6 to 6
- passage_ids: int32 [1024, 2], P('st'), may hold values from 0 to 1023, as said below
- passage_store: bfloat16 [1024, 64, 2048], P('st'), may hold values from -6 to 6
- norm_gain: bfloat16 [2048], replicated, may hold values from 0.099609375 to 1.8984375
- conv_value_weight: bfloat16 [2048, 1536], P(None, 'tp'), may hold values from -0.125 to 0.125
- conv_gate_weight: bfloat16 [2048, 1536], P(None, 'tp'), may hold values from -0.125 to 0.125
- conv_weight: bfloat16 [31, 1536], P(None, 'tp'), may hold values from -1 to 1
- ln_gain: bfloat16 [1536], P('tp'), may hold values from 0.099609375 to 1.8984375
- query_weight: bfloat16 [2048, 512], P(None, 'tp'), may hold values from -0.125 to 0.125
- query_gain: bfloat16 [512], P('tp'), may hold values from 0.5 to 10
- passage_gain: bfloat16 [2048], replicated, may hold values from 0.099609375 to 1.8984375
- key_weight: bfloat16 [2048, 512], P(None, 'tp'), may hold values from -0.125 to 0.125
- value_weight: bfloat16 [2048, 512], P(None, 'tp'), may hold values from -0.125 to 0.125
- key_gain: bfloat16 [512], P('tp'), may hold values from 0.5 to 10
- memory_gate: bfloat16 [512], P('tp'), may hold values from 0.29882812 to 1.5
- conv_out_weight: bfloat16 [1536, 2048], P('tp'), may hold values from -0.125 to 0.125
- memory_out_weight: bfloat16 [512, 2048], P('tp'), may hold values from -0.125 to 0.125
Outputs:
- layer_out: bfloat16 [65536, 2048], P(('st', 'tp'))
Inputs may be any that keep to these rules, and one draw needn't show every extreme that they name: The owner of passage p is p // 16. Among the 32 entries of the rows of passage_ids that lie on one index of st (aligned runs of 16 rows, that is the blocks of one index of st), no owner is named more than 1 times, and in every such run some owner is named exactly 1 times.
All inputs are finite; a program needn't handle non-finite values.
Results may differ from a plain program's by a relative error of at most 0.008.
The roundings to bfloat16 on the way count: a program that leaves them out, or rounds other values in their place, can miss the bound.
Values may be sent and summed in bfloat16 or wider, within the bound.
No kernel may reach another device: no remote copies, remote signals or barrier semaphores. Data moves between devices by JAX's collectives and lax.ppermute only.
A program may use at most 192 MiB of HBM per device.

v0:
```python
import jax
import jax.numpy as jnp
from jax import lax
from jax.experimental import pallas as pl
from jax.experimental.pallas import tpu as pltpu
from jax.sharding import PartitionSpec as P

D = 2048
HALF_D = 1024
C_A = 1536
C_DEV = 768
MEM_HD = 64
MEM_DEV = 256
KW = 31
SEQ_LEN = 512
BLOCK = 64
PLEN = 64
PASS_DEV = 16
TOK_DEV = 1024
NORM_EPS = 1e-06
LAYER_EPS = 1e-05

KV_TILE = 256
TOK_TILE = 256
OUT_TILE = 256
ATT_TILE = 128
LANES = 128
CONV_ROWS = 128
HISTORY = 32

F32 = jnp.float32
BF16 = jnp.bfloat16


def matmul(a, b):
    return lax.dot_general(a, b, (((1,), (0,)), ((), ())), preferred_element_type=F32)


def matmul_t(a, b):
    return lax.dot_general(a, b, (((1,), (1,)), ((), ())), preferred_element_type=F32)


def head_norm(product, gain):
    width = product.shape[1]
    rows = lax.broadcasted_iota(jnp.int32, (width, width), 0) // MEM_HD
    cols = lax.broadcasted_iota(jnp.int32, (width, width), 1) // MEM_HD
    same_head = jnp.where(rows == cols, 1.0, 0.0).astype(BF16)
    squares = product * product
    coarse = squares.astype(BF16)
    fine = (squares - coarse.astype(F32)).astype(BF16)
    total = matmul(coarse, same_head) + matmul(fine, same_head)
    return product * lax.rsqrt(total * (1.0 / MEM_HD) + NORM_EPS) * gain


def kv_kernel(rows_ref, gain_ref, wk_ref, wv_ref, kg_ref, out_ref):
    widened = rows_ref[...].astype(F32)
    factor = lax.rsqrt(jnp.sum(widened * widened, axis=1, keepdims=True) * (1.0 / D) + NORM_EPS)
    normed = (widened * factor * gain_ref[...]).astype(BF16)
    keys = head_norm(matmul(normed, wk_ref[...]), kg_ref[...])
    out_ref[:, :MEM_DEV] = keys.astype(BF16)
    out_ref[:, MEM_DEV:] = matmul(normed, wv_ref[...]).astype(BF16)


def resident(shape):
    zeros = (0,) * len(shape)
    return pl.BlockSpec(shape, lambda *_: zeros, pipeline_mode=pl.Buffered(1))


def project_store(rows, passage_gain, key_weight, value_weight, key_gain):
    n = rows.shape[0]
    return pl.pallas_call(
        kv_kernel,
        out_shape=jax.ShapeDtypeStruct((n, 2 * MEM_DEV), BF16),
        grid=(n // KV_TILE,),
        in_specs=[
            pl.BlockSpec((KV_TILE, D), lambda i: (i, 0)),
            resident((1, D)),
            resident((D, MEM_DEV)),
            resident((D, MEM_DEV)),
            resident((1, MEM_DEV)),
        ],
        out_specs=pl.BlockSpec((KV_TILE, 2 * MEM_DEV), lambda i: (i, 0)),
        cost_estimate=pl.CostEstimate(flops=2 * n * D * 2 * MEM_DEV, transcendentals=0, bytes_accessed=8 << 20),
        name="project_store",
    )(rows, passage_gain, key_weight, value_weight, key_gain)


def slots_kernel(asked_ref, kv_ref, out_ref, sem):
    count = out_ref.shape[0]
    copies = [pltpu.make_async_copy(kv_ref.at[asked_ref[s]], out_ref.at[s], sem.at[s]) for s in range(count)]
    for c in copies:
        c.start()
    for c in copies:
        c.wait()


def fill_slots(asked, kv):
    count = asked.shape[0]
    return pl.pallas_call(
        slots_kernel,
        out_shape=jax.ShapeDtypeStruct((count, PLEN, 2 * MEM_DEV), BF16),
        grid_spec=pltpu.PrefetchScalarGridSpec(
            num_scalar_prefetch=1,
            grid=(1,),
            in_specs=[pl.BlockSpec((PASS_DEV, PLEN, 2 * MEM_DEV), lambda i, s: (0, 0, 0))],
            out_specs=pl.BlockSpec(memory_space=pl.ANY),
            scratch_shapes=[pltpu.SemaphoreType.DMA((count,))],
        ),
        name="fill_slots",
    )(asked, kv)


def token_kernel(
    tp_ref, own_ref, peer_ref, gain_ref, wv_ref, wg_ref, wq_ref, cw_ref, qg_ref, filt_ref, stat_ref, q_ref, xs_ref
):
    tile = pl.program_id(0)
    me = tp_ref[0]
    own_at = pl.multiple_of(me * HALF_D, HALF_D)
    peer_at = pl.multiple_of((1 - me) * HALF_D, HALF_D)
    own = own_ref[...].astype(F32)
    peer = peer_ref[...].astype(F32)
    total = jnp.sum(own * own, axis=1, keepdims=True) + jnp.sum(peer * peer, axis=1, keepdims=True)
    factor = lax.rsqrt(total * (1.0 / D) + NORM_EPS)
    own_n = (own * factor * gain_ref[me]).astype(BF16)
    peer_n = (peer * factor * gain_ref[1 - me]).astype(BF16)

    def product(w_ref):
        return matmul(own_n, w_ref[pl.ds(own_at, HALF_D), :]) + matmul(peer_n, w_ref[pl.ds(peer_at, HALF_D), :])

    q_ref[...] = head_norm(product(wq_ref), qg_ref[...]).astype(BF16)
    gated = (product(wv_ref) * jax.nn.sigmoid(product(wg_ref))).astype(BF16)

    @pl.when(tile % (SEQ_LEN // TOK_TILE) == 0)
    def _():
        xs_ref[:HISTORY, :] = jnp.zeros((HISTORY, C_DEV), F32)

    xs_ref[HISTORY:, :] = gated.astype(F32)
    first = HISTORY - (KW - 1)
    for base in range(0, TOK_TILE, CONV_ROWS):
        sums = jnp.zeros((CONV_ROWS, LANES), F32)
        squares = jnp.zeros((CONV_ROWS, LANES), F32)
        for lane in range(0, C_DEV, LANES):
            lanes = slice(lane, lane + LANES)
            acc = None
            for r in range(8):
                steps = [s for s in range(first, first + KW) if s % 8 == r]
                reach = max(steps) - r + CONV_ROWS
                shifted = xs_ref[base + r : base + r + reach, lanes]
                for s in steps:
                    term = shifted[s - r : s - r + CONV_ROWS] * cw_ref[s - first : s - first + 1, lanes]
                    acc = term if acc is None else acc + term
            filt_ref[base : base + CONV_ROWS, lanes] = acc
            sums = sums + acc
            squares = squares + acc * acc
        stat_ref[base : base + CONV_ROWS, 0:1] = jnp.sum(sums, axis=1, keepdims=True)
        stat_ref[base : base + CONV_ROWS, 1:2] = jnp.sum(squares, axis=1, keepdims=True)
    xs_ref[:HISTORY, :] = xs_ref[TOK_TILE:, :]


def token_branch(me, own, peer, gain, wv, wg, wq, cw, qg):
    n = own.shape[0]
    tile = lambda width: pl.BlockSpec((TOK_TILE, width), lambda i, s: (i, 0))
    return pl.pallas_call(
        token_kernel,
        out_shape=(
            jax.ShapeDtypeStruct((n, C_DEV), F32),
            jax.ShapeDtypeStruct((n, 2), F32),
            jax.ShapeDtypeStruct((n, MEM_DEV), BF16),
        ),
        grid_spec=pltpu.PrefetchScalarGridSpec(
            num_scalar_prefetch=1,
            grid=(n // TOK_TILE,),
            in_specs=[
                tile(HALF_D),
                tile(HALF_D),
                resident((2, 1, HALF_D)),
                resident((D, C_DEV)),
                resident((D, C_DEV)),
                resident((D, MEM_DEV)),
                resident((KW, C_DEV)),
                resident((1, MEM_DEV)),
            ],
            out_specs=(tile(C_DEV), tile(2), tile(MEM_DEV)),
            scratch_shapes=[pltpu.VMEM((HISTORY + TOK_TILE, C_DEV), F32)],
        ),
        cost_estimate=pl.CostEstimate(flops=20 * n * D * 768, transcendentals=0, bytes_accessed=16 << 20),
        name="token_branch",
    )(me, own, peer, gain, wv, wg, wq, cw, qg)


def conv_out_kernel(filt_ref, own_ref, peer_ref, gain_ref, w_ref, out_ref):
    stats = (own_ref[...] + peer_ref[...]) * (1.0 / C_A)
    mean = stats[:, 0:1]
    var = stats[:, 1:2] - mean * mean
    scaled = (filt_ref[...] - mean) * lax.rsqrt(var + LAYER_EPS) * gain_ref[...]
    out_ref[...] = matmul((scaled * jax.nn.sigmoid(scaled)).astype(BF16), w_ref[...])


def conv_product(filtered, own_stats, peer_stats, gain, weight):
    n = filtered.shape[0]
    tile = lambda width: pl.BlockSpec((OUT_TILE, width), lambda i: (i, 0))
    return pl.pallas_call(
        conv_out_kernel,
        out_shape=jax.ShapeDtypeStruct((n, D), F32),
        grid=(n // OUT_TILE,),
        in_specs=[tile(C_DEV), tile(2), tile(2), resident((1, C_DEV)), resident((C_DEV, D))],
        out_specs=tile(D),
        cost_estimate=pl.CostEstimate(flops=4 * n * D * 768, transcendentals=0, bytes_accessed=16 << 20),
        name="conv_product",
    )(filtered, own_stats, peer_stats, gain, weight)


def attend_kernel(half_ref, owner_ref, recv_ref, q_ref, conv_ref, gate_ref, w_ref, out_ref, kv_ref, sem):
    step = pl.program_id(0)
    steps = pl.num_programs(0)
    blocks = ATT_TILE // BLOCK
    count = kv_ref.shape[0]
    first = half_ref[0] * count

    def copy(i):
        return pltpu.make_async_copy(recv_ref.at[owner_ref[first + i]], kv_ref.at[i], sem.at[i])

    @pl.when(step == 0)
    def _():
        for i in range(count):
            copy(i).start()

    for j in range(2 * blocks):
        copy(step * 2 * blocks + j).wait()

    heads = MEM_DEV // MEM_HD
    lane_head = lax.broadcasted_iota(jnp.int32, (BLOCK, MEM_DEV), 1) // MEM_HD
    rows = []
    for b in range(blocks):
        at = step * 2 * blocks + 2 * b
        kv = kv_ref[pl.ds(at, 2)].reshape(2 * PLEN, 2 * MEM_DEV)
        q = q_ref[b * BLOCK : (b + 1) * BLOCK, :]
        spread = jnp.concatenate([jnp.where(lane_head == h, q, jnp.zeros_like(q)) for h in range(heads)], axis=0)
        scores = matmul_t(spread, kv[:, :MEM_DEV])
        expanded = jnp.exp(scores - jnp.max(scores, axis=1, keepdims=True))
        weights = (expanded / jnp.sum(expanded, axis=1, keepdims=True)).astype(BF16)
        mixed = matmul(weights, kv[:, MEM_DEV:])
        attended = mixed[:BLOCK]
        for h in range(1, heads):
            attended = jnp.where(lane_head == h, mixed[h * BLOCK : (h + 1) * BLOCK], attended)
        rows.append((attended * gate_ref[...]).astype(BF16))
    memory = jnp.concatenate(rows, axis=0)
    out_ref[...] = (conv_ref[...] + matmul(memory, w_ref[...])).astype(BF16)


def attend(half, owners, received, queries, conv_part, gate, weight):
    n = queries.shape[0] // 2
    steps = n // ATT_TILE
    count = owners.shape[0] // 2
    return pl.pallas_call(
        attend_kernel,
        out_shape=jax.ShapeDtypeStruct((n, D), BF16),
        grid_spec=pltpu.PrefetchScalarGridSpec(
            num_scalar_prefetch=2,
            grid=(steps,),
            in_specs=[
                pl.BlockSpec(memory_space=pl.ANY),
                pl.BlockSpec((ATT_TILE, MEM_DEV), lambda i, h, o: (h[0] * steps + i, 0)),
                pl.BlockSpec((ATT_TILE, D), lambda i, h, o: (h[0] * steps + i, 0)),
                resident((1, MEM_DEV)),
                resident((MEM_DEV, D)),
            ],
            out_specs=pl.BlockSpec((ATT_TILE, D), lambda i, h, o: (i, 0)),
            scratch_shapes=[
                pltpu.VMEM((count, PLEN, 2 * MEM_DEV), BF16),
                pltpu.SemaphoreType.DMA((count,)),
            ],
        ),
        cost_estimate=pl.CostEstimate(flops=4 * n * D * 256, transcendentals=0, bytes_accessed=8 << 20),
        name="attend",
    )(half, owners, received, queries, conv_part, gate, weight)


def body(
    tokens,
    passage_ids,
    passage_store,
    norm_gain,
    conv_value_weight,
    conv_gate_weight,
    conv_weight,
    ln_gain,
    query_weight,
    query_gain,
    passage_gain,
    key_weight,
    value_weight,
    key_gain,
    memory_gate,
    conv_out_weight,
    memory_out_weight,
):
    owner_count = lax.axis_size("st")
    swap = [(0, 1), (1, 0)]
    me = lax.axis_index("tp").astype(jnp.int32).reshape(1)
    row = lambda v: v.astype(F32).reshape(1, -1)

    owner_ids = passage_ids // PASS_DEV
    local_ids = passage_ids % PASS_DEV
    everyone = jnp.arange(owner_count, dtype=jnp.int32)[:, None, None]
    wanted = jnp.sum(jnp.where(owner_ids[None] == everyone, local_ids[None], 0), axis=(1, 2))
    asked = lax.all_to_all(wanted.reshape(owner_count, 1), "st", 0, 0, tiled=True).reshape(-1)
    peer_tokens = lax.ppermute(tokens, "tp", swap)

    kv = project_store(
        passage_store.reshape(-1, D), row(passage_gain), key_weight, value_weight, row(key_gain)
    ).reshape(PASS_DEV, PLEN, 2 * MEM_DEV)
    sent = fill_slots(asked, kv)
    received = lax.all_to_all(sent, "st", 0, 0, tiled=True)

    filtered, own_stats, queries = token_branch(
        me,
        tokens,
        peer_tokens,
        norm_gain.astype(F32).reshape(2, 1, HALF_D),
        conv_value_weight,
        conv_gate_weight,
        query_weight,
        conv_weight.astype(F32),
        row(query_gain) * MEM_HD ** (-0.5),
    )
    peer_stats = lax.ppermute(own_stats, "tp", swap)
    conv_part = conv_product(filtered, own_stats, peer_stats, row(ln_gain), conv_out_weight)

    owners = owner_ids.reshape(-1)
    gate = jnp.tanh(row(memory_gate))
    theirs = attend(1 - me, owners, received, queries, conv_part, gate, memory_out_weight)
    from_peer = lax.ppermute(theirs, "tp", swap)
    mine = attend(me, owners, received, queries, conv_part, gate, memory_out_weight)
    return (mine.astype(F32) + from_peer.astype(F32)).astype(BF16)


def solution(mesh):
    return jax.shard_map(
        body,
        mesh=mesh,
        in_specs=(
            P("st", "tp"),
            P("st", None),
            P("st", None, None),
            P(),
            P(None, "tp"),
            P(None, "tp"),
            P(None, "tp"),
            P("tp"),
            P(None, "tp"),
            P("tp"),
            P(),
            P(None, "tp"),
            P(None, "tp"),
            P("tp"),
            P("tp"),
            P("tp", None),
            P("tp", None),
        ),
        out_specs=P(("st", "tp"), None),
        check_vma=False,
    )
```

profile of v0, /device:TPU:1, one launch (start us, length us, event | category | flops | bytes accessed | tf_op | source)
XLA Modules:
  0.0 120.3 jit_solution(16367569653588182256)
XLA Ops:
  0.0 1.4 %collective-permute-start = (bf16[1024,1024]{1,0:T(8,128)(2,1)}, bf16[1024,1024]{1,0:T(8,128)(2,1)S(1)}, u32[]{:S(2)}, u32[]{:S(2)}) collective-permute-start(bf16[1024,1024]{1,0:T(8,128)(2,1)} %own_ref.1), channel_id=1, source_target_pairs={{0,1},{1,0},{2,3},{3,2},{4,5},{5,4},{6,7},{7,6},{8,9},{9,8},{10,11... | collective-permute-start | bytes 6291464 | tf_op jit(solution)/shard_map/ppermute | solution.py:308
  1.4 0.7 and_select_fusion
  2.1 0.1 select_reduce_fusion
  2.2 0.7 copy.33
  2.9 11.2 %all-to-all-start = ((s32[64,1,1]{2,1,0:T(1,128)}), s32[64,1,1]{2,1,0:T(1,128)S(1)}, u32[]{:S(2)}, u32[]{:S(2)}) async-start(s32[64,1,1]{2,1,0:T(1,128)} %copy.33), calls=%async_computation | async-start | bytes 65536 | tf_op jit(solution)/shard_map/all_to_all | solution.py:307
  14.1 1.2 reshape.61
  15.3 1.3 %reshape.59 = f32[2048]{0:T(1024)} convert(bf16[2048]{0:T(1024)(128)(2,1)} %param.27) | non-fusion elementwise | flops 2048 | bytes 12288 | tf_op jit(solution)/shard_map/reshape | solution.py:301
  16.6 8.9 %project_store.1 = bf16[1024,512]{1,0:T(8,128)(2,1)} custom-call(bf16[1024,2048]{1,0:T(8,128)(2,1)} %bitcast.15, f32[1,2048]{1,0:T(1,128)} %bitcast.11, bf16[2048,256]{1,0:T(8,128)(2,1)} %wk_ref.1, bf16[2048,256]{1,0:T(8,128)(2,1)} %wv_ref.2, f32[1,256]{1,0:T(1,128)} %bitcast.17), custom_call_target="tpu_custom_call" | custom-call | flops 2147483648 | bytes 8388608 | tf_op jit(solution)/shard_map/project_store/pallas_call | solution.py:71
  25.6 0.0 all-to-all-done
  25.6 1.8 %reduce.asked_ref = s32[64]{0:T(128)} reduce(s32[64,1,1]{2,1,0:T(1,128)S(1)} %all-to-all-done, s32[]{:T(128)} %constant.30.clone.1), dimensions={1,2}, to_apply=%all_to_all.10.reduce_sub_computation | reduce | bytes 516 | tf_op jit(solution)/shard_map/all_to_all | solution.py:307
  27.3 4.4 %fill_slots.1 = bf16[64,64,512]{2,1,0:T(8,128)(2,1)} custom-call(s32[64]{0:T(128)} %reduce.asked_ref, bf16[16,64,512]{2,1,0:T(8,128)(2,1)} %bitcast.9), custom_call_target="tpu_custom_call" | custom-call | tf_op jit(solution)/shard_map/fill_slots/pallas_call | solution.py:99
  31.7 0.0 copy-start.1
  31.7 0.0 copy-start
  31.8 0.0 copy-start.5
  31.8 10.2 %all-to-all-start.1 = ((bf16[64,64,512]{2,1,0:T(8,128)(2,1)}), bf16[64,64,512]{2,1,0:T(8,128)(2,1)}, u32[]{:S(2)}, u32[]{:S(2)}) async-start(bf16[64,64,512]{2,1,0:T(8,128)(2,1)} %fill_slots.1), calls=%async_computation.1 | async-start | bytes 8388608 | tf_op jit(solution)/shard_map/all_to_all | solution.py:314
  42.0 0.0 copy-done.1
  42.0 0.6 reshape.63
  42.6 0.0 copy-done
  42.6 0.6 convert_element_type.22.cw_ref
  43.2 0.0 copy-done.5
  43.2 0.6 convert_multiply_fusion
  43.8 0.0 collective-permute-done.peer_ref
  43.8 0.0 copy-start.3
  43.8 1.3 %copy-done.3 = bf16[1024,1024]{1,0:T(8,128)(2,1)} copy-done((bf16[1024,1024]{1,0:T(8,128)(2,1)}, bf16[1024,1024]{1,0:T(8,128)(2,1)S(1)}, u32[]{:S(2)}) %copy-start.3) | copy-done | bytes 2097176
  45.1 0.0 copy-start.6
  45.1 0.0 copy-start.2
  45.1 31.4 %token_branch.1 = (f32[1024,768]{1,0:T(8,128)}, f32[1024,2]{1,0:T(8,128)}, bf16[1024,256]{1,0:T(8,128)(2,1)}) custom-call(s32[1]{0:T(128)} %bitcast.tp_ref.half_ref, bf16[1024,1024]{1,0:T(8,128)(2,1)} %own_ref.1, bf16[1024,1024]{1,0:T(8,128)(2,1)} %copy-done.3, f32[2,1,1024]{2,1,0:T(1,128)} %bitcast.10, bf16[2048,768]{1,0:T(8,128)(2,1)} %wv_ref.3, ...), custom_call_target="tpu_custom_call" | custom-call | flops 32212254720 | bytes 16777216 | tf_op jit(solution)/shard_map/token_branch/pallas_call | solution.py:163
  76.5 1.0 collective-permute-start.1
  77.6 0.0 copy-done.6
  77.6 0.6 convert_tanh_fusion
  78.2 0.1 copy.32
  78.2 0.0 copy-done.2
  78.2 0.6 reshape.66.gain_ref
  78.8 0.6 reshape.47.owner_ref
  79.4 0.0 collective-permute-done.1.peer_ref
  79.4 0.0 copy-start.4
  79.4 0.8 copy-done.4
  80.2 9.3 %conv_product.1.conv_ref = f32[1024,2048]{1,0:T(8,128)} custom-call(f32[1024,768]{1,0:T(8,128)} %get-tuple-element.9.filt_ref, f32[1024,2]{1,0:T(8,128)} %get-tuple-element.10.own_ref, f32[1024,2]{1,0:T(8,128)} %copy-done.4, f32[1,768]{1,0:T(1,128)} %reshape.66.gain_ref, bf16[768,2048]{1,0:T(8,128)(2,1)} %w_ref.3), custom_call_target="tpu_custom_call" | custom-call | flops 6442450944 | bytes 16777216 | tf_op jit(solution)/shard_map/conv_product/pallas_call | solution.py:202
  89.5 6.7 %all-to-all-done.1.recv_ref = bf16[64,64,512]{2,1,0:T(8,128)(2,1)} async-done(((bf16[64,64,512]{2,1,0:T(8,128)(2,1)}), bf16[64,64,512]{2,1,0:T(8,128)(2,1)}, u32[]{:S(2)}, u32[]{:S(2)}) %all-to-all-start.1) | async-done | bytes 4194336 | tf_op jit(solution)/shard_map/all_to_all | solution.py:314
  96.1 9.3 %attend.3 = bf16[512,2048]{1,0:T(8,128)(2,1)} custom-call(s32[1]{0:T(128)S(6)} %sub.10.half_ref, s32[32]{0:T(128)} %reshape.47.owner_ref, bf16[64,64,512]{2,1,0:T(8,128)(2,1)} %all-to-all-done.1.recv_ref, bf16[1024,256]{1,0:T(8,128)(2,1)} %get-tuple-element.8.q_ref, f32[1024,2048]{1,0:T(8,128)} %conv_product.1.conv_ref, f32[1,256]{1,0:T(1,128)} %bitcast.12, ...), custom_call_target="tpu_custom_call" | custom-call | flops 1073741824 | bytes 8388608 | tf_op jit(solution)/shard_map/attend/pallas_call | solution.py:255
  105.5 1.8 %collective-permute-start.2 = (bf16[512,2048]{1,0:T(8,128)(2,1)}, bf16[512,2048]{1,0:T(8,128)(2,1)S(1)}, u32[]{:S(2)}, u32[]{:S(2)}) collective-permute-start(bf16[512,2048]{1,0:T(8,128)(2,1)} %attend.3), channel_id=1, source_target_pairs={{0,1},{1,0},{2,3},{3,2},{4,5},{5,4},{6,7},{7,6},{8,9},{9,8},{10,11... | collective-permute-start | bytes 6291464 | tf_op jit(solution)/shard_map/ppermute | solution.py:333
  107.3 9.3 %attend.2 = bf16[512,2048]{1,0:T(8,128)(2,1)} custom-call(s32[1]{0:T(128)} %bitcast.tp_ref.half_ref, s32[32]{0:T(128)} %reshape.47.owner_ref, bf16[64,64,512]{2,1,0:T(8,128)(2,1)} %all-to-all-done.1.recv_ref, bf16[1024,256]{1,0:T(8,128)(2,1)} %get-tuple-element.8.q_ref, f32[1024,2048]{1,0:T(8,128)} %conv_product.1.conv_ref, f32[1,256]{1,0:T(1,128)} %bitcast.13, ...), custom_call_target="tpu_custom_call" | custom-call | flops 1073741824 | bytes 8388608 | tf_op jit(solution)/shard_map/attend/pallas_call | solution.py:255
  116.6 0.0 collective-permute-done.2
  116.6 3.7 %add_convert_fusion = bf16[512,2048]{1,0:T(8,128)(2,1)} fusion(bf16[512,2048]{1,0:T(8,128)(2,1)S(1)} %collective-permute-done.2, bf16[512,2048]{1,0:T(8,128)(2,1)} %attend.2), kind=kLoop, calls=%fused_computation | loop fusion | flops 4194304 | bytes 6291456 | tf_op jit(solution)/shard_map/convert_element_type | solution.py:335
Async XLA Ops:
  0.0 43.8 %collective-permute-start = (bf16[1024,1024]{1,0:T(8,128)(2,1)}, bf16[1024,1024]{1,0:T(8,128)(2,1)S(1)}, u32[]{:S(2)}, u32[]{:S(2)}) collective-permute-start(bf16[1024,1024]{1,0:T(8,128)(2,1)} %own_ref.1), channel_id=1, source_target_pairs={{0,1},{1,0},{2,3},{3,2},{4,5},{5,4},{6,7},{7,6},{8,9},{9,8},{10,11... | collective-permute-start | bytes 6291464 | tf_op jit(solution)/shard_map/ppermute | solution.py:308
  2.9 22.7 %all-to-all-start = ((s32[64,1,1]{2,1,0:T(1,128)}), s32[64,1,1]{2,1,0:T(1,128)S(1)}, u32[]{:S(2)}, u32[]{:S(2)}) async-start(s32[64,1,1]{2,1,0:T(1,128)} %copy.33), calls=%async_computation | async-start | bytes 65536 | tf_op jit(solution)/shard_map/all_to_all | solution.py:307
  31.7 10.2 %copy-start.1 = (bf16[2048]{0:T(1024)(128)(2,1)S(1)}, bf16[2048]{0:T(1024)(128)(2,1)}, u32[]{:S(2)}) copy-start(bf16[2048]{0:T(1024)(128)(2,1)} %param.20) | copy-start | bytes 12292
  31.7 10.8 %copy-start = (bf16[31,768]{1,0:T(8,128)(2,1)S(1)}, bf16[31,768]{1,0:T(8,128)(2,1)}, u32[]{:S(2)}) copy-start(bf16[31,768]{1,0:T(8,128)(2,1)} %param.23) | copy-start | bytes 142852
  31.8 11.5 %copy-start.5 = (bf16[256]{0:T(256)(128)(2,1)S(1)}, bf16[256]{0:T(256)(128)(2,1)}, u32[]{:S(2)}) copy-start(bf16[256]{0:T(256)(128)(2,1)} %param.26) | copy-start | bytes 1540
  31.8 64.4 %all-to-all-start.1 = ((bf16[64,64,512]{2,1,0:T(8,128)(2,1)}), bf16[64,64,512]{2,1,0:T(8,128)(2,1)}, u32[]{:S(2)}, u32[]{:S(2)}) async-start(bf16[64,64,512]{2,1,0:T(8,128)(2,1)} %fill_slots.1), calls=%async_computation.1 | async-start | bytes 8388608 | tf_op jit(solution)/shard_map/all_to_all | solution.py:314
  43.8 1.3 %copy-start.3 = (bf16[1024,1024]{1,0:T(8,128)(2,1)}, bf16[1024,1024]{1,0:T(8,128)(2,1)S(1)}, u32[]{:S(2)}) copy-start(bf16[1024,1024]{1,0:T(8,128)(2,1)S(1)} %collective-permute-done.peer_ref) | copy-start | bytes 6291460
  45.1 32.4 %copy-start.6 = (bf16[256]{0:T(256)(128)(2,1)S(1)}, bf16[256]{0:T(256)(128)(2,1)}, u32[]{:S(2)}) copy-start(bf16[256]{0:T(256)(128)(2,1)} %param.31) | copy-start | bytes 1540
  45.1 33.1 %copy-start.2 = (bf16[768]{0:T(1024)(128)(2,1)S(1)}, bf16[768]{0:T(1024)(128)(2,1)}, u32[]{:S(2)}) copy-start(bf16[768]{0:T(1024)(128)(2,1)} %param.24) | copy-start | bytes 4612
  76.5 2.9 %collective-permute-start.1 = (f32[1024,2]{1,0:T(8,128)}, f32[1024,2]{1,0:T(8,128)S(1)}, u32[]{:S(2)}, u32[]{:S(2)}) collective-permute-start(f32[1024,2]{1,0:T(8,128)} %get-tuple-element.10.own_ref), channel_id=1, source_target_pairs={{0,1},{1,0},{2,3},{3,2},{4,5},{5,4},{6,7},{7,6},{8,9},{9,8},{10,11... | collective-permute-start | bytes 24584 | tf_op jit(solution)/shard_map/ppermute | solution.py:327
  79.4 0.8 copy-start.4
  105.5 11.2 %collective-permute-start.2 = (bf16[512,2048]{1,0:T(8,128)(2,1)}, bf16[512,2048]{1,0:T(8,128)(2,1)S(1)}, u32[]{:S(2)}, u32[]{:S(2)}) collective-permute-start(bf16[512,2048]{1,0:T(8,128)(2,1)} %attend.3), channel_id=1, source_target_pairs={{0,1},{1,0},{2,3},{3,2},{4,5},{5,4},{6,7},{7,6},{8,9},{9,8},{10,11... | collective-permute-start | bytes 6291464 | tf_op jit(solution)/shard_map/ppermute | solution.py:333
where the time goes:
time: 121 us; the launch traced here: 120 us
  Pallas kernels  72.6 us (60%)
  starting transfers between devices  25.7 us (21%)
  other arithmetic  11.1 us (9%)
  waiting for transfers between devices  6.69 us (6%)
  local copies, waits for them, and re-layouts  4.1 us (3%)
    pallas_call x1, Pallas kernels, token_branch(): pl.pallas_call(token_kernel, out_shape=(jax.ShapeDtypeStruct((n, C_DEV),...  31.4 us
    pallas_call x2, Pallas kernels, attend(): pl.pallas_call(attend_kernel, out_shape=jax.ShapeDtypeStruct((n, D), BF16...  18.7 us
    all_to_all x1, starting transfers between devices, body(): lax.all_to_all(wanted.reshape(owner_count, 1), 'st', 0, 0, tiled=True)  11.2 us
    all_to_all x1, starting transfers between devices, body(): received = lax.all_to_all(sent, 'st', 0, 0, tiled=True)  10.2 us
    pallas_call x1, Pallas kernels, conv_product(): pl.pallas_call(conv_out_kernel, out_shape=jax.ShapeDtypeStruct((n, D), F3...  9.25 us
    pallas_call x1, Pallas kernels, project_store(): pl.pallas_call(kv_kernel, out_shape=jax.ShapeDtypeStruct((n, 2 * MEM_DEV)...  8.95 us
    all_to_all x1, waiting for transfers between devices, body(): received = lax.all_to_all(sent, 'st', 0, 0, tiled=True)  6.68 us
    pallas_call x1, Pallas kernels, fill_slots(): pl.pallas_call(slots_kernel, out_shape=jax.ShapeDtypeStruct((count, PLEN,...  4.38 us
  transfers between devices with their start and end apart: 5, of which 1 were waited for; matrix products, arithmetic and copies ran while one was open for 8% of the time, Pallas kernels for 53%

commit v1 on v0

v1 whole, which is shorter than its diff:
```python
import jax
import jax.numpy as jnp
from jax import lax
from jax.experimental import pallas as pl
from jax.experimental.pallas import tpu as pltpu
from jax.sharding import PartitionSpec as P

D = 2048
HALF_D = 1024
C_A = 1536
C_DEV = 768
MEM_HD = 64
MEM_DEV = 256
KW = 31
SEQ_LEN = 512
BLOCK = 64
PLEN = 64
PASS_DEV = 16
TOK_DEV = 1024
NORM_EPS = 1e-06
LAYER_EPS = 1e-05

KV_TILE = 256
TOK_TILE = 256
OUT_TILE = 256
ATT_TILE = 128
ATT_GROUP = 4
LANES = 128
CONV_ROWS = 128
HISTORY = 32

F32 = jnp.float32
BF16 = jnp.bfloat16


def matmul(a, b):
    return lax.dot_general(a, b, (((1,), (0,)), ((), ())), preferred_element_type=F32)


def matmul_t(a, b):
    return lax.dot_general(a, b, (((1,), (1,)), ((), ())), preferred_element_type=F32)


def row_norm(rows, gain):
    widened = rows.astype(F32)
    factor = lax.rsqrt(jnp.sum(widened * widened, axis=1, keepdims=True) * (1.0 / D) + NORM_EPS)
    return (widened * factor * gain).astype(BF16)


def head_norm(product, gain):
    width = product.shape[1]
    rows = lax.broadcasted_iota(jnp.int32, (width, width), 0) // MEM_HD
    cols = lax.broadcasted_iota(jnp.int32, (width, width), 1) // MEM_HD
    same_head = jnp.where(rows == cols, 1.0, 0.0).astype(BF16)
    squares = product * product
    coarse = squares.astype(BF16)
    fine = (squares - coarse.astype(F32)).astype(BF16)
    total = matmul(coarse, same_head) + matmul(fine, same_head)
    return product * lax.rsqrt(total * (1.0 / MEM_HD) + NORM_EPS) * gain


def wide_row(ref):
    values = ref[...].astype(F32)
    return jnp.concatenate([values[i : i + 1, :] for i in range(values.shape[0])], axis=1)


def kv_kernel(rows_hbm, gain_ref, wk_hbm, wv_hbm, kg_ref, out_hbm, rows_ref, wk_ref, wv_ref, out_ref, even, odd, r_sem, w_sem, o_sem):
    chunks = rows_hbm.shape[0] // KV_TILE
    span = lambda c: pl.ds(c * KV_TILE, KV_TILE)
    row_copies = [pltpu.make_async_copy(rows_hbm.at[span(c)], rows_ref.at[span(c)], r_sem.at[c]) for c in range(chunks)]
    out_copies = [pltpu.make_async_copy(out_ref.at[span(c)], out_hbm.at[span(c)], o_sem.at[c]) for c in range(chunks)]
    wk_copy = pltpu.make_async_copy(wk_hbm, wk_ref, w_sem.at[0])
    wv_copy = pltpu.make_async_copy(wv_hbm, wv_ref, w_sem.at[1])
    row_copies[0].start()
    wk_copy.start()
    wv_copy.start()
    for c in range(1, chunks):
        row_copies[c].start()
    gain = wide_row(gain_ref)
    key_gain = wide_row(kg_ref)
    held = (even, odd)

    def normalise(c):
        held[c % 2][...] = row_norm(rows_ref[span(c), :], gain)

    def project(c):
        normed = held[c % 2][...]
        keys = head_norm(matmul(normed, wk_ref[...]), key_gain)
        out_ref[span(c), :MEM_DEV] = keys.astype(BF16)
        out_ref[span(c), MEM_DEV:] = matmul(normed, wv_ref[...]).astype(BF16)

    row_copies[0].wait()
    normalise(0)
    wk_copy.wait()
    wv_copy.wait()
    for c in range(chunks):
        if c + 1 < chunks:
            row_copies[c + 1].wait()
            normalise(c + 1)
        project(c)
        out_copies[c].start()
    for c in range(chunks):
        out_copies[c].wait()


def resident(shape):
    zeros = (0,) * len(shape)
    return pl.BlockSpec(shape, lambda *_: zeros, pipeline_mode=pl.Buffered(1))


HBM = pl.BlockSpec(memory_space=pl.ANY)


def project_store(rows, passage_gain, key_weight, value_weight, key_gain):
    n = rows.shape[0]
    return pl.pallas_call(
        kv_kernel,
        out_shape=jax.ShapeDtypeStruct((n, 2 * MEM_DEV), BF16),
        grid=(1,),
        in_specs=[HBM, resident((D // LANES, LANES)), HBM, HBM, resident((MEM_DEV // LANES, LANES))],
        out_specs=HBM,
        scratch_shapes=[
            pltpu.VMEM((n, D), BF16),
            pltpu.VMEM((D, MEM_DEV), BF16),
            pltpu.VMEM((D, MEM_DEV), BF16),
            pltpu.VMEM((n, 2 * MEM_DEV), BF16),
            pltpu.VMEM((KV_TILE, D), BF16),
            pltpu.VMEM((KV_TILE, D), BF16),
            pltpu.SemaphoreType.DMA((n // KV_TILE,)),
            pltpu.SemaphoreType.DMA((2,)),
            pltpu.SemaphoreType.DMA((n // KV_TILE,)),
        ],
        cost_estimate=pl.CostEstimate(flops=2 * n * D * 2 * MEM_DEV, transcendentals=0, bytes_accessed=8 << 20),
        name="project_store",
    )(rows, passage_gain, key_weight, value_weight, key_gain)


def slots_kernel(asked_ref, kv_ref, out_ref, sem):
    count = out_ref.shape[0]
    copies = [pltpu.make_async_copy(kv_ref.at[asked_ref[s, 0]], out_ref.at[s], sem.at[s]) for s in range(count)]
    for c in copies:
        c.start()
    for c in copies:
        c.wait()


def fill_slots(asked, kv):
    count = asked.shape[0]
    return pl.pallas_call(
        slots_kernel,
        out_shape=jax.ShapeDtypeStruct((count, PLEN, 2 * MEM_DEV), BF16),
        grid_spec=pltpu.PrefetchScalarGridSpec(
            num_scalar_prefetch=1,
            grid=(1,),
            in_specs=[pl.BlockSpec((PASS_DEV, PLEN, 2 * MEM_DEV), lambda i, s: (0, 0, 0))],
            out_specs=pl.BlockSpec(memory_space=pl.ANY),
            scratch_shapes=[pltpu.SemaphoreType.DMA((count,))],
        ),
        name="fill_slots",
    )(asked, kv)


def token_kernel(
    tp_ref, own_ref, peer_ref, gain_ref, wv_ref, wg_ref, wq_ref, cw_ref, qg_ref, filt_ref, stat_ref, q_ref, xs_ref, taps_ref
):
    tile = pl.program_id(0)
    me = tp_ref[0]
    own_at = pl.multiple_of(me * HALF_D, HALF_D)
    peer_at = pl.multiple_of((1 - me) * HALF_D, HALF_D)
    own = own_ref[...].astype(F32)
    peer = peer_ref[...].astype(F32)
    total = jnp.sum(own * own, axis=1, keepdims=True) + jnp.sum(peer * peer, axis=1, keepdims=True)
    factor = lax.rsqrt(total * (1.0 / D) + NORM_EPS)
    own_n = (own * factor * wide_row(gain_ref.at[me])).astype(BF16)
    peer_n = (peer * factor * wide_row(gain_ref.at[1 - me])).astype(BF16)

    def product(w_ref):
        return matmul(own_n, w_ref[pl.ds(own_at, HALF_D), :]) + matmul(peer_n, w_ref[pl.ds(peer_at, HALF_D), :])

    q_ref[...] = head_norm(product(wq_ref), wide_row(qg_ref) * MEM_HD ** (-0.5)).astype(BF16)
    gated = (product(wv_ref) * jax.nn.sigmoid(product(wg_ref))).astype(BF16)

    @pl.when(tile % (SEQ_LEN // TOK_TILE) == 0)
    def _():
        xs_ref[:HISTORY, :] = jnp.zeros((HISTORY, C_DEV), F32)

    taps_ref[...] = cw_ref[...].astype(F32)
    xs_ref[HISTORY:, :] = gated.astype(F32)
    first = HISTORY - (KW - 1)
    for base in range(0, TOK_TILE, CONV_ROWS):
        sums = jnp.zeros((CONV_ROWS, LANES), F32)
        squares = jnp.zeros((CONV_ROWS, LANES), F32)
        for lane in range(0, C_DEV, LANES):
            lanes = slice(lane, lane + LANES)
            acc = None
            for r in range(8):
                steps = [s for s in range(first, first + KW) if s % 8 == r]
                reach = max(steps) - r + CONV_ROWS
                shifted = xs_ref[base + r : base + r + reach, lanes]
                part = None
                for s in steps:
                    term = shifted[s - r : s - r + CONV_ROWS] * taps_ref[s - first : s - first + 1, lanes]
                    part = term if part is None else part + term
                acc = part if acc is None else acc + part
            filt_ref[base : base + CONV_ROWS, lanes] = acc
            sums = sums + acc
            squares = squares + acc * acc
        stat_ref[base : base + CONV_ROWS, 0:1] = jnp.sum(sums, axis=1, keepdims=True)
        stat_ref[base : base + CONV_ROWS, 1:2] = jnp.sum(squares, axis=1, keepdims=True)
    xs_ref[:HISTORY, :] = xs_ref[TOK_TILE:, :]


def token_branch(me, own, peer, gain, wv, wg, wq, cw, qg):
    n = own.shape[0]
    tile = lambda width: pl.BlockSpec((TOK_TILE, width), lambda i, s: (i, 0))
    return pl.pallas_call(
        token_kernel,
        out_shape=(
            jax.ShapeDtypeStruct((n, C_DEV), F32),
            jax.ShapeDtypeStruct((n, 2), F32),
            jax.ShapeDtypeStruct((n, MEM_DEV), BF16),
        ),
        grid_spec=pltpu.PrefetchScalarGridSpec(
            num_scalar_prefetch=1,
            grid=(n // TOK_TILE,),
            in_specs=[
                tile(HALF_D),
                tile(HALF_D),
                resident((2, HALF_D // LANES, LANES)),
                resident((D, C_DEV)),
                resident((D, C_DEV)),
                resident((D, MEM_DEV)),
                resident((KW, C_DEV)),
                resident((MEM_DEV // LANES, LANES)),
            ],
            out_specs=(tile(C_DEV), tile(2), tile(MEM_DEV)),
            scratch_shapes=[pltpu.VMEM((HISTORY + TOK_TILE, C_DEV), F32), pltpu.VMEM((KW, C_DEV), F32)],
        ),
        cost_estimate=pl.CostEstimate(flops=20 * n * D * 768, transcendentals=0, bytes_accessed=16 << 20),
        name="token_branch",
    )(me, own, peer, gain, wv, wg, wq, cw, qg)


def swish_kernel(filt_ref, own_ref, peer_ref, gain_ref, out_ref):
    stats = (own_ref[...] + peer_ref[...]) * (1.0 / C_A)
    mean = stats[:, 0:1]
    var = stats[:, 1:2] - mean * mean
    scaled = (filt_ref[...] - mean) * lax.rsqrt(var + LAYER_EPS) * wide_row(gain_ref)
    out_ref[...] = (scaled * jax.nn.sigmoid(scaled)).astype(BF16)


def channel_swish(half, filtered, own_stats, peer_stats, gain):
    n = filtered.shape[0] // 2
    steps = n // OUT_TILE
    tile = lambda width: pl.BlockSpec((OUT_TILE, width), lambda i, h: (h[0] * steps + i, 0))
    return pl.pallas_call(
        lambda half_ref, *refs: swish_kernel(*refs),
        out_shape=jax.ShapeDtypeStruct((n, C_DEV), BF16),
        grid_spec=pltpu.PrefetchScalarGridSpec(
            num_scalar_prefetch=1,
            grid=(steps,),
            in_specs=[tile(C_DEV), tile(2), tile(2), resident((C_DEV // LANES, LANES))],
            out_specs=pl.BlockSpec((OUT_TILE, C_DEV), lambda i, h: (i, 0)),
        ),
        cost_estimate=pl.CostEstimate(flops=n * D * 768, transcendentals=0, bytes_accessed=4 << 20),
        name="channel_swish",
    )(half, filtered, own_stats, peer_stats, gain)


def pair_kernel(own_ref, peer_ref, w_own_ref, w_peer_ref, out_ref):
    out_ref[...] = matmul(own_ref[...], w_own_ref[...]) + matmul(peer_ref[...], w_peer_ref[...])


def conv_product(own, peer, w_own, w_peer):
    n = own.shape[0]
    tile = lambda width: pl.BlockSpec((OUT_TILE, width), lambda i: (i, 0))
    return pl.pallas_call(
        pair_kernel,
        out_shape=jax.ShapeDtypeStruct((n, D), F32),
        grid=(n // OUT_TILE,),
        in_specs=[tile(C_DEV), tile(C_DEV), resident((C_DEV, D)), resident((C_DEV, D))],
        out_specs=tile(D),
        cost_estimate=pl.CostEstimate(flops=4 * n * D * C_DEV, transcendentals=0, bytes_accessed=12 << 20),
        name="conv_product",
    )(own, peer, w_own, w_peer)


def attend_blocks(blocks, kv_ref, q_ref, gate):
    heads = MEM_DEV // MEM_HD
    lane_head = lax.broadcasted_iota(jnp.int32, (BLOCK, MEM_DEV), 1) // MEM_HD
    scores = []
    for b in blocks:
        q = q_ref[b * BLOCK : (b + 1) * BLOCK, :]
        spread = jnp.concatenate([jnp.where(lane_head == h, q, jnp.zeros_like(q)) for h in range(heads)], axis=0)
        scores.append(matmul_t(spread, kv_ref[2 * b : 2 * b + 2, :, :MEM_DEV].reshape(2 * PLEN, MEM_DEV)))
    expanded = [jnp.exp(s - jnp.max(s, axis=1, keepdims=True)) for s in scores]
    weights = [(e * (1.0 / jnp.sum(e, axis=1, keepdims=True))).astype(BF16) for e in expanded]
    rows = []
    for w, b in zip(weights, blocks):
        mixed = matmul(w, kv_ref[2 * b : 2 * b + 2, :, MEM_DEV:].reshape(2 * PLEN, MEM_DEV))
        attended = mixed[:BLOCK]
        for h in range(1, heads):
            attended = jnp.where(lane_head == h, mixed[h * BLOCK : (h + 1) * BLOCK], attended)
        rows.append((attended * gate).astype(BF16))
    return jnp.concatenate(rows, axis=0)


def read_copies(half_ref, owner_ref, recv_hbm, q_hbm, kv_ref, q_ref, sem, q_sem):
    count = kv_ref.shape[0]
    n = q_ref.shape[0]
    first = half_ref[0] * count
    q_copy = pltpu.make_async_copy(q_hbm.at[pl.ds(pl.multiple_of(half_ref[0] * n, n), n), :], q_ref, q_sem)
    return q_copy, [
        pltpu.make_async_copy(recv_hbm.at[owner_ref[first + i]], kv_ref.at[i], sem.at[i]) for i in range(count)
    ]


def attend_kernel(half_ref, owner_ref, recv_hbm, q_hbm, gate_hbm, out_ref, kv_ref, q_ref, gate_ref, sem, q_sem, gate_sem):
    q_copy, copies = read_copies(half_ref, owner_ref, recv_hbm, q_hbm, kv_ref, q_ref, sem, q_sem)
    gate_copy = pltpu.make_async_copy(gate_hbm, gate_ref, gate_sem)
    q_copy.start()
    for c in copies:
        c.start()
    gate_copy.start()
    q_copy.wait()
    gate_copy.wait()
    gate = jnp.tanh(wide_row(gate_ref))
    for group in range(0, q_ref.shape[0] // BLOCK, ATT_GROUP):
        for c in copies[2 * group : 2 * (group + ATT_GROUP)]:
            c.wait()
        blocks = range(group, group + ATT_GROUP)
        out_ref[group * BLOCK : (group + ATT_GROUP) * BLOCK, :] = attend_blocks(blocks, kv_ref, q_ref, gate)


def attend(half, owners, received, queries, gate):
    n = queries.shape[0] // 2
    count = owners.shape[0] // 2
    return pl.pallas_call(
        attend_kernel,
        out_shape=jax.ShapeDtypeStruct((n, MEM_DEV), BF16),
        grid_spec=pltpu.PrefetchScalarGridSpec(
            num_scalar_prefetch=2,
            grid=(1,),
            in_specs=[HBM, HBM, HBM],
            out_specs=pl.BlockSpec((n, MEM_DEV), lambda i, h, o: (0, 0)),
            scratch_shapes=[
                pltpu.VMEM((count, PLEN, 2 * MEM_DEV), BF16),
                pltpu.VMEM((n, MEM_DEV), BF16),
                pltpu.VMEM((MEM_DEV // LANES, LANES), BF16),
                pltpu.SemaphoreType.DMA((count,)),
                pltpu.SemaphoreType.DMA(()),
                pltpu.SemaphoreType.DMA(()),
            ],
        ),
        cost_estimate=pl.CostEstimate(flops=n * D * 256, transcendentals=0, bytes_accessed=2 << 20),
        name="attend",
    )(half, owners, received, queries, gate)


def finish_kernel(
    half_ref, owner_ref, recv_hbm, q_hbm, gate_hbm, peer_hbm, w_own_hbm, w_peer_hbm, conv_hbm, out_hbm,
    kv_ref, q_ref, gate_ref, peer_ref, w_own_ref, w_peer_ref, conv_ref, out_ref, sem, q_sem, gate_sem, w_sem, conv_sem, out_sem,
):
    q_copy, copies = read_copies(half_ref, owner_ref, recv_hbm, q_hbm, kv_ref, q_ref, sem, q_sem)
    size = ATT_GROUP * BLOCK
    groups = q_ref.shape[0] // size
    span = lambda g: pl.ds(g * size, size)
    gate_copy = pltpu.make_async_copy(gate_hbm, gate_ref, gate_sem)
    late = [
        pltpu.make_async_copy(w_own_hbm, w_own_ref, w_sem.at[0]),
        pltpu.make_async_copy(w_peer_hbm, w_peer_ref, w_sem.at[1]),
        pltpu.make_async_copy(peer_hbm, peer_ref, w_sem.at[2]),
    ]
    conv_copies = [pltpu.make_async_copy(conv_hbm.at[span(g)], conv_ref.at[span(g)], conv_sem.at[g]) for g in range(groups)]
    out_copies = [pltpu.make_async_copy(out_ref.at[span(g)], out_hbm.at[span(g)], out_sem.at[g]) for g in range(groups)]
    for c in [q_copy, *copies, gate_copy, *late, *conv_copies]:
        c.start()
    q_copy.wait()
    gate_copy.wait()
    gate = jnp.tanh(wide_row(gate_ref))
    for g in range(groups):
        for c in copies[2 * g * ATT_GROUP : 2 * (g + 1) * ATT_GROUP]:
            c.wait()
        own = attend_blocks(range(g * ATT_GROUP, (g + 1) * ATT_GROUP), kv_ref, q_ref, gate)
        if g == 0:
            for c in late:
                c.wait()
        conv_copies[g].wait()
        memory = matmul(own, w_own_ref[...]) + matmul(peer_ref[span(g), :], w_peer_ref[...])
        out_ref[span(g), :] = (conv_ref[span(g), :] + memory).astype(BF16)
        out_copies[g].start()
    for c in out_copies:
        c.wait()


def finish(half, owners, received, queries, gate, peer, w_own, w_peer, conv_sum):
    n = conv_sum.shape[0]
    count = owners.shape[0] // 2
    groups = n // (ATT_GROUP * BLOCK)
    return pl.pallas_call(
        finish_kernel,
        out_shape=jax.ShapeDtypeStruct((n, D), BF16),
        grid_spec=pltpu.PrefetchScalarGridSpec(
            num_scalar_prefetch=2,
            grid=(1,),
            in_specs=[HBM] * 7,
            out_specs=HBM,
            scratch_shapes=[
                pltpu.VMEM((count, PLEN, 2 * MEM_DEV), BF16),
                pltpu.VMEM((n, MEM_DEV), BF16),
                pltpu.VMEM((MEM_DEV // LANES, LANES), BF16),
                pltpu.VMEM((n, MEM_DEV), BF16),
                pltpu.VMEM((MEM_DEV, D), BF16),
                pltpu.VMEM((MEM_DEV, D), BF16),
                pltpu.VMEM((n, D), F32),
                pltpu.VMEM((n, D), BF16),
                pltpu.SemaphoreType.DMA((count,)),
                pltpu.SemaphoreType.DMA(()),
                pltpu.SemaphoreType.DMA(()),
                pltpu.SemaphoreType.DMA((3,)),
                pltpu.SemaphoreType.DMA((groups,)),
                pltpu.SemaphoreType.DMA((groups,)),
            ],
        ),
        cost_estimate=pl.CostEstimate(flops=5 * n * D * MEM_DEV, transcendentals=0, bytes_accessed=8 << 20),
        name="finish",
    )(half, owners, received, queries, gate, peer, w_own, w_peer, conv_sum)


def body(
    tokens,
    passage_ids,
    passage_store,
    norm_gain,
    conv_value_weight,
    conv_gate_weight,
    conv_weight,
    ln_gain,
    query_weight,
    query_gain,
    passage_gain,
    key_weight,
    value_weight,
    key_gain,
    memory_gate,
    conv_out_weight,
    memory_out_weight,
):
    owner_count = lax.axis_size("st")
    swap = [(0, 1), (1, 0)]
    me = lax.axis_index("tp").astype(jnp.int32).reshape(1)

    owner_ids = passage_ids // PASS_DEV
    local_ids = passage_ids % PASS_DEV
    everyone = jnp.arange(owner_count, dtype=jnp.int32)[:, None, None]
    wanted = jnp.sum(jnp.where(owner_ids[None] == everyone, local_ids[None], 0), axis=(1, 2))
    wanted = jnp.broadcast_to(wanted[:, None], (owner_count, LANES))
    asked = lax.all_to_all(wanted, "st", 0, 0, tiled=True)
    peer_tokens = lax.ppermute(tokens, "tp", swap)
    peer_conv_weight = lax.ppermute(conv_out_weight, "tp", swap)
    peer_memory_weight = lax.ppermute(memory_out_weight, "tp", swap)

    kv = project_store(
        passage_store.reshape(-1, D),
        passage_gain.reshape(-1, LANES),
        key_weight,
        value_weight,
        key_gain.reshape(-1, LANES),
    ).reshape(PASS_DEV, PLEN, 2 * MEM_DEV)
    sent = fill_slots(asked, kv)
    received = lax.all_to_all(sent, "st", 0, 0, tiled=True)

    filtered, own_stats, queries = token_branch(
        me,
        tokens,
        peer_tokens,
        norm_gain.reshape(2, -1, LANES),
        conv_value_weight,
        conv_gate_weight,
        query_weight,
        conv_weight,
        query_gain.reshape(-1, LANES),
    )
    peer_stats = lax.ppermute(own_stats, "tp", swap)
    conv_theirs = channel_swish(1 - me, filtered, own_stats, peer_stats, ln_gain.reshape(-1, LANES))
    conv_peer = lax.ppermute(conv_theirs, "tp", swap)
    conv_mine = channel_swish(me, filtered, own_stats, peer_stats, ln_gain.reshape(-1, LANES))
    conv_sum = conv_product(conv_mine, conv_peer, conv_out_weight, peer_conv_weight)

    received, conv_sum = lax.optimization_barrier((received, conv_sum))
    owners = owner_ids.reshape(-1)
    gate = memory_gate.reshape(-1, LANES)
    memory_theirs = attend(1 - me, owners, received, queries, gate)
    memory_peer = lax.ppermute(memory_theirs, "tp", swap)
    return finish(
        me, owners, received, queries, gate, memory_peer, memory_out_weight, peer_memory_weight, conv_sum
    )


def solution(mesh):
    return jax.shard_map(
        body,
        mesh=mesh,
        in_specs=(
            P("st", "tp"),
            P("st", None),
            P("st", None, None),
            P(),
            P(None, "tp"),
            P(None, "tp"),
            P(None, "tp"),
            P("tp"),
            P(None, "tp"),
            P("tp"),
            P(),
            P(None, "tp"),
            P(None, "tp"),
            P("tp"),
            P("tp"),
            P("tp", None),
            P("tp", None),
        ),
        out_specs=P(("st", "tp"), None),
        check_vma=False,
    )
```

time: 121 us -> 107 us (0.88)
  other arithmetic: 11.1 us -> 0.78 us
  Pallas kernels: 72.6 us -> 63.4 us
  waiting for transfers between devices: 6.69 us -> 9.49 us
  starting transfers between devices: 25.7 us -> 28.1 us
    pallas_call x1, Pallas kernels: 31.4 us -> 24.8 us  [token_branch(): pl.pallas_call(token_kernel, out_shape=(jax.ShapeDtypeStruct((n, C_DEV),...]
    convert_element_type x2 -> x0, other arithmetic: 4.33 us -> none  [the longest x1 3.69 us: body(): return (mine.astype(F32) + from_peer.astype(F32)).astype(BF16)]
    pallas_call x3 -> x5, Pallas kernels: 27.9 us -> 24.7 us  [the longest x1 8.03 us: conv_product(): pl.pallas_call(pair_kernel, out_shape=jax.ShapeDtypeStruct((n, D), F32),...]
    reshape x3 -> x0, other arithmetic: 3.08 us -> none  [the longest x2 2.48 us: body(): row = lambda v: v.astype(F32).reshape(1, -1)]
    ppermute x1 -> x4, starting transfers between devices: 1.81 us -> 3.89 us  [the longest x1 3.37 us: body(): memory_peer = lax.ppermute(memory_theirs, 'tp', swap)]
    ppermute x1, waiting for transfers between devices: 0.01 us -> 1.88 us  [body(): peer_stats = lax.ppermute(own_stats, 'tp', swap)]
    all_to_all x1 -> x0, other arithmetic: 1.76 us -> none  [body(): lax.all_to_all(wanted.reshape(owner_count, 1), 'st', 0, 0, tiled=True)]
    ppermute x1 -> x4, waiting for transfers between devices: 0.01 us -> 1.38 us  [the longest x1 1.37 us: body(): memory_peer = lax.ppermute(memory_theirs, 'tp', swap)]
  transfers between devices with their start and end apart: 5 -> 8, of which waited for: 1 -> 3; matrix products, arithmetic and copies ran while one was open for 8% -> 2% of each run, Pallas kernels for 53% -> 53%
where the time goes in v1:
time: 107 us; the launch traced here: 106 us
  Pallas kernels  63.4 us (59%)
  starting transfers between devices  28.1 us (26%)
  waiting for transfers between devices  9.49 us (9%)
  local copies, waits for them, and re-layouts  4.36 us (4%)
    pallas_call x1, Pallas kernels, token_branch(): pl.pallas_call(token_kernel, out_shape=(jax.ShapeDtypeStruct((n, C_DEV),...  24.8 us
    all_to_all x1, starting transfers between devices, body(): asked = lax.all_to_all(wanted, 'st', 0, 0, tiled=True)  11.2 us
    all_to_all x1, starting transfers between devices, body(): received = lax.all_to_all(sent, 'st', 0, 0, tiled=True)  10.2 us
    pallas_call x1, Pallas kernels, project_store(): pl.pallas_call(kv_kernel, out_shape=jax.ShapeDtypeStruct((n, 2 * MEM_DEV)...  8.84 us
    pallas_call x1, Pallas kernels, conv_product(): pl.pallas_call(pair_kernel, out_shape=jax.ShapeDtypeStruct((n, D), F32),...  8.03 us
    pallas_call x1, Pallas kernels, finish(): pl.pallas_call(finish_kernel, out_shape=jax.ShapeDtypeStruct((n, D), BF16...  7.22 us
    all_to_all x1, waiting for transfers between devices, body(): received = lax.all_to_all(sent, 'st', 0, 0, tiled=True)  6.23 us
    pallas_call x2, Pallas kernels, channel_swish(): pl.pallas_call(lambda half_ref, *refs: swish_kernel(*refs), out_shape=jax...  5.3 us
  transfers between devices with their start and end apart: 8, of which 3 were waited for; matrix products, arithmetic and copies ran while one was open for 2% of the time, Pallas kernels for 53%

profile of v1, /device:TPU:1, one launch (start us, length us, event | category | flops | bytes accessed | tf_op | source)
XLA Modules:
  0.0 106.3 jit_solution(13746568321714352381)
XLA Ops:
  0.0 1.4 %collective-permute-start = (bf16[1024,1024]{1,0:T(8,128)(2,1)}, bf16[1024,1024]{1,0:T(8,128)(2,1)}, u32[]{:S(2)}, u32[]{:S(2)}) collective-permute-start(bf16[1024,1024]{1,0:T(8,128)(2,1)} %own_ref.1), channel_id=1, source_target_pairs={{0,1},{1,0},{2,3},{3,2},{4,5},{5,4},{6,7},{7,6},{8,9},{9,8},{10,11... | collective-permute-start | bytes 6291464 | tf_op jit(solution)/shard_map/ppermute | solution.py:459
  1.4 0.0 collective-permute-start.3
  1.4 0.7 and_select_fusion
  2.1 0.1 select_reduce_fusion
  2.2 0.8 broadcast_in_dim.23
  2.9 11.2 %all-to-all-start = ((s32[64,1,128]{2,1,0:T(1,128)}), s32[64,1,128]{2,1,0:T(1,128)S(1)}, u32[]{:S(2)}, u32[]{:S(2)}) async-start(s32[64,1,128]{2,1,0:T(1,128)} %broadcast_in_dim.23), calls=%async_computation | async-start | bytes 65536 | tf_op jit(solution)/shard_map/all_to_all | solution.py:458
  14.2 8.8 %project_store.1 = bf16[1024,512]{1,0:T(8,128)(2,1)} custom-call(bf16[1024,2048]{1,0:T(8,128)(2,1)} %bitcast.16, bf16[16,128]{1,0:T(8,128)(2,1)} %bitcast.17, bf16[2048,256]{1,0:T(8,128)(2,1)} %wk_hbm.1, bf16[2048,256]{1,0:T(8,128)(2,1)} %wv_hbm.1, bf16[2,128]{1,0:T(2,128)(2,1)} %bitcast.19), custom_call_target="tpu_custom_call" | custom-call | flops 2147483648 | bytes 8388608 | tf_op jit(solution)/shard_map/project_store/pallas_call | solution.py:116
  23.0 0.0 all-to-all-done
  23.0 0.0 copy-start.2
  23.0 0.6 copy-done.2
  23.6 4.9 %fill_slots.1 = bf16[64,64,512]{2,1,0:T(8,128)(2,1)} custom-call(s32[64,128]{1,0:T(8,128)} %bitcast.11, bf16[16,64,512]{2,1,0:T(8,128)(2,1)} %bitcast.10), custom_call_target="tpu_custom_call" | custom-call | tf_op jit(solution)/shard_map/fill_slots/pallas_call | solution.py:149
  28.6 10.2 %all-to-all-start.1 = ((bf16[64,64,512]{2,1,0:T(8,128)(2,1)}), bf16[64,64,512]{2,1,0:T(8,128)(2,1)}, u32[]{:S(2)}, u32[]{:S(2)}) async-start(bf16[64,64,512]{2,1,0:T(8,128)(2,1)} %fill_slots.1), calls=%async_computation.1 | async-start | bytes 8388608 | tf_op jit(solution)/shard_map/all_to_all | solution.py:471
  38.8 0.0 collective-permute-done.peer_ref
  38.9 24.8 %token_branch.1 = (f32[1024,768]{1,0:T(8,128)}, f32[1024,2]{1,0:T(8,128)}, bf16[1024,256]{1,0:T(8,128)(2,1)}) custom-call(s32[1]{0:T(128)} %bitcast.tp_ref.half_ref, bf16[1024,1024]{1,0:T(8,128)(2,1)} %own_ref.1, bf16[1024,1024]{1,0:T(8,128)(2,1)} %collective-permute-done.peer_ref, bf16[2,8,128]{2,1,0:T(8,128)(2,1)} %bitcast.18, bf16[2048,768]{1,0:T(8,128)(2,1)} %wv_ref.1, ...), custom_call_target="tpu_custom_call" | custom-call | flops 32212254720 | bytes 16777216 | tf_op jit(solution)/shard_map/token_branch/pallas_call | solution.py:216
  63.7 1.3 %collective-permute-start.1 = (f32[1024,2]{1,0:T(8,128)}, f32[1024,2]{1,0:T(8,128)}, u32[]{:S(2)}, u32[]{:S(2)}) collective-permute-start(f32[1024,2]{1,0:T(8,128)} %get-tuple-element.11.refs_1_), channel_id=1, source_target_pairs={{0,1},{1,0},{2,3},{3,2},{4,5},{5,4},{6,7},{7,6},{8,9},{9,8},{10,11... | collective-permute-start | bytes 24584 | tf_op jit(solution)/shard_map/ppermute | solution.py:484
  65.0 1.9 %collective-permute-done.1.refs_2_ = f32[1024,2]{1,0:T(8,128)} collective-permute-done((f32[1024,2]{1,0:T(8,128)}, f32[1024,2]{1,0:T(8,128)}, u32[]{:S(2)}, u32[]{:S(2)}) %collective-permute-start.1) | collective-permute-done | bytes 8224 | tf_op jit(solution)/shard_map/ppermute | solution.py:484
  66.9 2.7 %channel_swish.3 = bf16[512,768]{1,0:T(8,128)(2,1)} custom-call(s32[1]{0:T(128)S(6)} %sub.11.half_ref, f32[1024,768]{1,0:T(8,128)} %get-tuple-element.10.refs_0_, f32[1024,2]{1,0:T(8,128)} %get-tuple-element.11.refs_1_, f32[1024,2]{1,0:T(8,128)} %collective-permute-done.1.refs_2_, bf16[6,128]{1,0:T(8,128)(2,1)} %bitcast.12), custom_call_target="tpu_custom_call" | custom-call | flops 805306368 | bytes 4194304 | tf_op jit(solution)/shard_map/channel_swish/pallas_call | solution.py:256
  69.6 0.4 collective-permute-start.2
  69.9 0.1 collective-permute-start.5
  70.1 0.1 copy.27
  70.2 0.6 reshape.40.owner_ref
  70.7 2.6 %channel_swish.2.own_ref = bf16[512,768]{1,0:T(8,128)(2,1)} custom-call(s32[1]{0:T(128)} %bitcast.tp_ref.half_ref, f32[1024,768]{1,0:T(8,128)} %get-tuple-element.10.refs_0_, f32[1024,2]{1,0:T(8,128)} %get-tuple-element.11.refs_1_, f32[1024,2]{1,0:T(8,128)} %collective-permute-done.1.refs_2_, bf16[6,128]{1,0:T(8,128)(2,1)} %bitcast.13), custom_call_target="tpu_custom_call" | custom-call | flops 805306368 | bytes 4194304 | tf_op jit(solution)/shard_map/channel_swish/pallas_call | solution.py:256
  73.4 0.0 collective-permute-done.2.peer_ref
  73.4 0.0 collective-permute-done.3.w_peer_ref
  73.4 0.0 copy-start
  73.4 1.6 %copy-done = bf16[768,2048]{1,0:T(8,128)(2,1)} copy-done((bf16[768,2048]{1,0:T(8,128)(2,1)}, bf16[768,2048]{1,0:T(8,128)(2,1)S(1)}, u32[]{:S(2)}) %copy-start) | copy-done | bytes 3145752
  75.0 8.0 %conv_product.1.conv_hbm = f32[512,2048]{1,0:T(8,128)} custom-call(bf16[512,768]{1,0:T(8,128)(2,1)} %channel_swish.2.own_ref, bf16[512,768]{1,0:T(8,128)(2,1)} %collective-permute-done.2.peer_ref, bf16[768,2048]{1,0:T(8,128)(2,1)} %w_own_ref.1, bf16[768,2048]{1,0:T(8,128)(2,1)} %copy-done), custom_call_target="tpu_custom_call" | custom-call | flops 3221225472 | bytes 12582912 | tf_op jit(solution)/shard_map/conv_product/pallas_call | solution.py:277
  83.1 6.2 %all-to-all-done.1.recv_hbm = bf16[64,64,512]{2,1,0:T(8,128)(2,1)} async-done(((bf16[64,64,512]{2,1,0:T(8,128)(2,1)}), bf16[64,64,512]{2,1,0:T(8,128)(2,1)}, u32[]{:S(2)}, u32[]{:S(2)}) %all-to-all-start.1) | async-done | bytes 4194336 | tf_op jit(solution)/shard_map/all_to_all | solution.py:471
  89.3 4.2 %attend.1 = bf16[512,256]{1,0:T(8,128)(2,1)} custom-call(s32[1]{0:T(128)S(6)} %sub.11.half_ref, s32[32]{0:T(128)} %reshape.40.owner_ref, bf16[64,64,512]{2,1,0:T(8,128)(2,1)} %all-to-all-done.1.recv_hbm, bf16[1024,256]{1,0:T(8,128)(2,1)} %get-tuple-element.13.q_hbm, bf16[2,128]{1,0:T(2,128)(2,1)} %bitcast.14), custom_call_target="tpu_custom_call" | custom-call | flops 268435456 | bytes 2097152 | tf_op jit(solution)/shard_map/attend/pallas_call | solution.py:338
  93.5 3.4 %collective-permute-start.4 = (bf16[512,256]{1,0:T(8,128)(2,1)}, bf16[512,256]{1,0:T(8,128)(2,1)S(1)}, u32[]{:S(2)}, u32[]{:S(2)}) collective-permute-start(bf16[512,256]{1,0:T(8,128)(2,1)} %attend.1), channel_id=1, source_target_pairs={{0,1},{1,0},{2,3},{3,2},{4,5},{5,4},{6,7},{7,6},{8,9},{9,8},{10,11... | collective-permute-start | bytes 786440 | tf_op jit(solution)/shard_map/ppermute | solution.py:494
  96.9 0.0 collective-permute-done.5.w_peer_hbm
  96.9 1.4 %collective-permute-done.4.peer_hbm = bf16[512,256]{1,0:T(8,128)(2,1)S(1)} collective-permute-done((bf16[512,256]{1,0:T(8,128)(2,1)}, bf16[512,256]{1,0:T(8,128)(2,1)S(1)}, u32[]{:S(2)}, u32[]{:S(2)}) %collective-permute-start.4) | collective-permute-done | bytes 262176 | tf_op jit(solution)/shard_map/ppermute | solution.py:494
  98.3 0.0 copy-start.1
  98.3 0.7 copy-done.1
  99.0 7.2 %finish.1 = bf16[512,2048]{1,0:T(8,128)(2,1)} custom-call(s32[1]{0:T(128)} %bitcast.tp_ref.half_ref, s32[32]{0:T(128)} %reshape.40.owner_ref, bf16[64,64,512]{2,1,0:T(8,128)(2,1)} %all-to-all-done.1.recv_hbm, bf16[1024,256]{1,0:T(8,128)(2,1)} %get-tuple-element.13.q_hbm, bf16[2,128]{1,0:T(2,128)(2,1)} %bitcast.15, bf16[512,256]{1,0:T(8,128)(2,1)} %copy-done.1, ...), custom_call_target="tpu_custom_call" | custom-call | flops 1342177280 | bytes 8388608 | tf_op jit(solution)/shard_map/finish/pallas_call | solution.py:400
Async XLA Ops:
  0.0 38.8 %collective-permute-start = (bf16[1024,1024]{1,0:T(8,128)(2,1)}, bf16[1024,1024]{1,0:T(8,128)(2,1)}, u32[]{:S(2)}, u32[]{:S(2)}) collective-permute-start(bf16[1024,1024]{1,0:T(8,128)(2,1)} %own_ref.1), channel_id=1, source_target_pairs={{0,1},{1,0},{2,3},{3,2},{4,5},{5,4},{6,7},{7,6},{8,9},{9,8},{10,11... | collective-permute-start | bytes 6291464 | tf_op jit(solution)/shard_map/ppermute | solution.py:459
  1.4 72.0 %collective-permute-start.3 = (bf16[768,2048]{1,0:T(8,128)(2,1)}, bf16[768,2048]{1,0:T(8,128)(2,1)S(1)}, u32[]{:S(2)}, u32[]{:S(2)}) collective-permute-start(bf16[768,2048]{1,0:T(8,128)(2,1)} %w_own_ref.1), channel_id=1, source_target_pairs={{0,1},{1,0},{2,3},{3,2},{4,5},{5,4},{6,7},{7,6},{8,9},{9,8},{10,11... | collective-permute-start | bytes 9437192 | tf_op jit(solution)/shard_map/ppermute | solution.py:460
  2.9 20.1 %all-to-all-start = ((s32[64,1,128]{2,1,0:T(1,128)}), s32[64,1,128]{2,1,0:T(1,128)S(1)}, u32[]{:S(2)}, u32[]{:S(2)}) async-start(s32[64,1,128]{2,1,0:T(1,128)} %broadcast_in_dim.23), calls=%async_computation | async-start | bytes 65536 | tf_op jit(solution)/shard_map/all_to_all | solution.py:458
  23.0 0.6 copy-start.2
  28.6 60.7 %all-to-all-start.1 = ((bf16[64,64,512]{2,1,0:T(8,128)(2,1)}), bf16[64,64,512]{2,1,0:T(8,128)(2,1)}, u32[]{:S(2)}, u32[]{:S(2)}) async-start(bf16[64,64,512]{2,1,0:T(8,128)(2,1)} %fill_slots.1), calls=%async_computation.1 | async-start | bytes 8388608 | tf_op jit(solution)/shard_map/all_to_all | solution.py:471
  63.7 3.2 %collective-permute-start.1 = (f32[1024,2]{1,0:T(8,128)}, f32[1024,2]{1,0:T(8,128)}, u32[]{:S(2)}, u32[]{:S(2)}) collective-permute-start(f32[1024,2]{1,0:T(8,128)} %get-tuple-element.11.refs_1_), channel_id=1, source_target_pairs={{0,1},{1,0},{2,3},{3,2},{4,5},{5,4},{6,7},{7,6},{8,9},{9,8},{10,11... | collective-permute-start | bytes 24584 | tf_op jit(solution)/shard_map/ppermute | solution.py:484
  69.6 3.8 %collective-permute-start.2 = (bf16[512,768]{1,0:T(8,128)(2,1)}, bf16[512,768]{1,0:T(8,128)(2,1)}, u32[]{:S(2)}, u32[]{:S(2)}) collective-permute-start(bf16[512,768]{1,0:T(8,128)(2,1)} %channel_swish.3), channel_id=1, source_target_pairs={{0,1},{1,0},{2,3},{3,2},{4,5},{5,4},{6,7},{7,6},{8,9},{9,8},{10,11... | collective-permute-start | bytes 2359304 | tf_op jit(solution)/shard_map/ppermute | solution.py:486
  69.9 26.9 %collective-permute-start.5 = (bf16[256,2048]{1,0:T(8,128)(2,1)}, bf16[256,2048]{1,0:T(8,128)(2,1)}, u32[]{:S(2)}, u32[]{:S(2)}) collective-permute-start(bf16[256,2048]{1,0:T(8,128)(2,1)} %w_own_hbm.1), channel_id=1, source_target_pairs={{0,1},{1,0},{2,3},{3,2},{4,5},{5,4},{6,7},{7,6},{8,9},{9,8},{10,11... | collective-permute-start | bytes 3145736 | tf_op jit(solution)/shard_map/ppermute | solution.py:461
  73.4 1.6 %copy-start = (bf16[768,2048]{1,0:T(8,128)(2,1)}, bf16[768,2048]{1,0:T(8,128)(2,1)S(1)}, u32[]{:S(2)}) copy-start(bf16[768,2048]{1,0:T(8,128)(2,1)S(1)} %collective-permute-done.3.w_peer_ref) | copy-start | bytes 9437188
  93.5 4.7 %collective-permute-start.4 = (bf16[512,256]{1,0:T(8,128)(2,1)}, bf16[512,256]{1,0:T(8,128)(2,1)S(1)}, u32[]{:S(2)}, u32[]{:S(2)}) collective-permute-start(bf16[512,256]{1,0:T(8,128)(2,1)} %attend.1), channel_id=1, source_target_pairs={{0,1},{1,0},{2,3},{3,2},{4,5},{5,4},{6,7},{7,6},{8,9},{9,8},{10,11... | collective-permute-start | bytes 786440 | tf_op jit(solution)/shard_map/ppermute | solution.py:494
  98.3 0.7 copy-start.1

commit v2 on v1

--- a/solution.py
+++ b/solution.py
@@ -27,6 +27,7 @@
 ATT_GROUP = 4
 LANES = 128
 CONV_ROWS = 128
+NORM_ROWS = 16
 HISTORY = 32
 
 F32 = jnp.float32
@@ -64,30 +65,29 @@
     return jnp.concatenate([values[i : i + 1, :] for i in range(values.shape[0])], axis=1)
 
 
-def kv_kernel(rows_hbm, gain_ref, wk_hbm, wv_hbm, kg_ref, out_hbm, rows_ref, wk_ref, wv_ref, out_ref, even, odd, r_sem, w_sem, o_sem):
+def kv_kernel(
+    rows_hbm, gain_hbm, wk_hbm, wv_hbm, kg_hbm, out_ref,
+    rows_ref, gain_ref, wk_ref, wv_ref, kg_ref, even, odd, r_sem, w_sem
+):
     chunks = rows_hbm.shape[0] // KV_TILE
     span = lambda c: pl.ds(c * KV_TILE, KV_TILE)
     row_copies = [pltpu.make_async_copy(rows_hbm.at[span(c)], rows_ref.at[span(c)], r_sem.at[c]) for c in range(chunks)]
-    out_copies = [pltpu.make_async_copy(out_ref.at[span(c)], out_hbm.at[span(c)], o_sem.at[c]) for c in range(chunks)]
     wk_copy = pltpu.make_async_copy(wk_hbm, wk_ref, w_sem.at[0])
     wv_copy = pltpu.make_async_copy(wv_hbm, wv_ref, w_sem.at[1])
-    row_copies[0].start()
-    wk_copy.start()
-    wv_copy.start()
-    for c in range(1, chunks):
-        row_copies[c].start()
+    gain_copy = pltpu.make_async_copy(gain_hbm, gain_ref, w_sem.at[2])
+    kg_copy = pltpu.make_async_copy(kg_hbm, kg_ref, w_sem.at[3])
+    for c in [gain_copy, kg_copy, row_copies[0], wk_copy, wv_copy, *row_copies[1:]]:
+        c.start()
+    gain_copy.wait()
+    kg_copy.wait()
     gain = wide_row(gain_ref)
     key_gain = wide_row(kg_ref)
     held = (even, odd)
 
     def normalise(c):
-        held[c % 2][...] = row_norm(rows_ref[span(c), :], gain)
-
-    def project(c):
-        normed = held[c % 2][...]
-        keys = head_norm(matmul(normed, wk_ref[...]), key_gain)
-        out_ref[span(c), :MEM_DEV] = keys.astype(BF16)
-        out_ref[span(c), MEM_DEV:] = matmul(normed, wv_ref[...]).astype(BF16)
+        for r in range(0, KV_TILE, NORM_ROWS):
+            rows = rows_ref[c * KV_TILE + r : c * KV_TILE + r + NORM_ROWS, :]
+            held[c % 2][r : r + NORM_ROWS, :] = row_norm(rows, gain)
 
     row_copies[0].wait()
     normalise(0)
@@ -97,10 +97,9 @@
         if c + 1 < chunks:
             row_copies[c + 1].wait()
             normalise(c + 1)
-        project(c)
-        out_copies[c].start()
-    for c in range(chunks):
-        out_copies[c].wait()
+        keys = head_norm(matmul(held[c % 2][...], wk_ref[...]), key_gain)
+        out_ref[span(c), :MEM_DEV] = keys.astype(BF16)
+        out_ref[span(c), MEM_DEV:] = matmul(held[c % 2][...], wv_ref[...]).astype(BF16)
 
 
 def resident(shape):
@@ -109,35 +108,51 @@
 
 
 HBM = pl.BlockSpec(memory_space=pl.ANY)
+ONCHIP = pl.BlockSpec(memory_space=pltpu.VMEM)
+
+
+def onchip(*arrays):
+    return tuple(pltpu.with_memory_space_constraint(a, pltpu.VMEM) for a in arrays)
+
+
+def offchip(*arrays):
+    return tuple(pltpu.with_memory_space_constraint(a, pltpu.HBM) for a in arrays)
+
+
+def grant(mib):
+    return pltpu.CompilerParams(vmem_limit_bytes=mib << 20)
 
 
 def project_store(rows, passage_gain, key_weight, value_weight, key_gain):
     n = rows.shape[0]
     return pl.pallas_call(
         kv_kernel,
-        out_shape=jax.ShapeDtypeStruct((n, 2 * MEM_DEV), BF16),
-        grid=(1,),
-        in_specs=[HBM, resident((D // LANES, LANES)), HBM, HBM, resident((MEM_DEV // LANES, LANES))],
-        out_specs=HBM,
+        out_shape=pltpu.VMEM((n, 2 * MEM_DEV), BF16),
+        in_specs=[HBM] * 5,
+        out_specs=ONCHIP,
         scratch_shapes=[
             pltpu.VMEM((n, D), BF16),
+            pltpu.VMEM((D // LANES, LANES), BF16),
             pltpu.VMEM((D, MEM_DEV), BF16),
             pltpu.VMEM((D, MEM_DEV), BF16),
-            pltpu.VMEM((n, 2 * MEM_DEV), BF16),
+            pltpu.VMEM((MEM_DEV // LANES, LANES), BF16),
             pltpu.VMEM((KV_TILE, D), BF16),
             pltpu.VMEM((KV_TILE, D), BF16),
             pltpu.SemaphoreType.DMA((n // KV_TILE,)),
-            pltpu.SemaphoreType.DMA((2,)),
-            pltpu.SemaphoreType.DMA((n // KV_TILE,)),
+            pltpu.SemaphoreType.DMA((4,)),
         ],
+        compiler_params=grant(24),
         cost_estimate=pl.CostEstimate(flops=2 * n * D * 2 * MEM_DEV, transcendentals=0, bytes_accessed=8 << 20),
         name="project_store",
-    )(rows, passage_gain, key_weight, value_weight, key_gain)
-
-
-def slots_kernel(asked_ref, kv_ref, out_ref, sem):
+    )(*offchip(rows, passage_gain, key_weight, value_weight, key_gain))
+
+
+def slots_kernel(asked_ref, kv_ref, out_ref, table, table_sem, sem):
     count = out_ref.shape[0]
-    copies = [pltpu.make_async_copy(kv_ref.at[asked_ref[s, 0]], out_ref.at[s], sem.at[s]) for s in range(count)]
+    fetch = pltpu.make_async_copy(asked_ref, table, table_sem)
+    fetch.start()
+    fetch.wait()
+    copies = [pltpu.make_async_copy(kv_ref.at[table[s, 0]], out_ref.at[s], sem.at[s]) for s in range(count)]
     for c in copies:
         c.start()
     for c in copies:
@@ -148,34 +163,41 @@
     count = asked.shape[0]
     return pl.pallas_call(
         slots_kernel,
-        out_shape=jax.ShapeDtypeStruct((count, PLEN, 2 * MEM_DEV), BF16),
-        grid_spec=pltpu.PrefetchScalarGridSpec(
-            num_scalar_prefetch=1,
-            grid=(1,),
-            in_specs=[pl.BlockSpec((PASS_DEV, PLEN, 2 * MEM_DEV), lambda i, s: (0, 0, 0))],
-            out_specs=pl.BlockSpec(memory_space=pl.ANY),
-            scratch_shapes=[pltpu.SemaphoreType.DMA((count,))],
-        ),
+        out_shape=pltpu.HBM((count, PLEN, 2 * MEM_DEV), BF16),
+        in_specs=[ONCHIP, ONCHIP],
+        out_specs=HBM,
+        scratch_shapes=[
+            pltpu.SMEM(asked.shape, jnp.int32),
+            pltpu.SemaphoreType.DMA(()),
+            pltpu.SemaphoreType.DMA((count,)),
+        ],
+        compiler_params=grant(2),
         name="fill_slots",
-    )(asked, kv)
+    )(*onchip(asked, kv))
 
 
 def token_kernel(
-    tp_ref, own_ref, peer_ref, gain_ref, wv_ref, wg_ref, wq_ref, cw_ref, qg_ref, filt_ref, stat_ref, q_ref, xs_ref, taps_ref
+    tp_ref, own_ref, peer_ref, gain_ref, wv_ref, wg_ref, wq_ref, cw_ref, qg_ref, filt_ref, stat_ref, q_ref, xs_ref, taps_ref,
+    own_n, peer_n
 ):
     tile = pl.program_id(0)
     me = tp_ref[0]
     own_at = pl.multiple_of(me * HALF_D, HALF_D)
     peer_at = pl.multiple_of((1 - me) * HALF_D, HALF_D)
-    own = own_ref[...].astype(F32)
-    peer = peer_ref[...].astype(F32)
-    total = jnp.sum(own * own, axis=1, keepdims=True) + jnp.sum(peer * peer, axis=1, keepdims=True)
-    factor = lax.rsqrt(total * (1.0 / D) + NORM_EPS)
-    own_n = (own * factor * wide_row(gain_ref.at[me])).astype(BF16)
-    peer_n = (peer * factor * wide_row(gain_ref.at[1 - me])).astype(BF16)
+    own_gain = wide_row(gain_ref.at[me])
+    peer_gain = wide_row(gain_ref.at[1 - me])
+    for r in range(0, TOK_TILE, NORM_ROWS):
+        rows = slice(r, r + NORM_ROWS)
+        own = own_ref[rows, :].astype(F32)
+        peer = peer_ref[rows, :].astype(F32)
+        total = jnp.sum(own * own + peer * peer, axis=1, keepdims=True)
+        factor = lax.rsqrt(total * (1.0 / D) + NORM_EPS)
+        own_n[rows, :] = (own * factor * own_gain).astype(BF16)
+        peer_n[rows, :] = (peer * factor * peer_gain).astype(BF16)
 
     def product(w_ref):
-        return matmul(own_n, w_ref[pl.ds(own_at, HALF_D), :]) + matmul(peer_n, w_ref[pl.ds(peer_at, HALF_D), :])
+        own_part = matmul(own_n[...], w_ref[pl.ds(own_at, HALF_D), :])
+        return own_part + matmul(peer_n[...], w_ref[pl.ds(peer_at, HALF_D), :])
 
     q_ref[...] = head_norm(product(wq_ref), wide_row(qg_ref) * MEM_HD ** (-0.5)).astype(BF16)
     gated = (product(wv_ref) * jax.nn.sigmoid(product(wg_ref))).astype(BF16)
@@ -234,7 +256,12 @@
                 resident((MEM_DEV // LANES, LANES)),
             ],
             out_specs=(tile(C_DEV), tile(2), tile(MEM_DEV)),
-            scratch_shapes=[pltpu.VMEM((HISTORY + TOK_TILE, C_DEV), F32), pltpu.VMEM((KW, C_DEV), F32)],
+            scratch_shapes=[
+                pltpu.VMEM((HISTORY + TOK_TILE, C_DEV), F32),
+                pltpu.VMEM((KW, C_DEV), F32),
+                pltpu.VMEM((TOK_TILE, HALF_D), BF16),
+                pltpu.VMEM((TOK_TILE, HALF_D), BF16),
+            ],
         ),
         cost_estimate=pl.CostEstimate(flops=20 * n * D * 768, transcendentals=0, bytes_accessed=16 << 20),
         name="token_branch",
@@ -315,77 +342,63 @@
     ]
 
 
-def attend_kernel(half_ref, owner_ref, recv_hbm, q_hbm, gate_hbm, out_ref, kv_ref, q_ref, gate_ref, sem, q_sem, gate_sem):
+SCALARS = pl.BlockSpec(memory_space=pltpu.SMEM)
+
+
+def read_scratch(count, n):
+    return [
+        pltpu.VMEM((count, PLEN, 2 * MEM_DEV), BF16),
+        pltpu.VMEM((n, MEM_DEV), BF16),
+        pltpu.SemaphoreType.DMA((count,)),
+        pltpu.SemaphoreType.DMA(()),
+    ]
+
+
+def attend_kernel(half_ref, owner_ref, recv_hbm, q_hbm, gate_ref, out_ref, kv_ref, q_ref, sem, q_sem):
     q_copy, copies = read_copies(half_ref, owner_ref, recv_hbm, q_hbm, kv_ref, q_ref, sem, q_sem)
-    gate_copy = pltpu.make_async_copy(gate_hbm, gate_ref, gate_sem)
-    q_copy.start()
-    for c in copies:
+    for c in [q_copy, *copies]:
         c.start()
-    gate_copy.start()
+    gate = jnp.tanh(wide_row(gate_ref))
+    size = ATT_GROUP * BLOCK
     q_copy.wait()
-    gate_copy.wait()
-    gate = jnp.tanh(wide_row(gate_ref))
-    for group in range(0, q_ref.shape[0] // BLOCK, ATT_GROUP):
-        for c in copies[2 * group : 2 * (group + ATT_GROUP)]:
+    for g in range(out_ref.shape[0] // size):
+        for c in copies[2 * g * ATT_GROUP : 2 * (g + 1) * ATT_GROUP]:
             c.wait()
-        blocks = range(group, group + ATT_GROUP)
-        out_ref[group * BLOCK : (group + ATT_GROUP) * BLOCK, :] = attend_blocks(blocks, kv_ref, q_ref, gate)
+        blocks = range(g * ATT_GROUP, (g + 1) * ATT_GROUP)
+        out_ref[pl.ds(g * size, size), :] = attend_blocks(blocks, kv_ref, q_ref, gate)
 
 
 def attend(half, owners, received, queries, gate):
     n = queries.shape[0] // 2
-    count = owners.shape[0] // 2
     return pl.pallas_call(
         attend_kernel,
-        out_shape=jax.ShapeDtypeStruct((n, MEM_DEV), BF16),
-        grid_spec=pltpu.PrefetchScalarGridSpec(
-            num_scalar_prefetch=2,
-            grid=(1,),
-            in_specs=[HBM, HBM, HBM],
-            out_specs=pl.BlockSpec((n, MEM_DEV), lambda i, h, o: (0, 0)),
-            scratch_shapes=[
-                pltpu.VMEM((count, PLEN, 2 * MEM_DEV), BF16),
-                pltpu.VMEM((n, MEM_DEV), BF16),
-                pltpu.VMEM((MEM_DEV // LANES, LANES), BF16),
-                pltpu.SemaphoreType.DMA((count,)),
-                pltpu.SemaphoreType.DMA(()),
-                pltpu.SemaphoreType.DMA(()),
-            ],
-        ),
+        out_shape=pltpu.VMEM((n, MEM_DEV), BF16),
+        in_specs=[SCALARS, SCALARS, HBM, HBM, ONCHIP],
+        out_specs=ONCHIP,
+        scratch_shapes=read_scratch(owners.shape[0] // 2, n),
+        compiler_params=grant(8),
         cost_estimate=pl.CostEstimate(flops=n * D * 256, transcendentals=0, bytes_accessed=2 << 20),
         name="attend",
-    )(half, owners, received, queries, gate)
+    )(half, owners, *offchip(received, queries), *onchip(gate))
 
 
 def finish_kernel(
-    half_ref, owner_ref, recv_hbm, q_hbm, gate_hbm, peer_hbm, w_own_hbm, w_peer_hbm, conv_hbm, out_hbm,
-    kv_ref, q_ref, gate_ref, peer_ref, w_own_ref, w_peer_ref, conv_ref, out_ref, sem, q_sem, gate_sem, w_sem, conv_sem, out_sem,
+    half_ref, owner_ref, recv_hbm, q_hbm, gate_ref, peer_ref, w_own_ref, w_peer_ref, conv_ref, out_hbm,
+    kv_ref, q_ref, sem, q_sem, out_ref, out_sem
 ):
     q_copy, copies = read_copies(half_ref, owner_ref, recv_hbm, q_hbm, kv_ref, q_ref, sem, q_sem)
+    for c in [q_copy, *copies]:
+        c.start()
+    gate = jnp.tanh(wide_row(gate_ref))
     size = ATT_GROUP * BLOCK
-    groups = q_ref.shape[0] // size
+    groups = out_ref.shape[0] // size
     span = lambda g: pl.ds(g * size, size)
-    gate_copy = pltpu.make_async_copy(gate_hbm, gate_ref, gate_sem)
-    late = [
-        pltpu.make_async_copy(w_own_hbm, w_own_ref, w_sem.at[0]),
-        pltpu.make_async_copy(w_peer_hbm, w_peer_ref, w_sem.at[1]),
-        pltpu.make_async_copy(peer_hbm, peer_ref, w_sem.at[2]),
-    ]
-    conv_copies = [pltpu.make_async_copy(conv_hbm.at[span(g)], conv_ref.at[span(g)], conv_sem.at[g]) for g in range(groups)]
     out_copies = [pltpu.make_async_copy(out_ref.at[span(g)], out_hbm.at[span(g)], out_sem.at[g]) for g in range(groups)]
-    for c in [q_copy, *copies, gate_copy, *late, *conv_copies]:
-        c.start()
     q_copy.wait()
-    gate_copy.wait()
-    gate = jnp.tanh(wide_row(gate_ref))
     for g in range(groups):
         for c in copies[2 * g * ATT_GROUP : 2 * (g + 1) * ATT_GROUP]:
             c.wait()
         own = attend_blocks(range(g * ATT_GROUP, (g + 1) * ATT_GROUP), kv_ref, q_ref, gate)
-        if g == 0:
-            for c in late:
-                c.wait()
-        conv_copies[g].wait()
         memory = matmul(own, w_own_ref[...]) + matmul(peer_ref[span(g), :], w_peer_ref[...])
         out_ref[span(g), :] = (conv_ref[span(g), :] + memory).astype(BF16)
         out_copies[g].start()
@@ -395,36 +408,17 @@
 
 def finish(half, owners, received, queries, gate, peer, w_own, w_peer, conv_sum):
     n = conv_sum.shape[0]
-    count = owners.shape[0] // 2
-    groups = n // (ATT_GROUP * BLOCK)
     return pl.pallas_call(
         finish_kernel,
-        out_shape=jax.ShapeDtypeStruct((n, D), BF16),
-        grid_spec=pltpu.PrefetchScalarGridSpec(
-            num_scalar_prefetch=2,
-            grid=(1,),
-            in_specs=[HBM] * 7,
-            out_specs=HBM,
-            scratch_shapes=[
-                pltpu.VMEM((count, PLEN, 2 * MEM_DEV), BF16),
-                pltpu.VMEM((n, MEM_DEV), BF16),
-                pltpu.VMEM((MEM_DEV // LANES, LANES), BF16),
-                pltpu.VMEM((n, MEM_DEV), BF16),
-                pltpu.VMEM((MEM_DEV, D), BF16),
-                pltpu.VMEM((MEM_DEV, D), BF16),
-                pltpu.VMEM((n, D), F32),
-                pltpu.VMEM((n, D), BF16),
-                pltpu.SemaphoreType.DMA((count,)),
-                pltpu.SemaphoreType.DMA(()),
-                pltpu.SemaphoreType.DMA(()),
-                pltpu.SemaphoreType.DMA((3,)),
-                pltpu.SemaphoreType.DMA((groups,)),
-                pltpu.SemaphoreType.DMA((groups,)),
-            ],
-        ),
+        out_shape=pltpu.HBM((n, D), BF16),
+        in_specs=[SCALARS, SCALARS, HBM, HBM] + [ONCHIP] * 5,
+        out_specs=HBM,
+        scratch_shapes=read_scratch(owners.shape[0] // 2, n)
+        + [pltpu.VMEM((n, D), BF16), pltpu.SemaphoreType.DMA((n // (ATT_GROUP * BLOCK),))],
+        compiler_params=grant(16),
         cost_estimate=pl.CostEstimate(flops=5 * n * D * MEM_DEV, transcendentals=0, bytes_accessed=8 << 20),
         name="finish",
-    )(half, owners, received, queries, gate, peer, w_own, w_peer, conv_sum)
+    )(half, owners, *offchip(received, queries), *onchip(gate, peer, w_own, w_peer, conv_sum))
 
 
 def body(

time: 107 us -> 100 us (0.935)
  Pallas kernels: 63.4 us -> 58.3 us
  local copies, waits for them, and re-layouts: 4.36 us -> 2.67 us
    pallas_call x4, Pallas kernels: 25.2 us -> 20.1 us  [the longest x1 7.45 us: project_store(): pl.pallas_call(kv_kernel, out_shape=pltpu.VMEM((n, 2 * MEM_DEV), BF16), i...]
    unnamed x6 -> x10, local copies, waits for them, and re-layouts: 2.95 us -> 1.75 us
  transfers between devices with their start and end apart: 8 -> 8, of which waited for: 3 -> 4; matrix products, arithmetic and copies ran while one was open for 2% -> 2% of each run, Pallas kernels for 53% -> 53%
where the time goes in v2:
time: 100 us; the launch traced here: 99.7 us
  Pallas kernels  58.3 us (58%)
  starting transfers between devices  27.3 us (27%)
  waiting for transfers between devices  10.4 us (10%)
  local copies, waits for them, and re-layouts  2.67 us (3%)
    pallas_call x1, Pallas kernels, token_branch(): pl.pallas_call(token_kernel, out_shape=(jax.ShapeDtypeStruct((n, C_DEV),...  24.9 us
    all_to_all x1, starting transfers between devices, body(): asked = lax.all_to_all(wanted, 'st', 0, 0, tiled=True)  11.2 us
    all_to_all x1, starting transfers between devices, body(): received = lax.all_to_all(sent, 'st', 0, 0, tiled=True)  9.35 us
    pallas_call x1, Pallas kernels, conv_product(): pl.pallas_call(pair_kernel, out_shape=jax.ShapeDtypeStruct((n, D), F32),...  8.03 us
    pallas_call x1, Pallas kernels, project_store(): pl.pallas_call(kv_kernel, out_shape=pltpu.VMEM((n, 2 * MEM_DEV), BF16), i...  7.45 us
    all_to_all x1, waiting for transfers between devices, body(): received = lax.all_to_all(sent, 'st', 0, 0, tiled=True)  6.61 us
    pallas_call x1, Pallas kernels, finish(): pl.pallas_call(finish_kernel, out_shape=pltpu.HBM((n, D), BF16), in_specs...  5.44 us
    pallas_call x2, Pallas kernels, channel_swish(): pl.pallas_call(lambda half_ref, *refs: swish_kernel(*refs), out_shape=jax...  5.33 us
  transfers between devices with their start and end apart: 8, of which 4 were waited for; matrix products, arithmetic and copies ran while one was open for 2% of the time, Pallas kernels for 53%

profile of v2, /device:TPU:1, one launch (start us, length us, event | category | flops | bytes accessed | tf_op | source)
XLA Modules:
  0.0 99.7 jit_solution(14959928357734148002)
XLA Ops:
  0.0 1.4 %collective-permute-start = (bf16[1024,1024]{1,0:T(8,128)(2,1)}, bf16[1024,1024]{1,0:T(8,128)(2,1)}, u32[]{:S(2)}, u32[]{:S(2)}) collective-permute-start(bf16[1024,1024]{1,0:T(8,128)(2,1)} %own_ref.1), channel_id=1, source_target_pairs={{0,1},{1,0},{2,3},{3,2},{4,5},{5,4},{6,7},{7,6},{8,9},{9,8},{10,11... | collective-permute-start | bytes 6291464 | tf_op jit(solution)/shard_map/ppermute | solution.py:453
  1.4 0.0 collective-permute-start.3
  1.4 0.7 and_select_fusion
  2.1 0.1 select_reduce_fusion
  2.2 0.8 broadcast_in_dim.23
  2.9 11.2 %all-to-all-start = ((s32[64,1,128]{2,1,0:T(1,128)}), s32[64,1,128]{2,1,0:T(1,128)S(1)}, u32[]{:S(2)}, u32[]{:S(2)}) async-start(s32[64,1,128]{2,1,0:T(1,128)} %broadcast_in_dim.23), calls=%async_computation | async-start | bytes 65536 | tf_op jit(solution)/shard_map/all_to_all | solution.py:452
  14.2 7.4 %project_store.1 = bf16[1024,512]{1,0:T(8,128)(2,1)S(1)} custom-call(bf16[1024,2048]{1,0:T(8,128)(2,1)} %bitcast.16, bf16[16,128]{1,0:T(8,128)(2,1)} %bitcast.17, bf16[2048,256]{1,0:T(8,128)(2,1)} %wk_hbm.1, bf16[2048,256]{1,0:T(8,128)(2,1)} %wv_hbm.1, bf16[2,128]{1,0:T(2,128)(2,1)} %bitcast.19), custom_call_target="tpu_custom_call" | custom-call | flops 2147483648 | bytes 8388608 | tf_op jit(solution)/shard_map/project_store/pallas_call | solution.py:128
  21.6 0.9 all-to-all-done
  22.5 3.6 %fill_slots.1 = bf16[64,64,512]{2,1,0:T(8,128)(2,1)} custom-call(s32[64,128]{1,0:T(8,128)S(1)} %bitcast.11, bf16[16,64,512]{2,1,0:T(8,128)(2,1)S(1)} %bitcast.10), custom_call_target="tpu_custom_call" | custom-call | tf_op jit(solution)/shard_map/fill_slots/pallas_call | solution.py:164
  26.2 9.4 %all-to-all-start.1 = ((bf16[64,64,512]{2,1,0:T(8,128)(2,1)}), bf16[64,64,512]{2,1,0:T(8,128)(2,1)}, u32[]{:S(2)}, u32[]{:S(2)}) async-start(bf16[64,64,512]{2,1,0:T(8,128)(2,1)} %fill_slots.1), calls=%async_computation.1 | async-start | bytes 8388608 | tf_op jit(solution)/shard_map/all_to_all | solution.py:465
  35.5 0.0 collective-permute-done.peer_ref
  35.5 24.9 %token_branch.1 = (f32[1024,768]{1,0:T(8,128)}, f32[1024,2]{1,0:T(8,128)}, bf16[1024,256]{1,0:T(8,128)(2,1)}) custom-call(s32[1]{0:T(128)} %bitcast.tp_ref.half_ref, bf16[1024,1024]{1,0:T(8,128)(2,1)} %own_ref.1, bf16[1024,1024]{1,0:T(8,128)(2,1)} %collective-permute-done.peer_ref, bf16[2,8,128]{2,1,0:T(8,128)(2,1)} %bitcast.18, bf16[2048,768]{1,0:T(8,128)(2,1)} %wv_ref.1, ...), custom_call_target="tpu_custom_call" | custom-call | flops 32212254720 | bytes 16777216 | tf_op jit(solution)/shard_map/token_branch/pallas_call | solution.py:238
  60.4 0.0 copy-start.1
  60.4 1.4 %collective-permute-start.1 = (f32[1024,2]{1,0:T(8,128)}, f32[1024,2]{1,0:T(8,128)S(1)}, u32[]{:S(2)}, u32[]{:S(2)}) collective-permute-start(f32[1024,2]{1,0:T(8,128)} %get-tuple-element.11.refs_1_), channel_id=1, source_target_pairs={{0,1},{1,0},{2,3},{3,2},{4,5},{5,4},{6,7},{7,6},{8,9},{9,8},{10,11... | collective-permute-start | bytes 24584 | tf_op jit(solution)/shard_map/ppermute | solution.py:478
  61.8 1.7 %collective-permute-done.1.refs_2_ = f32[1024,2]{1,0:T(8,128)S(1)} collective-permute-done((f32[1024,2]{1,0:T(8,128)}, f32[1024,2]{1,0:T(8,128)S(1)}, u32[]{:S(2)}, u32[]{:S(2)}) %collective-permute-start.1) | collective-permute-done | bytes 8224 | tf_op jit(solution)/shard_map/ppermute | solution.py:478
  63.6 0.0 copy-start.3
  63.6 0.8 copy-done.3
  64.4 2.7 %channel_swish.3 = bf16[512,768]{1,0:T(8,128)(2,1)} custom-call(s32[1]{0:T(128)S(6)} %sub.11.half_ref, f32[1024,768]{1,0:T(8,128)} %get-tuple-element.10.refs_0_, f32[1024,2]{1,0:T(8,128)} %get-tuple-element.11.refs_1_, f32[1024,2]{1,0:T(8,128)} %copy-done.3, bf16[6,128]{1,0:T(8,128)(2,1)} %bitcast.14), custom_call_target="tpu_custom_call" | custom-call | flops 805306368 | bytes 4194304 | tf_op jit(solution)/shard_map/channel_swish/pallas_call | solution.py:283
  67.1 0.4 collective-permute-start.2
  67.4 0.0 copy-done.1
  67.4 0.1 collective-permute-start.5
  67.6 0.1 copy.27
  67.7 0.1 reshape.40.owner_ref
  67.8 2.7 %channel_swish.2.own_ref = bf16[512,768]{1,0:T(8,128)(2,1)} custom-call(s32[1]{0:T(128)} %bitcast.tp_ref.half_ref, f32[1024,768]{1,0:T(8,128)} %get-tuple-element.10.refs_0_, f32[1024,2]{1,0:T(8,128)} %get-tuple-element.11.refs_1_, f32[1024,2]{1,0:T(8,128)} %copy-done.3, bf16[6,128]{1,0:T(8,128)(2,1)} %bitcast.15), custom_call_target="tpu_custom_call" | custom-call | flops 805306368 | bytes 4194304 | tf_op jit(solution)/shard_map/channel_swish/pallas_call | solution.py:283
  70.4 0.0 copy-start.2
  70.4 0.0 collective-permute-done.2.peer_ref
  70.4 0.0 copy-start.4
  70.4 0.0 collective-permute-done.3.w_peer_ref
  70.4 0.9 copy-done.4
  71.3 8.0 %conv_product.1.conv_ref = f32[512,2048]{1,0:T(8,128)} custom-call(bf16[512,768]{1,0:T(8,128)(2,1)} %channel_swish.2.own_ref, bf16[512,768]{1,0:T(8,128)(2,1)} %copy-done.4, bf16[768,2048]{1,0:T(8,128)(2,1)} %w_own_ref.2, bf16[768,2048]{1,0:T(8,128)(2,1)} %collective-permute-done.3.w_peer_ref), custom_call_target="tpu_custom_call" | custom-call | flops 3221225472 | bytes 12582912 | tf_op jit(solution)/shard_map/conv_product/pallas_call | solution.py:304
  79.4 6.6 %all-to-all-done.1.recv_hbm = bf16[64,64,512]{2,1,0:T(8,128)(2,1)} async-done(((bf16[64,64,512]{2,1,0:T(8,128)(2,1)}), bf16[64,64,512]{2,1,0:T(8,128)(2,1)}, u32[]{:S(2)}, u32[]{:S(2)}) %all-to-all-start.1) | async-done | bytes 4194336 | tf_op jit(solution)/shard_map/all_to_all | solution.py:465
  86.0 0.0 copy-start
  86.0 0.0 copy-done.2
  86.0 3.6 %attend.1 = bf16[512,256]{1,0:T(8,128)(2,1)S(1)} custom-call(s32[1]{0:T(128)S(6)} %sub.11.half_ref, s32[32]{0:T(128)S(1)} %reshape.40.owner_ref, bf16[64,64,512]{2,1,0:T(8,128)(2,1)} %all-to-all-done.1.recv_hbm, bf16[1024,256]{1,0:T(8,128)(2,1)} %get-tuple-element.13.q_hbm, bf16[2,128]{1,0:T(2,128)(2,1)S(1)} %bitcast.12), custom_call_target="tpu_custom_call" | custom-call | flops 268435456 | bytes 2097152 | tf_op jit(solution)/shard_map/attend/pallas_call | solution.py:373
  89.6 3.4 %collective-permute-start.4 = (bf16[512,256]{1,0:T(8,128)(2,1)S(1)}, bf16[512,256]{1,0:T(8,128)(2,1)S(1)}, u32[]{:S(2)}, u32[]{:S(2)}) collective-permute-start(bf16[512,256]{1,0:T(8,128)(2,1)S(1)} %attend.1), channel_id=1, source_target_pairs={{0,1},{1,0},{2,3},{3,2},{4,5},{5,4},{6,7},{7,6},{8,9},{9,8},{10,11... | collective-permute-start | bytes 786440 | tf_op jit(solution)/shard_map/ppermute | solution.py:488
  93.0 0.0 collective-permute-done.5.w_peer_ref
  93.0 1.2 %collective-permute-done.4.peer_ref = bf16[512,256]{1,0:T(8,128)(2,1)S(1)} collective-permute-done((bf16[512,256]{1,0:T(8,128)(2,1)S(1)}, bf16[512,256]{1,0:T(8,128)(2,1)S(1)}, u32[]{:S(2)}, u32[]{:S(2)}) %collective-permute-start.4) | collective-permute-done | bytes 262176 | tf_op jit(solution)/shard_map/ppermute | solution.py:488
  94.1 0.0 copy-done
  94.1 5.4 %finish.1 = bf16[512,2048]{1,0:T(8,128)(2,1)} custom-call(s32[1]{0:T(128)} %bitcast.tp_ref.half_ref, s32[32]{0:T(128)S(1)} %reshape.40.owner_ref, bf16[64,64,512]{2,1,0:T(8,128)(2,1)} %all-to-all-done.1.recv_hbm, bf16[1024,256]{1,0:T(8,128)(2,1)} %get-tuple-element.13.q_hbm, bf16[2,128]{1,0:T(2,128)(2,1)S(1)} %bitcast.13, ...), custom_call_target="tpu_custom_call" | custom-call | flops 1342177280 | bytes 8388608 | tf_op jit(solution)/shard_map/finish/pallas_call | solution.py:411
Async XLA Ops:
  0.0 35.5 %collective-permute-start = (bf16[1024,1024]{1,0:T(8,128)(2,1)}, bf16[1024,1024]{1,0:T(8,128)(2,1)}, u32[]{:S(2)}, u32[]{:S(2)}) collective-permute-start(bf16[1024,1024]{1,0:T(8,128)(2,1)} %own_ref.1), channel_id=1, source_target_pairs={{0,1},{1,0},{2,3},{3,2},{4,5},{5,4},{6,7},{7,6},{8,9},{9,8},{10,11... | collective-permute-start | bytes 6291464 | tf_op jit(solution)/shard_map/ppermute | solution.py:453
  1.4 69.1 %collective-permute-start.3 = (bf16[768,2048]{1,0:T(8,128)(2,1)}, bf16[768,2048]{1,0:T(8,128)(2,1)}, u32[]{:S(2)}, u32[]{:S(2)}) collective-permute-start(bf16[768,2048]{1,0:T(8,128)(2,1)} %w_own_ref.2), channel_id=1, source_target_pairs={{0,1},{1,0},{2,3},{3,2},{4,5},{5,4},{6,7},{7,6},{8,9},{9,8},{10,11... | collective-permute-start | bytes 9437192 | tf_op jit(solution)/shard_map/ppermute | solution.py:454
  2.9 19.6 %all-to-all-start = ((s32[64,1,128]{2,1,0:T(1,128)}), s32[64,1,128]{2,1,0:T(1,128)S(1)}, u32[]{:S(2)}, u32[]{:S(2)}) async-start(s32[64,1,128]{2,1,0:T(1,128)} %broadcast_in_dim.23), calls=%async_computation | async-start | bytes 65536 | tf_op jit(solution)/shard_map/all_to_all | solution.py:452
  26.2 59.8 %all-to-all-start.1 = ((bf16[64,64,512]{2,1,0:T(8,128)(2,1)}), bf16[64,64,512]{2,1,0:T(8,128)(2,1)}, u32[]{:S(2)}, u32[]{:S(2)}) async-start(bf16[64,64,512]{2,1,0:T(8,128)(2,1)} %fill_slots.1), calls=%async_computation.1 | async-start | bytes 8388608 | tf_op jit(solution)/shard_map/all_to_all | solution.py:465
  60.4 7.1 %copy-start.1 = (bf16[256,2048]{1,0:T(8,128)(2,1)S(1)}, bf16[256,2048]{1,0:T(8,128)(2,1)}, u32[]{:S(2)}) copy-start(bf16[256,2048]{1,0:T(8,128)(2,1)} %w_own_ref.3) | copy-start | bytes 3145732
  60.4 3.2 %collective-permute-start.1 = (f32[1024,2]{1,0:T(8,128)}, f32[1024,2]{1,0:T(8,128)S(1)}, u32[]{:S(2)}, u32[]{:S(2)}) collective-permute-start(f32[1024,2]{1,0:T(8,128)} %get-tuple-element.11.refs_1_), channel_id=1, source_target_pairs={{0,1},{1,0},{2,3},{3,2},{4,5},{5,4},{6,7},{7,6},{8,9},{9,8},{10,11... | collective-permute-start | bytes 24584 | tf_op jit(solution)/shard_map/ppermute | solution.py:478
  63.6 0.8 copy-start.3
  67.1 3.4 %collective-permute-start.2 = (bf16[512,768]{1,0:T(8,128)(2,1)}, bf16[512,768]{1,0:T(8,128)(2,1)S(1)}, u32[]{:S(2)}, u32[]{:S(2)}) collective-permute-start(bf16[512,768]{1,0:T(8,128)(2,1)} %channel_swish.3), channel_id=1, source_target_pairs={{0,1},{1,0},{2,3},{3,2},{4,5},{5,4},{6,7},{7,6},{8,9},{9,8},{10,11... | collective-permute-start | bytes 2359304 | tf_op jit(solution)/shard_map/ppermute | solution.py:480
  67.4 25.5 %collective-permute-start.5 = (bf16[256,2048]{1,0:T(8,128)(2,1)S(1)}, bf16[256,2048]{1,0:T(8,128)(2,1)S(1)}, u32[]{:S(2)}, u32[]{:S(2)}) collective-permute-start(bf16[256,2048]{1,0:T(8,128)(2,1)S(1)} %copy-done.1), channel_id=1, source_target_pairs={{0,1},{1,0},{2,3},{3,2},{4,5},{5,4},{6,7},{7,6},{8,9},{9,8},{10,11... | collective-permute-start | bytes 3145736 | tf_op jit(solution)/shard_map/ppermute | solution.py:455
  70.4 15.6 %copy-start.2 = (bf16[256]{0:T(256)(128)(2,1)S(1)}, bf16[256]{0:T(256)(128)(2,1)}, u32[]{:S(2)}) copy-start(bf16[256]{0:T(256)(128)(2,1)} %param.31) | copy-start | bytes 1540
  70.4 0.9 copy-start.4
  86.0 8.1 %copy-start = (f32[512,2048]{1,0:T(8,128)S(1)}, f32[512,2048]{1,0:T(8,128)}, u32[]{:S(2)}) copy-start(f32[512,2048]{1,0:T(8,128)} %conv_product.1.conv_ref) | copy-start | bytes 12582916
  89.6 4.5 %collective-permute-start.4 = (bf16[512,256]{1,0:T(8,128)(2,1)S(1)}, bf16[512,256]{1,0:T(8,128)(2,1)S(1)}, u32[]{:S(2)}, u32[]{:S(2)}) collective-permute-start(bf16[512,256]{1,0:T(8,128)(2,1)S(1)} %attend.1), channel_id=1, source_target_pairs={{0,1},{1,0},{2,3},{3,2},{4,5},{5,4},{6,7},{7,6},{8,9},{9,8},{10,11... | collective-permute-start | bytes 786440 | tf_op jit(solution)/shard_map/ppermute | solution.py:488

commit v3 on v2

--- a/solution.py
+++ b/solution.py
@@ -16,14 +16,14 @@
 BLOCK = 64
 PLEN = 64
 PASS_DEV = 16
-TOK_DEV = 1024
+OWNER_SHIFT = 4
 NORM_EPS = 1e-06
 LAYER_EPS = 1e-05
 
 KV_TILE = 256
 TOK_TILE = 256
 OUT_TILE = 256
-ATT_TILE = 128
+ATT_TILE = 256
 ATT_GROUP = 4
 LANES = 128
 CONV_ROWS = 128
@@ -332,16 +332,6 @@
     return jnp.concatenate(rows, axis=0)
 
 
-def read_copies(half_ref, owner_ref, recv_hbm, q_hbm, kv_ref, q_ref, sem, q_sem):
-    count = kv_ref.shape[0]
-    n = q_ref.shape[0]
-    first = half_ref[0] * count
-    q_copy = pltpu.make_async_copy(q_hbm.at[pl.ds(pl.multiple_of(half_ref[0] * n, n), n), :], q_ref, q_sem)
-    return q_copy, [
-        pltpu.make_async_copy(recv_hbm.at[owner_ref[first + i]], kv_ref.at[i], sem.at[i]) for i in range(count)
-    ]
-
-
 SCALARS = pl.BlockSpec(memory_space=pltpu.SMEM)
 
 
@@ -354,71 +344,102 @@
     ]
 
 
-def attend_kernel(half_ref, owner_ref, recv_hbm, q_hbm, gate_ref, out_ref, kv_ref, q_ref, sem, q_sem):
-    q_copy, copies = read_copies(half_ref, owner_ref, recv_hbm, q_hbm, kv_ref, q_ref, sem, q_sem)
-    for c in [q_copy, *copies]:
+def attend_all(out_ref, kv_ref, q_ref, gate, arrived):
+    size = ATT_GROUP * BLOCK
+    for g in range(out_ref.shape[0] // size):
+        arrived(g)
+        blocks = range(g * ATT_GROUP, (g + 1) * ATT_GROUP)
+        out_ref[pl.ds(g * size, size), :] = attend_blocks(blocks, kv_ref, q_ref, gate)
+
+
+def attend_kernel(
+    half_ref, owner_ref, recv_hbm, q_hbm, gate_ref, out_ref, next_kv_ref, next_q_ref, kv_ref, q_ref, sem, q_sem, next_sem, next_q_sem
+):
+    count = kv_ref.shape[0]
+    n = q_ref.shape[0]
+    first, second = half_ref[0], 1 - half_ref[0]
+    q_copy = pltpu.make_async_copy(q_hbm.at[pl.ds(pl.multiple_of(first * n, n), n), :], q_ref, q_sem)
+    copies = [
+        pltpu.make_async_copy(recv_hbm.at[owner_ref[first * count + i]], kv_ref.at[i], sem.at[i]) for i in range(count)
+    ]
+    later = [pltpu.make_async_copy(q_hbm.at[pl.ds(pl.multiple_of(second * n, n), n), :], next_q_ref, next_q_sem)] + [
+        pltpu.make_async_copy(recv_hbm.at[owner_ref[second * count + i]], next_kv_ref.at[i], next_sem.at[i])
+        for i in range(count)
+    ]
+    for c in [q_copy, *copies, *later]:
         c.start()
     gate = jnp.tanh(wide_row(gate_ref))
-    size = ATT_GROUP * BLOCK
     q_copy.wait()
-    for g in range(out_ref.shape[0] // size):
+
+    def arrived(g):
         for c in copies[2 * g * ATT_GROUP : 2 * (g + 1) * ATT_GROUP]:
             c.wait()
-        blocks = range(g * ATT_GROUP, (g + 1) * ATT_GROUP)
-        out_ref[pl.ds(g * size, size), :] = attend_blocks(blocks, kv_ref, q_ref, gate)
-
-
-def attend(half, owners, received, queries, gate):
+
+    attend_all(out_ref, kv_ref, q_ref, gate, arrived)
+    for c in later:
+        c.wait()
+
+
+def attend_first(half, owners, received, queries, gate):
     n = queries.shape[0] // 2
+    count = owners.shape[0] // 2
     return pl.pallas_call(
         attend_kernel,
-        out_shape=pltpu.VMEM((n, MEM_DEV), BF16),
+        out_shape=(
+            pltpu.VMEM((n, MEM_DEV), BF16),
+            pltpu.VMEM((count, PLEN, 2 * MEM_DEV), BF16),
+            pltpu.VMEM((n, MEM_DEV), BF16),
+        ),
         in_specs=[SCALARS, SCALARS, HBM, HBM, ONCHIP],
-        out_specs=ONCHIP,
-        scratch_shapes=read_scratch(owners.shape[0] // 2, n),
+        out_specs=(ONCHIP, ONCHIP, ONCHIP),
+        scratch_shapes=read_scratch(count, n) + [pltpu.SemaphoreType.DMA((count,)), pltpu.SemaphoreType.DMA(())],
         compiler_params=grant(8),
         cost_estimate=pl.CostEstimate(flops=n * D * 256, transcendentals=0, bytes_accessed=2 << 20),
-        name="attend",
+        name="attend_first",
     )(half, owners, *offchip(received, queries), *onchip(gate))
 
 
-def finish_kernel(
-    half_ref, owner_ref, recv_hbm, q_hbm, gate_ref, peer_ref, w_own_ref, w_peer_ref, conv_ref, out_hbm,
-    kv_ref, q_ref, sem, q_sem, out_ref, out_sem
-):
-    q_copy, copies = read_copies(half_ref, owner_ref, recv_hbm, q_hbm, kv_ref, q_ref, sem, q_sem)
-    for c in [q_copy, *copies]:
-        c.start()
-    gate = jnp.tanh(wide_row(gate_ref))
-    size = ATT_GROUP * BLOCK
-    groups = out_ref.shape[0] // size
-    span = lambda g: pl.ds(g * size, size)
+def attend_rest_kernel(kv_ref, q_ref, gate_ref, out_ref):
+    attend_all(out_ref, kv_ref, q_ref, jnp.tanh(wide_row(gate_ref)), lambda g: None)
+
+
+def attend_rest(kv, queries, gate):
+    n = queries.shape[0]
+    return pl.pallas_call(
+        attend_rest_kernel,
+        out_shape=pltpu.VMEM((n, MEM_DEV), BF16),
+        in_specs=[ONCHIP] * 3,
+        out_specs=ONCHIP,
+        compiler_params=grant(6),
+        cost_estimate=pl.CostEstimate(flops=n * D * 256, transcendentals=0, bytes_accessed=2 << 20),
+        name="attend_rest",
+    )(*onchip(kv, queries, gate))
+
+
+def finish_kernel(own_ref, peer_ref, w_own_ref, w_peer_ref, conv_ref, out_hbm, out_ref, out_sem):
+    groups = out_ref.shape[0] // ATT_TILE
+    span = lambda g: pl.ds(g * ATT_TILE, ATT_TILE)
     out_copies = [pltpu.make_async_copy(out_ref.at[span(g)], out_hbm.at[span(g)], out_sem.at[g]) for g in range(groups)]
-    q_copy.wait()
     for g in range(groups):
-        for c in copies[2 * g * ATT_GROUP : 2 * (g + 1) * ATT_GROUP]:
-            c.wait()
-        own = attend_blocks(range(g * ATT_GROUP, (g + 1) * ATT_GROUP), kv_ref, q_ref, gate)
-        memory = matmul(own, w_own_ref[...]) + matmul(peer_ref[span(g), :], w_peer_ref[...])
+        memory = matmul(own_ref[span(g), :], w_own_ref[...]) + matmul(peer_ref[span(g), :], w_peer_ref[...])
         out_ref[span(g), :] = (conv_ref[span(g), :] + memory).astype(BF16)
         out_copies[g].start()
     for c in out_copies:
         c.wait()
 
 
-def finish(half, owners, received, queries, gate, peer, w_own, w_peer, conv_sum):
+def finish(own, peer, w_own, w_peer, conv_sum):
     n = conv_sum.shape[0]
     return pl.pallas_call(
         finish_kernel,
         out_shape=pltpu.HBM((n, D), BF16),
-        in_specs=[SCALARS, SCALARS, HBM, HBM] + [ONCHIP] * 5,
+        in_specs=[ONCHIP] * 5,
         out_specs=HBM,
-        scratch_shapes=read_scratch(owners.shape[0] // 2, n)
-        + [pltpu.VMEM((n, D), BF16), pltpu.SemaphoreType.DMA((n // (ATT_GROUP * BLOCK),))],
-        compiler_params=grant(16),
-        cost_estimate=pl.CostEstimate(flops=5 * n * D * MEM_DEV, transcendentals=0, bytes_accessed=8 << 20),
+        scratch_shapes=[pltpu.VMEM((n, D), BF16), pltpu.SemaphoreType.DMA((n // ATT_TILE,))],
+        compiler_params=grant(12),
+        cost_estimate=pl.CostEstimate(flops=4 * n * D * MEM_DEV, transcendentals=0, bytes_accessed=8 << 20),
         name="finish",
-    )(half, owners, *offchip(received, queries), *onchip(gate, peer, w_own, w_peer, conv_sum))
+    )(*onchip(own, peer, w_own, w_peer, conv_sum))
 
 
 def body(
@@ -444,11 +465,9 @@
     swap = [(0, 1), (1, 0)]
     me = lax.axis_index("tp").astype(jnp.int32).reshape(1)
 
-    owner_ids = passage_ids // PASS_DEV
-    local_ids = passage_ids % PASS_DEV
-    everyone = jnp.arange(owner_count, dtype=jnp.int32)[:, None, None]
-    wanted = jnp.sum(jnp.where(owner_ids[None] == everyone, local_ids[None], 0), axis=(1, 2))
-    wanted = jnp.broadcast_to(wanted[:, None], (owner_count, LANES))
+    everyone = jnp.arange(owner_count, dtype=jnp.int32)[:, None, None, None]
+    spread = jnp.broadcast_to(passage_ids, (owner_count, LANES, *passage_ids.shape))
+    wanted = jnp.sum(jnp.where(spread >> OWNER_SHIFT == everyone, spread & (PASS_DEV - 1), 0), axis=(2, 3))
     asked = lax.all_to_all(wanted, "st", 0, 0, tiled=True)
     peer_tokens = lax.ppermute(tokens, "tp", swap)
     peer_conv_weight = lax.ppermute(conv_out_weight, "tp", swap)
@@ -482,13 +501,12 @@
     conv_sum = conv_product(conv_mine, conv_peer, conv_out_weight, peer_conv_weight)
 
     received, conv_sum = lax.optimization_barrier((received, conv_sum))
-    owners = owner_ids.reshape(-1)
+    owners = lax.optimization_barrier((passage_ids, filtered))[0].reshape(-1) >> OWNER_SHIFT
     gate = memory_gate.reshape(-1, LANES)
-    memory_theirs = attend(1 - me, owners, received, queries, gate)
+    memory_theirs, next_kv, next_queries = attend_first(1 - me, owners, received, queries, gate)
     memory_peer = lax.ppermute(memory_theirs, "tp", swap)
-    return finish(
-        me, owners, received, queries, gate, memory_peer, memory_out_weight, peer_memory_weight, conv_sum
-    )
+    memory_mine = attend_rest(next_kv, next_queries, gate)
+    return finish(memory_mine, memory_peer, memory_out_weight, peer_memory_weight, conv_sum)
 
 
 def solution(mesh):

time: 100 us -> 99.4 us (level)
  starting transfers between devices: 27.3 us -> 25.4 us
  Pallas kernels: 58.3 us -> 56.8 us
  waiting for transfers between devices: 10.4 us -> 11.9 us
    pallas_call x1, Pallas kernels: 5.44 us -> 2.25 us  [finish(): pl.pallas_call(finish_kernel, out_shape=pltpu.HBM((n, D), BF16), in_specs...]
    all_to_all x1, waiting for transfers between devices: 6.61 us -> 9.53 us  [body(): received = lax.all_to_all(sent, 'st', 0, 0, tiled=True)]
    ppermute x1, starting transfers between devices: 3.36 us -> 1.54 us  [body(): memory_peer = lax.ppermute(memory_theirs, 'tp', swap)]
    pallas_call x1 -> x2, Pallas kernels: 3.61 us -> 5.21 us  [the longest x1 4.08 us: attend_first(): pl.pallas_call(attend_kernel, out_shape=(pltpu.VMEM((n, MEM_DEV), BF16),...]
    unnamed x10 -> x14, local copies, waits for them, and re-layouts: 1.75 us -> 3 us
    ppermute x1, waiting for transfers between devices: 1.16 us -> 0.02 us  [body(): memory_peer = lax.ppermute(memory_theirs, 'tp', swap)]
    ppermute x1, starting transfers between devices: 1.42 us -> 0.38 us  [body(): peer_stats = lax.ppermute(own_stats, 'tp', swap)]
  transfers between devices with their start and end apart: 8 -> 8, of which waited for: 4 -> 3; matrix products, arithmetic and copies ran while one was open for 2% -> 2% of each run, Pallas kernels for 53% -> 55%
where the time goes in v3:
time: 99.4 us; the launch traced here: 99.1 us
  Pallas kernels  56.8 us (57%)
  starting transfers between devices  25.4 us (26%)
  waiting for transfers between devices  11.9 us (12%)
  local copies, waits for them, and re-layouts  3.18 us (3%)
  other arithmetic  1.53 us (2%)
    pallas_call x1, Pallas kernels, token_branch(): pl.pallas_call(token_kernel, out_shape=(jax.ShapeDtypeStruct((n, C_DEV),...  24.9 us
    all_to_all x1, starting transfers between devices, body(): asked = lax.all_to_all(wanted, 'st', 0, 0, tiled=True)  11.2 us
    all_to_all x1, starting transfers between devices, body(): received = lax.all_to_all(sent, 'st', 0, 0, tiled=True)  9.99 us
    all_to_all x1, waiting for transfers between devices, body(): received = lax.all_to_all(sent, 'st', 0, 0, tiled=True)  9.53 us
    pallas_call x1, Pallas kernels, conv_product(): pl.pallas_call(pair_kernel, out_shape=jax.ShapeDtypeStruct((n, D), F32),...  8.03 us
    pallas_call x1, Pallas kernels, project_store(): pl.pallas_call(kv_kernel, out_shape=pltpu.VMEM((n, 2 * MEM_DEV), BF16), i...  7.44 us
    pallas_call x2, Pallas kernels, channel_swish(): pl.pallas_call(lambda half_ref, *refs: swish_kernel(*refs), out_shape=jax...  5.34 us
    pallas_call x1, Pallas kernels, attend_first(): pl.pallas_call(attend_kernel, out_shape=(pltpu.VMEM((n, MEM_DEV), BF16),...  4.08 us
  transfers between devices with their start and end apart: 8, of which 3 were waited for; matrix products, arithmetic and copies ran while one was open for 2% of the time, Pallas kernels for 55%

profile of v3, /device:TPU:1, one launch (start us, length us, event | category | flops | bytes accessed | tf_op | source)
XLA Modules:
  0.0 99.1 jit_solution(17479800522173979379)
XLA Ops:
  0.0 1.4 %collective-permute-start = (bf16[1024,1024]{1,0:T(8,128)(2,1)}, bf16[1024,1024]{1,0:T(8,128)(2,1)S(1)}, u32[]{:S(2)}, u32[]{:S(2)}) collective-permute-start(bf16[1024,1024]{1,0:T(8,128)(2,1)} %own_ref.1), channel_id=1, source_target_pairs={{0,1},{1,0},{2,3},{3,2},{4,5},{5,4},{6,7},{7,6},{8,9},{9,8},{10,11... | collective-permute-start | bytes 6291464 | tf_op jit(solution)/shard_map/ppermute | solution.py:472
  1.4 0.7 broadcast_shift-right-arithmetic_fusion
  2.1 0.8 select_reduce_fusion
  2.9 11.2 %all-to-all-start = ((s32[64,1,128]{2,1,0:T(1,128)}), s32[64,1,128]{2,1,0:T(1,128)S(1)}, u32[]{:S(2)}, u32[]{:S(2)}) async-start(s32[64,1,128]{2,1,0:T(1,128)} %bitcast.4), calls=%async_computation | async-start | bytes 65536 | tf_op jit(solution)/shard_map/all_to_all | solution.py:471
  14.2 0.4 collective-permute-start.3
  14.5 7.4 %project_store.1 = bf16[1024,512]{1,0:T(8,128)(2,1)S(1)} custom-call(bf16[1024,2048]{1,0:T(8,128)(2,1)} %bitcast.19, bf16[16,128]{1,0:T(8,128)(2,1)} %bitcast.20, bf16[2048,256]{1,0:T(8,128)(2,1)} %wk_hbm.1, bf16[2048,256]{1,0:T(8,128)(2,1)} %wv_hbm.1, bf16[2,128]{1,0:T(2,128)(2,1)} %bitcast.22), custom_call_target="tpu_custom_call" | custom-call | flops 2147483648 | bytes 8388608 | tf_op jit(solution)/shard_map/project_store/pallas_call | solution.py:128
  22.0 0.5 all-to-all-done
  22.5 3.6 %fill_slots.1 = bf16[64,64,512]{2,1,0:T(8,128)(2,1)} custom-call(s32[64,128]{1,0:T(8,128)S(1)} %bitcast.14, bf16[16,64,512]{2,1,0:T(8,128)(2,1)S(1)} %bitcast.13), custom_call_target="tpu_custom_call" | custom-call | tf_op jit(solution)/shard_map/fill_slots/pallas_call | solution.py:164
  26.2 10.0 %all-to-all-start.1 = ((bf16[64,64,512]{2,1,0:T(8,128)(2,1)}), bf16[64,64,512]{2,1,0:T(8,128)(2,1)}, u32[]{:S(2)}, u32[]{:S(2)}) async-start(bf16[64,64,512]{2,1,0:T(8,128)(2,1)} %fill_slots.1), calls=%async_computation.1 | async-start | bytes 8388608 | tf_op jit(solution)/shard_map/all_to_all | solution.py:484
  36.2 0.0 collective-permute-done.peer_ref
  36.2 0.0 copy-start.6
  36.2 1.3 %copy-done.6 = bf16[1024,1024]{1,0:T(8,128)(2,1)} copy-done((bf16[1024,1024]{1,0:T(8,128)(2,1)}, bf16[1024,1024]{1,0:T(8,128)(2,1)S(1)}, u32[]{:S(2)}) %copy-start.6) | copy-done | bytes 2097176
  37.5 24.9 %token_branch.1 = (f32[1024,768]{1,0:T(8,128)}, f32[1024,2]{1,0:T(8,128)}, bf16[1024,256]{1,0:T(8,128)(2,1)}) custom-call(s32[1]{0:T(128)} %bitcast.tp_ref.half_ref, bf16[1024,1024]{1,0:T(8,128)(2,1)} %own_ref.1, bf16[1024,1024]{1,0:T(8,128)(2,1)} %copy-done.6, bf16[2,8,128]{2,1,0:T(8,128)(2,1)} %bitcast.21, bf16[2048,768]{1,0:T(8,128)(2,1)} %wv_ref.1, ...), custom_call_target="tpu_custom_call" | custom-call | flops 32212254720 | bytes 16777216 | tf_op jit(solution)/shard_map/token_branch/pallas_call | solution.py:238
  62.3 0.0 copy-start.1
  62.3 0.0 copy-start.5
  62.4 0.4 collective-permute-start.1
  62.7 1.8 %collective-permute-done.1.refs_2_ = f32[1024,2]{1,0:T(8,128)S(1)} collective-permute-done((f32[1024,2]{1,0:T(8,128)}, f32[1024,2]{1,0:T(8,128)S(1)}, u32[]{:S(2)}, u32[]{:S(2)}) %collective-permute-start.1) | collective-permute-done | bytes 8224 | tf_op jit(solution)/shard_map/ppermute | solution.py:497
  64.6 0.0 copy-start.3
  64.6 0.8 copy-done.3
  65.4 2.7 %channel_swish.3 = bf16[512,768]{1,0:T(8,128)(2,1)} custom-call(s32[1]{0:T(128)S(6)} %sub.4.half_ref, f32[1024,768]{1,0:T(8,128)} %get-tuple-element.14.refs_0_, f32[1024,2]{1,0:T(8,128)} %get-tuple-element.16.refs_1_, f32[1024,2]{1,0:T(8,128)} %copy-done.3, bf16[6,128]{1,0:T(8,128)(2,1)} %bitcast.17), custom_call_target="tpu_custom_call" | custom-call | flops 805306368 | bytes 4194304 | tf_op jit(solution)/shard_map/channel_swish/pallas_call | solution.py:283
  68.0 0.3 collective-permute-start.2
  68.3 0.0 copy-done.1
  68.3 0.2 collective-permute-start.5
  68.5 0.0 copy-done.5
  68.5 0.1 copy.27
  68.6 0.1 shift_right_arithmetic.15.owner_ref
  68.7 2.7 %channel_swish.2.own_ref = bf16[512,768]{1,0:T(8,128)(2,1)} custom-call(s32[1]{0:T(128)} %bitcast.tp_ref.half_ref, f32[1024,768]{1,0:T(8,128)} %get-tuple-element.14.refs_0_, f32[1024,2]{1,0:T(8,128)} %get-tuple-element.16.refs_1_, f32[1024,2]{1,0:T(8,128)} %copy-done.3, bf16[6,128]{1,0:T(8,128)(2,1)} %bitcast.18), custom_call_target="tpu_custom_call" | custom-call | flops 805306368 | bytes 4194304 | tf_op jit(solution)/shard_map/channel_swish/pallas_call | solution.py:283
  71.4 0.0 copy-start.2
  71.4 0.0 collective-permute-done.2.peer_ref
  71.4 0.0 copy-start.4
  71.4 0.0 collective-permute-done.3.w_peer_ref
  71.4 0.9 copy-done.4
  72.3 8.0 %conv_product.1.conv_ref = f32[512,2048]{1,0:T(8,128)} custom-call(bf16[512,768]{1,0:T(8,128)(2,1)} %channel_swish.2.own_ref, bf16[512,768]{1,0:T(8,128)(2,1)} %copy-done.4, bf16[768,2048]{1,0:T(8,128)(2,1)} %w_own_ref.2, bf16[768,2048]{1,0:T(8,128)(2,1)} %collective-permute-done.3.w_peer_ref), custom_call_target="tpu_custom_call" | custom-call | flops 3221225472 | bytes 12582912 | tf_op jit(solution)/shard_map/conv_product/pallas_call | solution.py:304
  80.3 9.5 %all-to-all-done.1.recv_hbm = bf16[64,64,512]{2,1,0:T(8,128)(2,1)} async-done(((bf16[64,64,512]{2,1,0:T(8,128)(2,1)}), bf16[64,64,512]{2,1,0:T(8,128)(2,1)}, u32[]{:S(2)}, u32[]{:S(2)}) %all-to-all-start.1) | async-done | bytes 4194336 | tf_op jit(solution)/shard_map/all_to_all | solution.py:484
  89.9 0.0 copy-done.2
  89.9 0.0 copy-start
  89.9 4.1 %attend_first.1 = (bf16[512,256]{1,0:T(8,128)(2,1)S(1)}, bf16[16,64,512]{2,1,0:T(8,128)(2,1)S(1)}, bf16[512,256]{1,0:T(8,128)(2,1)S(1)}) custom-call(s32[1]{0:T(128)S(6)} %sub.4.half_ref, s32[32]{0:T(128)S(1)} %shift_right_arithmetic.15.owner_ref, bf16[64,64,512]{2,1,0:T(8,128)(2,1)} %all-to-all-done.1.recv_hbm, bf16[1024,256]{1,0:T(8,128)(2,1)} %get-tuple-element.18.q_hbm, ...), custom_call_target="tpu_custom_call" | custom-call | flops 268435456 | bytes 2097152 | tf_op jit(solution)/shard_map/attend_first/pallas_call | solution.py:386
  94.0 1.5 %collective-permute-start.4 = (bf16[512,256]{1,0:T(8,128)(2,1)S(1)}, bf16[512,256]{1,0:T(8,128)(2,1)S(1)}, u32[]{:S(2)}, u32[]{:S(2)}) collective-permute-start(bf16[512,256]{1,0:T(8,128)(2,1)S(1)} %get-tuple-element.21), channel_id=1, source_target_pairs={{0,1},{1,0},{2,3},{3,2},{4,5},{5,4},{6,7},{7,6},{8,9},{9,8},{10,11... | collective-permute-start | bytes 786440 | tf_op jit(solution)/shard_map/ppermute | solution.py:507
  95.5 1.1 %attend_rest.1.own_ref = bf16[512,256]{1,0:T(8,128)(2,1)S(1)} custom-call(bf16[16,64,512]{2,1,0:T(8,128)(2,1)S(1)} %get-tuple-element.19.kv_ref, bf16[512,256]{1,0:T(8,128)(2,1)S(1)} %get-tuple-element.20.q_ref, bf16[2,128]{1,0:T(2,128)(2,1)S(1)} %bitcast.16), custom_call_target="tpu_custom_call" | custom-call | flops 268435456 | bytes 2097152 | tf_op jit(solution)/shard_map/attend_rest/pallas_call | solution.py:408
  96.6 0.0 collective-permute-done.5.w_peer_ref
  96.6 0.0 collective-permute-done.4.peer_ref
  96.7 0.0 copy-done
  96.7 2.2 %finish.1 = bf16[512,2048]{1,0:T(8,128)(2,1)} custom-call(bf16[512,256]{1,0:T(8,128)(2,1)S(1)} %attend_rest.1.own_ref, bf16[512,256]{1,0:T(8,128)(2,1)S(1)} %collective-permute-done.4.peer_ref, bf16[256,2048]{1,0:T(8,128)(2,1)S(1)} %copy-done.1, bf16[256,2048]{1,0:T(8,128)(2,1)S(1)} %collective-permute-done.5.w_peer_ref, f32[512,2048]{1,0:T(8,128)S(1)} %copy-done), custom_call_target="tpu_custom_call" | custom-call | flops 1073741824 | bytes 8388608 | tf_op jit(solution)/shard_map/finish/pallas_call | solution.py:433
  (1 shorter events, 0.0 us)
Async XLA Ops:
  0.0 36.2 %collective-permute-start = (bf16[1024,1024]{1,0:T(8,128)(2,1)}, bf16[1024,1024]{1,0:T(8,128)(2,1)S(1)}, u32[]{:S(2)}, u32[]{:S(2)}) collective-permute-start(bf16[1024,1024]{1,0:T(8,128)(2,1)} %own_ref.1), channel_id=1, source_target_pairs={{0,1},{1,0},{2,3},{3,2},{4,5},{5,4},{6,7},{7,6},{8,9},{9,8},{10,11... | collective-permute-start | bytes 6291464 | tf_op jit(solution)/shard_map/ppermute | solution.py:472
  2.9 19.6 %all-to-all-start = ((s32[64,1,128]{2,1,0:T(1,128)}), s32[64,1,128]{2,1,0:T(1,128)S(1)}, u32[]{:S(2)}, u32[]{:S(2)}) async-start(s32[64,1,128]{2,1,0:T(1,128)} %bitcast.4), calls=%async_computation | async-start | bytes 65536 | tf_op jit(solution)/shard_map/all_to_all | solution.py:471
  14.2 57.2 %collective-permute-start.3 = (bf16[768,2048]{1,0:T(8,128)(2,1)}, bf16[768,2048]{1,0:T(8,128)(2,1)}, u32[]{:S(2)}, u32[]{:S(2)}) collective-permute-start(bf16[768,2048]{1,0:T(8,128)(2,1)} %w_own_ref.2), channel_id=1, source_target_pairs={{0,1},{1,0},{2,3},{3,2},{4,5},{5,4},{6,7},{7,6},{8,9},{9,8},{10,11... | collective-permute-start | bytes 9437192 | tf_op jit(solution)/shard_map/ppermute | solution.py:473
  26.2 63.7 %all-to-all-start.1 = ((bf16[64,64,512]{2,1,0:T(8,128)(2,1)}), bf16[64,64,512]{2,1,0:T(8,128)(2,1)}, u32[]{:S(2)}, u32[]{:S(2)}) async-start(bf16[64,64,512]{2,1,0:T(8,128)(2,1)} %fill_slots.1), calls=%async_computation.1 | async-start | bytes 8388608 | tf_op jit(solution)/shard_map/all_to_all | solution.py:484
  36.2 1.3 %copy-start.6 = (bf16[1024,1024]{1,0:T(8,128)(2,1)}, bf16[1024,1024]{1,0:T(8,128)(2,1)S(1)}, u32[]{:S(2)}) copy-start(bf16[1024,1024]{1,0:T(8,128)(2,1)S(1)} %collective-permute-done.peer_ref) | copy-start | bytes 6291460
  62.3 6.0 %copy-start.1 = (bf16[256,2048]{1,0:T(8,128)(2,1)S(1)}, bf16[256,2048]{1,0:T(8,128)(2,1)}, u32[]{:S(2)}) copy-start(bf16[256,2048]{1,0:T(8,128)(2,1)} %w_own_ref.3) | copy-start | bytes 3145732
  62.3 6.2 %copy-start.5 = (s32[16,2]{0,1:T(2,128)S(1)}, s32[16,2]{0,1:T(2,128)}, u32[]{:S(2)}) copy-start(s32[16,2]{0,1:T(2,128)} %param.18) | copy-start | bytes 388
  62.4 2.2 %collective-permute-start.1 = (f32[1024,2]{1,0:T(8,128)}, f32[1024,2]{1,0:T(8,128)S(1)}, u32[]{:S(2)}, u32[]{:S(2)}) collective-permute-start(f32[1024,2]{1,0:T(8,128)} %get-tuple-element.16.refs_1_), channel_id=1, source_target_pairs={{0,1},{1,0},{2,3},{3,2},{4,5},{5,4},{6,7},{7,6},{8,9},{9,8},{10,11... | collective-permute-start | bytes 24584 | tf_op jit(solution)/shard_map/ppermute | solution.py:497
  64.6 0.8 copy-start.3
  68.0 3.4 %collective-permute-start.2 = (bf16[512,768]{1,0:T(8,128)(2,1)}, bf16[512,768]{1,0:T(8,128)(2,1)S(1)}, u32[]{:S(2)}, u32[]{:S(2)}) collective-permute-start(bf16[512,768]{1,0:T(8,128)(2,1)} %channel_swish.3), channel_id=1, source_target_pairs={{0,1},{1,0},{2,3},{3,2},{4,5},{5,4},{6,7},{7,6},{8,9},{9,8},{10,11... | collective-permute-start | bytes 2359304 | tf_op jit(solution)/shard_map/ppermute | solution.py:499
  68.3 28.3 %collective-permute-start.5 = (bf16[256,2048]{1,0:T(8,128)(2,1)S(1)}, bf16[256,2048]{1,0:T(8,128)(2,1)S(1)}, u32[]{:S(2)}, u32[]{:S(2)}) collective-permute-start(bf16[256,2048]{1,0:T(8,128)(2,1)S(1)} %copy-done.1), channel_id=1, source_target_pairs={{0,1},{1,0},{2,3},{3,2},{4,5},{5,4},{6,7},{7,6},{8,9},{9,8},{10,11... | collective-permute-start | bytes 3145736 | tf_op jit(solution)/shard_map/ppermute | solution.py:474
  71.4 18.5 %copy-start.2 = (bf16[256]{0:T(256)(128)(2,1)S(1)}, bf16[256]{0:T(256)(128)(2,1)}, u32[]{:S(2)}) copy-start(bf16[256]{0:T(256)(128)(2,1)} %param.31) | copy-start | bytes 1540
  71.4 0.9 copy-start.4
  89.9 6.8 %copy-start = (f32[512,2048]{1,0:T(8,128)S(1)}, f32[512,2048]{1,0:T(8,128)}, u32[]{:S(2)}) copy-start(f32[512,2048]{1,0:T(8,128)} %conv_product.1.conv_ref) | copy-start | bytes 12582916
  94.0 2.7 %collective-permute-start.4 = (bf16[512,256]{1,0:T(8,128)(2,1)S(1)}, bf16[512,256]{1,0:T(8,128)(2,1)S(1)}, u32[]{:S(2)}, u32[]{:S(2)}) collective-permute-start(bf16[512,256]{1,0:T(8,128)(2,1)S(1)} %get-tuple-element.21), channel_id=1, source_target_pairs={{0,1},{1,0},{2,3},{3,2},{4,5},{5,4},{6,7},{7,6},{8,9},{9,8},{10,11... | collective-permute-start | bytes 786440 | tf_op jit(solution)/shard_map/ppermute | solution.py:507

commit v4 on v3

--- a/solution.py
+++ b/solution.py
@@ -20,9 +20,10 @@
 NORM_EPS = 1e-06
 LAYER_EPS = 1e-05
 
-KV_TILE = 256
+KV_TILE = 512
 TOK_TILE = 256
 OUT_TILE = 256
+OUT_COLS = 512
 ATT_TILE = 256
 ATT_GROUP = 4
 LANES = 128
@@ -67,13 +68,13 @@
 
 def kv_kernel(
     rows_hbm, gain_hbm, wk_hbm, wv_hbm, kg_hbm, out_ref,
-    rows_ref, gain_ref, wk_ref, wv_ref, kg_ref, even, odd, r_sem, w_sem
+    rows_ref, gain_ref, w_ref, kg_ref, even, odd, r_sem, w_sem
 ):
     chunks = rows_hbm.shape[0] // KV_TILE
     span = lambda c: pl.ds(c * KV_TILE, KV_TILE)
     row_copies = [pltpu.make_async_copy(rows_hbm.at[span(c)], rows_ref.at[span(c)], r_sem.at[c]) for c in range(chunks)]
-    wk_copy = pltpu.make_async_copy(wk_hbm, wk_ref, w_sem.at[0])
-    wv_copy = pltpu.make_async_copy(wv_hbm, wv_ref, w_sem.at[1])
+    wk_copy = pltpu.make_async_copy(wk_hbm, w_ref.at[:, :MEM_DEV], w_sem.at[0])
+    wv_copy = pltpu.make_async_copy(wv_hbm, w_ref.at[:, MEM_DEV:], w_sem.at[1])
     gain_copy = pltpu.make_async_copy(gain_hbm, gain_ref, w_sem.at[2])
     kg_copy = pltpu.make_async_copy(kg_hbm, kg_ref, w_sem.at[3])
     for c in [gain_copy, kg_copy, row_copies[0], wk_copy, wv_copy, *row_copies[1:]]:
@@ -97,9 +98,9 @@
         if c + 1 < chunks:
             row_copies[c + 1].wait()
             normalise(c + 1)
-        keys = head_norm(matmul(held[c % 2][...], wk_ref[...]), key_gain)
-        out_ref[span(c), :MEM_DEV] = keys.astype(BF16)
-        out_ref[span(c), MEM_DEV:] = matmul(held[c % 2][...], wv_ref[...]).astype(BF16)
+        both = matmul(held[c % 2][...], w_ref[...])
+        out_ref[span(c), :MEM_DEV] = head_norm(both[:, :MEM_DEV], key_gain).astype(BF16)
+        out_ref[span(c), MEM_DEV:] = both[:, MEM_DEV:].astype(BF16)
 
 
 def resident(shape):
@@ -133,8 +134,7 @@
         scratch_shapes=[
             pltpu.VMEM((n, D), BF16),
             pltpu.VMEM((D // LANES, LANES), BF16),
-            pltpu.VMEM((D, MEM_DEV), BF16),
-            pltpu.VMEM((D, MEM_DEV), BF16),
+            pltpu.VMEM((D, 2 * MEM_DEV), BF16),
             pltpu.VMEM((MEM_DEV // LANES, LANES), BF16),
             pltpu.VMEM((KV_TILE, D), BF16),
             pltpu.VMEM((KV_TILE, D), BF16),
@@ -294,30 +294,47 @@
     )(half, filtered, own_stats, peer_stats, gain)
 
 
-def pair_kernel(own_ref, peer_ref, w_own_ref, w_peer_ref, out_ref):
-    out_ref[...] = matmul(own_ref[...], w_own_ref[...]) + matmul(peer_ref[...], w_peer_ref[...])
+def pair_kernel(own_ref, peer_ref, w_own_hbm, w_peer_hbm, out_ref, w_own_ref, w_peer_ref, sem):
+    parts = D // OUT_COLS
+    cols = lambda c: pl.ds(c * OUT_COLS, OUT_COLS)
+    copies = [
+        pltpu.make_async_copy(hbm.at[:, cols(c)], ref.at[:, cols(c)], sem.at[i, c])
+        for c in range(parts)
+        for i, (hbm, ref) in enumerate(((w_own_hbm, w_own_ref), (w_peer_hbm, w_peer_ref)))
+    ]
+    for c in copies:
+        c.start()
+    for c in range(parts):
+        copies[2 * c].wait()
+        copies[2 * c + 1].wait()
+        own_part = matmul(own_ref[...], w_own_ref[:, cols(c)])
+        out_ref[:, cols(c)] = (own_part + matmul(peer_ref[...], w_peer_ref[:, cols(c)])).astype(BF16)
 
 
 def conv_product(own, peer, w_own, w_peer):
     n = own.shape[0]
-    tile = lambda width: pl.BlockSpec((OUT_TILE, width), lambda i: (i, 0))
     return pl.pallas_call(
         pair_kernel,
-        out_shape=jax.ShapeDtypeStruct((n, D), F32),
-        grid=(n // OUT_TILE,),
-        in_specs=[tile(C_DEV), tile(C_DEV), resident((C_DEV, D)), resident((C_DEV, D))],
-        out_specs=tile(D),
+        out_shape=pltpu.HBM((n, D), BF16),
+        in_specs=[ONCHIP, ONCHIP, HBM, HBM],
+        out_specs=pl.BlockSpec((n, D), lambda: (0, 0)),
+        scratch_shapes=[
+            pltpu.VMEM((C_DEV, D), BF16),
+            pltpu.VMEM((C_DEV, D), BF16),
+            pltpu.SemaphoreType.DMA((2, D // OUT_COLS)),
+        ],
+        compiler_params=grant(16),
         cost_estimate=pl.CostEstimate(flops=4 * n * D * C_DEV, transcendentals=0, bytes_accessed=12 << 20),
         name="conv_product",
-    )(own, peer, w_own, w_peer)
-
-
-def attend_blocks(blocks, kv_ref, q_ref, gate):
+    )(*onchip(own, peer), *offchip(w_own, w_peer))
+
+
+def attend_blocks(blocks, kv_ref, q_ref, base, gate):
     heads = MEM_DEV // MEM_HD
     lane_head = lax.broadcasted_iota(jnp.int32, (BLOCK, MEM_DEV), 1) // MEM_HD
     scores = []
     for b in blocks:
-        q = q_ref[b * BLOCK : (b + 1) * BLOCK, :]
+        q = q_ref[pl.ds(base + b * BLOCK, BLOCK), :]
         spread = jnp.concatenate([jnp.where(lane_head == h, q, jnp.zeros_like(q)) for h in range(heads)], axis=0)
         scores.append(matmul_t(spread, kv_ref[2 * b : 2 * b + 2, :, :MEM_DEV].reshape(2 * PLEN, MEM_DEV)))
     expanded = [jnp.exp(s - jnp.max(s, axis=1, keepdims=True)) for s in scores]
@@ -335,47 +352,39 @@
 SCALARS = pl.BlockSpec(memory_space=pltpu.SMEM)
 
 
-def read_scratch(count, n):
-    return [
-        pltpu.VMEM((count, PLEN, 2 * MEM_DEV), BF16),
-        pltpu.VMEM((n, MEM_DEV), BF16),
-        pltpu.SemaphoreType.DMA((count,)),
-        pltpu.SemaphoreType.DMA(()),
-    ]
-
-
-def attend_all(out_ref, kv_ref, q_ref, gate, arrived):
+def attend_all(out_ref, kv_ref, q_ref, base, gate, arrived):
     size = ATT_GROUP * BLOCK
     for g in range(out_ref.shape[0] // size):
         arrived(g)
         blocks = range(g * ATT_GROUP, (g + 1) * ATT_GROUP)
-        out_ref[pl.ds(g * size, size), :] = attend_blocks(blocks, kv_ref, q_ref, gate)
+        out_ref[pl.ds(g * size, size), :] = attend_blocks(blocks, kv_ref, q_ref, base, gate)
 
 
 def attend_kernel(
-    half_ref, owner_ref, recv_hbm, q_hbm, gate_ref, out_ref, next_kv_ref, next_q_ref, kv_ref, q_ref, sem, q_sem, next_sem, next_q_sem
+    half_ref, owner_ref, recv_hbm, q_ref, gate_ref, out_ref, next_kv_ref, next_q_ref, kv_ref, sem, next_sem, q_sem
 ):
     count = kv_ref.shape[0]
-    n = q_ref.shape[0]
+    n = next_q_ref.shape[0]
     first, second = half_ref[0], 1 - half_ref[0]
-    q_copy = pltpu.make_async_copy(q_hbm.at[pl.ds(pl.multiple_of(first * n, n), n), :], q_ref, q_sem)
     copies = [
         pltpu.make_async_copy(recv_hbm.at[owner_ref[first * count + i]], kv_ref.at[i], sem.at[i]) for i in range(count)
     ]
-    later = [pltpu.make_async_copy(q_hbm.at[pl.ds(pl.multiple_of(second * n, n), n), :], next_q_ref, next_q_sem)] + [
+    later = [
         pltpu.make_async_copy(recv_hbm.at[owner_ref[second * count + i]], next_kv_ref.at[i], next_sem.at[i])
         for i in range(count)
-    ]
-    for c in [q_copy, *copies, *later]:
+    ] + [pltpu.make_async_copy(q_ref.at[pl.ds(pl.multiple_of(second * n, n), n), :], next_q_ref, q_sem)]
+    for c in copies:
         c.start()
     gate = jnp.tanh(wide_row(gate_ref))
-    q_copy.wait()
 
     def arrived(g):
         for c in copies[2 * g * ATT_GROUP : 2 * (g + 1) * ATT_GROUP]:
             c.wait()
-
-    attend_all(out_ref, kv_ref, q_ref, gate, arrived)
+        if g == 0:
+            for c in later:
+                c.start()
+
+    attend_all(out_ref, kv_ref, q_ref, pl.multiple_of(first * n, n), gate, arrived)
     for c in later:
         c.wait()
 
@@ -390,17 +399,22 @@
             pltpu.VMEM((count, PLEN, 2 * MEM_DEV), BF16),
             pltpu.VMEM((n, MEM_DEV), BF16),
         ),
-        in_specs=[SCALARS, SCALARS, HBM, HBM, ONCHIP],
+        in_specs=[SCALARS, SCALARS, HBM, ONCHIP, ONCHIP],
         out_specs=(ONCHIP, ONCHIP, ONCHIP),
-        scratch_shapes=read_scratch(count, n) + [pltpu.SemaphoreType.DMA((count,)), pltpu.SemaphoreType.DMA(())],
+        scratch_shapes=[
+            pltpu.VMEM((count, PLEN, 2 * MEM_DEV), BF16),
+            pltpu.SemaphoreType.DMA((count,)),
+            pltpu.SemaphoreType.DMA((count,)),
+            pltpu.SemaphoreType.DMA(()),
+        ],
         compiler_params=grant(8),
         cost_estimate=pl.CostEstimate(flops=n * D * 256, transcendentals=0, bytes_accessed=2 << 20),
         name="attend_first",
-    )(half, owners, *offchip(received, queries), *onchip(gate))
+    )(half, owners, *offchip(received), *onchip(queries, gate))
 
 
 def attend_rest_kernel(kv_ref, q_ref, gate_ref, out_ref):
-    attend_all(out_ref, kv_ref, q_ref, jnp.tanh(wide_row(gate_ref)), lambda g: None)
+    attend_all(out_ref, kv_ref, q_ref, 0, jnp.tanh(wide_row(gate_ref)), lambda g: None)
 
 
 def attend_rest(kv, queries, gate):
@@ -422,7 +436,7 @@
     out_copies = [pltpu.make_async_copy(out_ref.at[span(g)], out_hbm.at[span(g)], out_sem.at[g]) for g in range(groups)]
     for g in range(groups):
         memory = matmul(own_ref[span(g), :], w_own_ref[...]) + matmul(peer_ref[span(g), :], w_peer_ref[...])
-        out_ref[span(g), :] = (conv_ref[span(g), :] + memory).astype(BF16)
+        out_ref[span(g), :] = (conv_ref[span(g), :].astype(F32) + memory).astype(BF16)
         out_copies[g].start()
     for c in out_copies:
         c.wait()
@@ -465,9 +479,9 @@
     swap = [(0, 1), (1, 0)]
     me = lax.axis_index("tp").astype(jnp.int32).reshape(1)
 
-    everyone = jnp.arange(owner_count, dtype=jnp.int32)[:, None, None, None]
-    spread = jnp.broadcast_to(passage_ids, (owner_count, LANES, *passage_ids.shape))
-    wanted = jnp.sum(jnp.where(spread >> OWNER_SHIFT == everyone, spread & (PASS_DEV - 1), 0), axis=(2, 3))
+    everyone = lax.broadcasted_iota(jnp.int32, (owner_count, LANES, *passage_ids.shape), 0)
+    local = passage_ids ^ (everyone << OWNER_SHIFT)
+    wanted = jnp.sum(jnp.where(local < PASS_DEV, local, 0), axis=(2, 3))
     asked = lax.all_to_all(wanted, "st", 0, 0, tiled=True)
     peer_tokens = lax.ppermute(tokens, "tp", swap)
     peer_conv_weight = lax.ppermute(conv_out_weight, "tp", swap)
@@ -500,7 +514,6 @@
     conv_mine = channel_swish(me, filtered, own_stats, peer_stats, ln_gain.reshape(-1, LANES))
     conv_sum = conv_product(conv_mine, conv_peer, conv_out_weight, peer_conv_weight)
 
-    received, conv_sum = lax.optimization_barrier((received, conv_sum))
     owners = lax.optimization_barrier((passage_ids, filtered))[0].reshape(-1) >> OWNER_SHIFT
     gate = memory_gate.reshape(-1, LANES)
     memory_theirs, next_kv, next_queries = attend_first(1 - me, owners, received, queries, gate)

time: 99.4 us -> 107 us (1.076)
  waiting for transfers between devices: 11.9 us -> 22.5 us
  Pallas kernels: 56.8 us -> 54.1 us
  starting transfers between devices: 25.4 us -> 23.8 us
    all_to_all x1, waiting for transfers between devices: 9.53 us -> 17.9 us  [body(): received = lax.all_to_all(sent, 'st', 0, 0, tiled=True)]
    all_to_all x1, starting transfers between devices: 9.99 us -> 7.59 us  [body(): received = lax.all_to_all(sent, 'st', 0, 0, tiled=True)]
    all_to_all x1, waiting for transfers between devices: 0.53 us -> 2.46 us  [body(): asked = lax.all_to_all(wanted, 'st', 0, 0, tiled=True)]
    pallas_call x1, Pallas kernels: 7.44 us -> 5.88 us  [project_store(): pl.pallas_call(kv_kernel, out_shape=pltpu.VMEM((n, 2 * MEM_DEV), BF16), i...]
    unnamed x14 -> x16, local copies, waits for them, and re-layouts: 3 us -> 3.73 us
  transfers between devices with their start and end apart: 8 -> 8, of which waited for: 3 -> 3; matrix products, arithmetic and copies ran while one was open for 2% -> 2% of each run, Pallas kernels for 55% -> 49%
where the time goes in v4:
time: 107 us; the launch traced here: 106 us
  Pallas kernels  54.1 us (51%)
  starting transfers between devices  23.8 us (22%)
  waiting for transfers between devices  22.5 us (21%)
  local copies, waits for them, and re-layouts  3.9 us (4%)
  other arithmetic  1.74 us (2%)
    pallas_call x1, Pallas kernels, token_branch(): pl.pallas_call(token_kernel, out_shape=(jax.ShapeDtypeStruct((n, C_DEV),...  24.8 us
    all_to_all x1, waiting for transfers between devices, body(): received = lax.all_to_all(sent, 'st', 0, 0, tiled=True)  17.9 us
    all_to_all x1, starting transfers between devices, body(): asked = lax.all_to_all(wanted, 'st', 0, 0, tiled=True)  11.2 us
    pallas_call x1, Pallas kernels, conv_product(): pl.pallas_call(pair_kernel, out_shape=pltpu.HBM((n, D), BF16), in_specs=[...  7.84 us
    all_to_all x1, starting transfers between devices, body(): received = lax.all_to_all(sent, 'st', 0, 0, tiled=True)  7.59 us
    pallas_call x1, Pallas kernels, project_store(): pl.pallas_call(kv_kernel, out_shape=pltpu.VMEM((n, 2 * MEM_DEV), BF16), i...  5.88 us
    pallas_call x2, Pallas kernels, channel_swish(): pl.pallas_call(lambda half_ref, *refs: swish_kernel(*refs), out_shape=jax...  5.34 us
    unnamed x16, local copies, waits for them, and re-layouts  3.73 us
  transfers between devices with their start and end apart: 8, of which 3 were waited for; matrix products, arithmetic and copies ran while one was open for 2% of the time, Pallas kernels for 49%

profile of v4, /device:TPU:1, one launch (start us, length us, event | category | flops | bytes accessed | tf_op | source)
XLA Modules:
  0.0 106.3 jit_solution(8946636808296047928)
XLA Ops:
  0.0 1.4 %collective-permute-start = (bf16[1024,1024]{1,0:T(8,128)(2,1)}, bf16[1024,1024]{1,0:T(8,128)(2,1)S(1)}, u32[]{:S(2)}, u32[]{:S(2)}) collective-permute-start(bf16[1024,1024]{1,0:T(8,128)(2,1)} %own_ref.1), channel_id=1, source_target_pairs={{0,1},{1,0},{2,3},{3,2},{4,5},{5,4},{6,7},{7,6},{8,9},{9,8},{10,11... | collective-permute-start | bytes 6291464 | tf_op jit(solution)/shard_map/ppermute | solution.py:486
  1.4 1.7 %fusion = s32[64,128]{1,0:T(8,128)} fusion(s32[64]{0:T(128)S(1)} %iota_shift-left_fusion, s32[16,2]{0,1:T(2,128)} %param.18), kind=kLoop, calls=%fused_computation.1 | loop fusion | flops 1040384 | bytes 33152 | tf_op jit(solution)/shard_map/reduce_sum | solution.py:484
  3.1 11.2 %all-to-all-start = ((s32[64,1,128]{2,1,0:T(1,128)}), s32[64,1,128]{2,1,0:T(1,128)S(1)}, u32[]{:S(2)}, u32[]{:S(2)}) async-start(s32[64,1,128]{2,1,0:T(1,128)} %bitcast.4), calls=%async_computation | async-start | bytes 65536 | tf_op jit(solution)/shard_map/all_to_all | solution.py:485
  14.4 5.9 %project_store.1 = bf16[1024,512]{1,0:T(8,128)(2,1)S(1)} custom-call(bf16[1024,2048]{1,0:T(8,128)(2,1)} %bitcast.19, bf16[16,128]{1,0:T(8,128)(2,1)} %bitcast.20, bf16[2048,256]{1,0:T(8,128)(2,1)} %wk_hbm.1, bf16[2048,256]{1,0:T(8,128)(2,1)} %wv_hbm.1, bf16[2,128]{1,0:T(2,128)(2,1)} %bitcast.22), custom_call_target="tpu_custom_call" | custom-call | flops 2147483648 | bytes 8388608 | tf_op jit(solution)/shard_map/project_store/pallas_call | solution.py:129
  20.3 2.5 %all-to-all-done = s32[64,1,128]{2,1,0:T(1,128)S(1)} async-done(((s32[64,1,128]{2,1,0:T(1,128)}), s32[64,1,128]{2,1,0:T(1,128)S(1)}, u32[]{:S(2)}, u32[]{:S(2)}) %all-to-all-start) | async-done | bytes 32800 | tf_op jit(solution)/shard_map/all_to_all | solution.py:485
  22.7 3.6 %fill_slots.1 = bf16[64,64,512]{2,1,0:T(8,128)(2,1)} custom-call(s32[64,128]{1,0:T(8,128)S(1)} %bitcast.14, bf16[16,64,512]{2,1,0:T(8,128)(2,1)S(1)} %bitcast.13), custom_call_target="tpu_custom_call" | custom-call | tf_op jit(solution)/shard_map/fill_slots/pallas_call | solution.py:164
  26.4 7.6 %all-to-all-start.1 = ((bf16[64,64,512]{2,1,0:T(8,128)(2,1)}), bf16[64,64,512]{2,1,0:T(8,128)(2,1)}, u32[]{:S(2)}, u32[]{:S(2)}) async-start(bf16[64,64,512]{2,1,0:T(8,128)(2,1)} %fill_slots.1), calls=%async_computation.1 | async-start | bytes 8388608 | tf_op jit(solution)/shard_map/all_to_all | solution.py:498
  34.0 0.9 collective-permute-start.5
  34.9 0.0 collective-permute-done.peer_ref
  34.9 0.0 copy-start.7
  34.9 1.3 %copy-done.7 = bf16[1024,1024]{1,0:T(8,128)(2,1)} copy-done((bf16[1024,1024]{1,0:T(8,128)(2,1)}, bf16[1024,1024]{1,0:T(8,128)(2,1)S(1)}, u32[]{:S(2)}) %copy-start.7) | copy-done | bytes 2097176
  36.2 24.8 %token_branch.1 = (f32[1024,768]{1,0:T(8,128)}, f32[1024,2]{1,0:T(8,128)}, bf16[1024,256]{1,0:T(8,128)(2,1)}) custom-call(s32[1]{0:T(128)} %bitcast.tp_ref.half_ref, bf16[1024,1024]{1,0:T(8,128)(2,1)} %own_ref.1, bf16[1024,1024]{1,0:T(8,128)(2,1)} %copy-done.7, bf16[2,8,128]{2,1,0:T(8,128)(2,1)} %bitcast.21, bf16[2048,768]{1,0:T(8,128)(2,1)} %wv_ref.1, ...), custom_call_target="tpu_custom_call" | custom-call | flops 32212254720 | bytes 16777216 | tf_op jit(solution)/shard_map/token_branch/pallas_call | solution.py:238
  61.0 0.0 copy-start.1
  61.0 0.0 copy-start.6
  61.0 0.3 collective-permute-start.3
  61.3 2.1 %collective-permute-done.3.refs_2_ = f32[1024,2]{1,0:T(8,128)S(1)} collective-permute-done((f32[1024,2]{1,0:T(8,128)}, f32[1024,2]{1,0:T(8,128)S(1)}, u32[]{:S(2)}, u32[]{:S(2)}) %collective-permute-start.3) | collective-permute-done | bytes 8224 | tf_op jit(solution)/shard_map/ppermute | solution.py:511
  63.4 0.0 copy-start.5
  63.4 0.8 copy-done.5
  64.2 2.7 %channel_swish.3 = bf16[512,768]{1,0:T(8,128)(2,1)} custom-call(s32[1]{0:T(128)S(6)} %sub.4.half_ref, f32[1024,768]{1,0:T(8,128)} %get-tuple-element.12.refs_0_, f32[1024,2]{1,0:T(8,128)} %get-tuple-element.18.refs_1_, f32[1024,2]{1,0:T(8,128)} %copy-done.5, bf16[6,128]{1,0:T(8,128)(2,1)} %bitcast.17), custom_call_target="tpu_custom_call" | custom-call | flops 805306368 | bytes 4194304 | tf_op jit(solution)/shard_map/channel_swish/pallas_call | solution.py:283
  66.9 0.0 copy-start.3
  66.9 0.0 copy-start.4
  66.9 0.1 collective-permute-start.4
  67.0 0.0 copy-done.1
  67.0 0.4 collective-permute-start.2
  67.4 0.0 copy-done.6
  67.4 0.1 copy.24
  67.5 0.1 shift_right_arithmetic.10.owner_ref
  67.6 2.7 %channel_swish.2.own_ref = bf16[512,768]{1,0:T(8,128)(2,1)} custom-call(s32[1]{0:T(128)} %bitcast.tp_ref.half_ref, f32[1024,768]{1,0:T(8,128)} %get-tuple-element.12.refs_0_, f32[1024,2]{1,0:T(8,128)} %get-tuple-element.18.refs_1_, f32[1024,2]{1,0:T(8,128)} %copy-done.5, bf16[6,128]{1,0:T(8,128)(2,1)} %bitcast.18), custom_call_target="tpu_custom_call" | custom-call | flops 805306368 | bytes 4194304 | tf_op jit(solution)/shard_map/channel_swish/pallas_call | solution.py:283
  70.3 0.0 copy-start.2
  70.3 17.9 %all-to-all-done.1.recv_hbm = bf16[64,64,512]{2,1,0:T(8,128)(2,1)} async-done(((bf16[64,64,512]{2,1,0:T(8,128)(2,1)}), bf16[64,64,512]{2,1,0:T(8,128)(2,1)}, u32[]{:S(2)}, u32[]{:S(2)}) %all-to-all-start.1) | async-done | bytes 4194336 | tf_op jit(solution)/shard_map/all_to_all | solution.py:498
  88.2 0.0 copy-done.3
  88.2 0.0 copy-done.4
  88.2 3.3 %attend_first.1 = (bf16[512,256]{1,0:T(8,128)(2,1)S(1)}, bf16[16,64,512]{2,1,0:T(8,128)(2,1)S(1)}, bf16[512,256]{1,0:T(8,128)(2,1)S(1)}) custom-call(s32[1]{0:T(128)S(6)} %sub.4.half_ref, s32[32]{0:T(128)S(1)} %shift_right_arithmetic.10.owner_ref, bf16[64,64,512]{2,1,0:T(8,128)(2,1)} %all-to-all-done.1.recv_hbm, bf16[1024,256]{1,0:T(8,128)(2,1)S(1)} %copy-done.3, ...), custom_call_target="tpu_custom_call" | custom-call | flops 268435456 | bytes 2097152 | tf_op jit(solution)/shard_map/attend_first/pallas_call | solution.py:395
  91.4 1.8 %collective-permute-start.1 = (bf16[512,256]{1,0:T(8,128)(2,1)S(1)}, bf16[512,256]{1,0:T(8,128)(2,1)S(1)}, u32[]{:S(2)}, u32[]{:S(2)}) collective-permute-start(bf16[512,256]{1,0:T(8,128)(2,1)S(1)} %get-tuple-element.17), channel_id=1, source_target_pairs={{0,1},{1,0},{2,3},{3,2},{4,5},{5,4},{6,7},{7,6},{8,9},{9,8},{10,11... | collective-permute-start | bytes 786440 | tf_op jit(solution)/shard_map/ppermute | solution.py:520
  93.3 0.0 collective-permute-done.4.peer_ref
  93.3 0.0 collective-permute-done.5.w_peer_hbm
  93.3 0.0 copy-done.2
  93.3 7.8 %conv_product.1.conv_ref = bf16[512,2048]{1,0:T(8,128)(2,1)} custom-call(bf16[512,768]{1,0:T(8,128)(2,1)S(1)} %copy-done.2, bf16[512,768]{1,0:T(8,128)(2,1)} %collective-permute-done.4.peer_ref, bf16[768,2048]{1,0:T(8,128)(2,1)} %w_own_hbm.1, bf16[768,2048]{1,0:T(8,128)(2,1)} %collective-permute-done.5.w_peer_hbm), custom_call_target="tpu_custom_call" | custom-call | flops 3221225472 | bytes 12582912 | tf_op jit(solution)/shard_map/conv_product/pallas_call | solution.py:316
  101.1 1.1 %attend_rest.1.own_ref = bf16[512,256]{1,0:T(8,128)(2,1)S(1)} custom-call(bf16[16,64,512]{2,1,0:T(8,128)(2,1)S(1)} %get-tuple-element.15.kv_ref, bf16[512,256]{1,0:T(8,128)(2,1)S(1)} %get-tuple-element.16.q_ref, bf16[2,128]{1,0:T(2,128)(2,1)S(1)} %bitcast.16), custom_call_target="tpu_custom_call" | custom-call | flops 268435456 | bytes 2097152 | tf_op jit(solution)/shard_map/attend_rest/pallas_call | solution.py:422
  102.3 0.0 collective-permute-done.2.w_peer_ref
  102.3 0.0 collective-permute-done.1.peer_ref
  102.3 0.0 copy-start
  102.3 1.6 %copy-done = bf16[512,2048]{1,0:T(8,128)(2,1)S(1)} copy-done((bf16[512,2048]{1,0:T(8,128)(2,1)S(1)}, bf16[512,2048]{1,0:T(8,128)(2,1)}, u32[]{:S(2)}) %copy-start) | copy-done | bytes 2097176
  103.9 2.2 %finish.1 = bf16[512,2048]{1,0:T(8,128)(2,1)} custom-call(bf16[512,256]{1,0:T(8,128)(2,1)S(1)} %attend_rest.1.own_ref, bf16[512,256]{1,0:T(8,128)(2,1)S(1)} %collective-permute-done.1.peer_ref, bf16[256,2048]{1,0:T(8,128)(2,1)S(1)} %copy-done.1, bf16[256,2048]{1,0:T(8,128)(2,1)S(1)} %collective-permute-done.2.w_peer_ref, bf16[512,2048]{1,0:T(8,128)(2,1)S(1)} %copy-done), custom_call_target="tpu_custom_call" | custom-call | flops 1073741824 | bytes 8388608 | tf_op jit(solution)/shard_map/finish/pallas_call | solution.py:447
  (2 shorter events, 0.0 us)
Async XLA Ops:
  0.0 34.9 %collective-permute-start = (bf16[1024,1024]{1,0:T(8,128)(2,1)}, bf16[1024,1024]{1,0:T(8,128)(2,1)S(1)}, u32[]{:S(2)}, u32[]{:S(2)}) collective-permute-start(bf16[1024,1024]{1,0:T(8,128)(2,1)} %own_ref.1), channel_id=1, source_target_pairs={{0,1},{1,0},{2,3},{3,2},{4,5},{5,4},{6,7},{7,6},{8,9},{9,8},{10,11... | collective-permute-start | bytes 6291464 | tf_op jit(solution)/shard_map/ppermute | solution.py:486
  3.1 19.6 %all-to-all-start = ((s32[64,1,128]{2,1,0:T(1,128)}), s32[64,1,128]{2,1,0:T(1,128)S(1)}, u32[]{:S(2)}, u32[]{:S(2)}) async-start(s32[64,1,128]{2,1,0:T(1,128)} %bitcast.4), calls=%async_computation | async-start | bytes 65536 | tf_op jit(solution)/shard_map/all_to_all | solution.py:485
  26.4 61.8 %all-to-all-start.1 = ((bf16[64,64,512]{2,1,0:T(8,128)(2,1)}), bf16[64,64,512]{2,1,0:T(8,128)(2,1)}, u32[]{:S(2)}, u32[]{:S(2)}) async-start(bf16[64,64,512]{2,1,0:T(8,128)(2,1)} %fill_slots.1), calls=%async_computation.1 | async-start | bytes 8388608 | tf_op jit(solution)/shard_map/all_to_all | solution.py:498
  34.0 59.3 %collective-permute-start.5 = (bf16[768,2048]{1,0:T(8,128)(2,1)}, bf16[768,2048]{1,0:T(8,128)(2,1)}, u32[]{:S(2)}, u32[]{:S(2)}) collective-permute-start(bf16[768,2048]{1,0:T(8,128)(2,1)} %w_own_hbm.1), channel_id=1, source_target_pairs={{0,1},{1,0},{2,3},{3,2},{4,5},{5,4},{6,7},{7,6},{8,9},{9,8},{10,11... | collective-permute-start | bytes 9437192 | tf_op jit(solution)/shard_map/ppermute | solution.py:487
  34.9 1.3 %copy-start.7 = (bf16[1024,1024]{1,0:T(8,128)(2,1)}, bf16[1024,1024]{1,0:T(8,128)(2,1)S(1)}, u32[]{:S(2)}) copy-start(bf16[1024,1024]{1,0:T(8,128)(2,1)S(1)} %collective-permute-done.peer_ref) | copy-start | bytes 6291460
  61.0 6.0 %copy-start.1 = (bf16[256,2048]{1,0:T(8,128)(2,1)S(1)}, bf16[256,2048]{1,0:T(8,128)(2,1)}, u32[]{:S(2)}) copy-start(bf16[256,2048]{1,0:T(8,128)(2,1)} %w_own_ref.1) | copy-start | bytes 3145732
  61.0 6.4 %copy-start.6 = (s32[16,2]{0,1:T(2,128)S(1)}, s32[16,2]{0,1:T(2,128)}, u32[]{:S(2)}) copy-start(s32[16,2]{0,1:T(2,128)} %param.18) | copy-start | bytes 388
  61.0 2.4 %collective-permute-start.3 = (f32[1024,2]{1,0:T(8,128)}, f32[1024,2]{1,0:T(8,128)S(1)}, u32[]{:S(2)}, u32[]{:S(2)}) collective-permute-start(f32[1024,2]{1,0:T(8,128)} %get-tuple-element.18.refs_1_), channel_id=1, source_target_pairs={{0,1},{1,0},{2,3},{3,2},{4,5},{5,4},{6,7},{7,6},{8,9},{9,8},{10,11... | collective-permute-start | bytes 24584 | tf_op jit(solution)/shard_map/ppermute | solution.py:511
  63.4 0.8 copy-start.5
  66.9 21.3 %copy-start.3 = (bf16[1024,256]{1,0:T(8,128)(2,1)S(1)}, bf16[1024,256]{1,0:T(8,128)(2,1)}, u32[]{:S(2)}) copy-start(bf16[1024,256]{1,0:T(8,128)(2,1)} %get-tuple-element.14.q_ref) | copy-start | bytes 1572868
  66.9 21.3 %copy-start.4 = (bf16[256]{0:T(256)(128)(2,1)S(1)}, bf16[256]{0:T(256)(128)(2,1)}, u32[]{:S(2)}) copy-start(bf16[256]{0:T(256)(128)(2,1)} %param.31) | copy-start | bytes 1540
  66.9 26.4 %collective-permute-start.4 = (bf16[512,768]{1,0:T(8,128)(2,1)}, bf16[512,768]{1,0:T(8,128)(2,1)}, u32[]{:S(2)}, u32[]{:S(2)}) collective-permute-start(bf16[512,768]{1,0:T(8,128)(2,1)} %channel_swish.3), channel_id=1, source_target_pairs={{0,1},{1,0},{2,3},{3,2},{4,5},{5,4},{6,7},{7,6},{8,9},{9,8},{10,11... | collective-permute-start | bytes 2359304 | tf_op jit(solution)/shard_map/ppermute | solution.py:513
  67.0 35.2 %collective-permute-start.2 = (bf16[256,2048]{1,0:T(8,128)(2,1)S(1)}, bf16[256,2048]{1,0:T(8,128)(2,1)S(1)}, u32[]{:S(2)}, u32[]{:S(2)}) collective-permute-start(bf16[256,2048]{1,0:T(8,128)(2,1)S(1)} %copy-done.1), channel_id=1, source_target_pairs={{0,1},{1,0},{2,3},{3,2},{4,5},{5,4},{6,7},{7,6},{8,9},{9,8},{10,11... | collective-permute-start | bytes 3145736 | tf_op jit(solution)/shard_map/ppermute | solution.py:488
  70.3 23.0 %copy-start.2 = (bf16[512,768]{1,0:T(8,128)(2,1)S(1)}, bf16[512,768]{1,0:T(8,128)(2,1)}, u32[]{:S(2)}) copy-start(bf16[512,768]{1,0:T(8,128)(2,1)} %channel_swish.2.own_ref) | copy-start | bytes 2359300
  91.4 10.8 %collective-permute-start.1 = (bf16[512,256]{1,0:T(8,128)(2,1)S(1)}, bf16[512,256]{1,0:T(8,128)(2,1)S(1)}, u32[]{:S(2)}, u32[]{:S(2)}) collective-permute-start(bf16[512,256]{1,0:T(8,128)(2,1)S(1)} %get-tuple-element.17), channel_id=1, source_target_pairs={{0,1},{1,0},{2,3},{3,2},{4,5},{5,4},{6,7},{7,6},{8,9},{9,8},{10,11... | collective-permute-start | bytes 786440 | tf_op jit(solution)/shard_map/ppermute | solution.py:520
  102.3 1.6 %copy-start = (bf16[512,2048]{1,0:T(8,128)(2,1)S(1)}, bf16[512,2048]{1,0:T(8,128)(2,1)}, u32[]{:S(2)}) copy-start(bf16[512,2048]{1,0:T(8,128)(2,1)} %conv_product.1.conv_ref) | copy-start | bytes 6291460

commit v5 on v4

--- a/solution.py
+++ b/solution.py
@@ -147,33 +147,39 @@
     )(*offchip(rows, passage_gain, key_weight, value_weight, key_gain))
 
 
-def slots_kernel(asked_ref, kv_ref, out_ref, table, table_sem, sem):
-    count = out_ref.shape[0]
-    fetch = pltpu.make_async_copy(asked_ref, table, table_sem)
+def slots_kernel(st_ref, ids_ref, kv_ref, out_hbm, row_ref, table, table_sem, sem):
+    count = out_hbm.shape[0]
+    local = ids_ref[...] ^ (st_ref[0] * PASS_DEV)
+    asked = jnp.where(local < PASS_DEV, local, 0)
+    asked = jnp.sum(asked[:, 0, :] + asked[:, 1, :], axis=1, keepdims=True).astype(F32)
+    square = jnp.concatenate([jnp.broadcast_to(asked, (count, LANES)), jnp.zeros((LANES - count, LANES), F32)], axis=0)
+    row_ref[...] = square.T[:8, :].astype(jnp.int32)
+    fetch = pltpu.make_async_copy(row_ref, table, table_sem)
     fetch.start()
     fetch.wait()
-    copies = [pltpu.make_async_copy(kv_ref.at[table[s, 0]], out_ref.at[s], sem.at[s]) for s in range(count)]
+    copies = [pltpu.make_async_copy(kv_ref.at[table[0, s]], out_hbm.at[s], sem.at[s]) for s in range(count)]
     for c in copies:
         c.start()
     for c in copies:
         c.wait()
 
 
-def fill_slots(asked, kv):
-    count = asked.shape[0]
+def fill_slots(st, ids, kv):
+    count = ids.shape[0]
     return pl.pallas_call(
         slots_kernel,
         out_shape=pltpu.HBM((count, PLEN, 2 * MEM_DEV), BF16),
-        in_specs=[ONCHIP, ONCHIP],
+        in_specs=[pl.BlockSpec(memory_space=pltpu.SMEM), ONCHIP, ONCHIP],
         out_specs=HBM,
         scratch_shapes=[
-            pltpu.SMEM(asked.shape, jnp.int32),
+            pltpu.VMEM((8, LANES), jnp.int32),
+            pltpu.SMEM((8, LANES), jnp.int32),
             pltpu.SemaphoreType.DMA(()),
             pltpu.SemaphoreType.DMA((count,)),
         ],
         compiler_params=grant(2),
         name="fill_slots",
-    )(*onchip(asked, kv))
+    )(st, *onchip(ids, kv))
 
 
 def token_kernel(
@@ -479,10 +485,7 @@
     swap = [(0, 1), (1, 0)]
     me = lax.axis_index("tp").astype(jnp.int32).reshape(1)
 
-    everyone = lax.broadcasted_iota(jnp.int32, (owner_count, LANES, *passage_ids.shape), 0)
-    local = passage_ids ^ (everyone << OWNER_SHIFT)
-    wanted = jnp.sum(jnp.where(local < PASS_DEV, local, 0), axis=(2, 3))
-    asked = lax.all_to_all(wanted, "st", 0, 0, tiled=True)
+    ids = lax.all_to_all(jnp.broadcast_to(passage_ids.T, (owner_count, *passage_ids.shape[::-1])), "st", 0, 0, tiled=True)
     peer_tokens = lax.ppermute(tokens, "tp", swap)
     peer_conv_weight = lax.ppermute(conv_out_weight, "tp", swap)
     peer_memory_weight = lax.ppermute(memory_out_weight, "tp", swap)
@@ -494,7 +497,7 @@
         value_weight,
         key_gain.reshape(-1, LANES),
     ).reshape(PASS_DEV, PLEN, 2 * MEM_DEV)
-    sent = fill_slots(asked, kv)
+    sent = fill_slots(lax.axis_index("st").astype(jnp.int32).reshape(1), ids, kv)
     received = lax.all_to_all(sent, "st", 0, 0, tiled=True)
 
     filtered, own_stats, queries = token_branch(

time: 107 us -> 106 us (level)
  other arithmetic: 1.74 us -> 0.01 us
  local copies, waits for them, and re-layouts: 3.9 us -> 5.22 us
    reduce_sum x1 -> x0, other arithmetic: 1.73 us -> none  [body(): wanted = jnp.sum(jnp.where(local < PASS_DEV, local, 0), axis=(2, 3))]
    broadcast_in_dim x0 -> x1, local copies, waits for them, and re-layouts: none -> 1.32 us  [body(): jnp.broadcast_to(passage_ids.T, (owner_count, *passage_ids.shape[::-1]))]
  transfers between devices with their start and end apart: 8 -> 8, of which waited for: 3 -> 3; matrix products, arithmetic and copies ran while one was open for 2% -> 1% of each run, Pallas kernels for 49% -> 49%
where the time goes in v5:
time: 106 us
  Pallas kernels  53.9 us (51%)
  starting transfers between devices  23.6 us (22%)
  waiting for transfers between devices  22.5 us (21%)
  local copies, waits for them, and re-layouts  5.22 us (5%)
    pallas_call x1, Pallas kernels, token_branch(): pl.pallas_call(token_kernel, out_shape=(jax.ShapeDtypeStruct((n, C_DEV),...  24.9 us
    all_to_all x1, waiting for transfers between devices, body(): received = lax.all_to_all(sent, 'st', 0, 0, tiled=True)  17.9 us
    all_to_all x1, starting transfers between devices, body(): lax.all_to_all(jnp.broadcast_to(passage_ids.T, (owner_count, *passage_ids...  11.2 us
    pallas_call x1, Pallas kernels, conv_product(): pl.pallas_call(pair_kernel, out_shape=pltpu.HBM((n, D), BF16), in_specs=[...  7.84 us
    all_to_all x1, starting transfers between devices, body(): received = lax.all_to_all(sent, 'st', 0, 0, tiled=True)  7.51 us
    pallas_call x1, Pallas kernels, project_store(): pl.pallas_call(kv_kernel, out_shape=pltpu.VMEM((n, 2 * MEM_DEV), BF16), i...  5.87 us
    pallas_call x2, Pallas kernels, channel_swish(): pl.pallas_call(lambda half_ref, *refs: swish_kernel(*refs), out_shape=jax...  5.33 us
    unnamed x16, local copies, waits for them, and re-layouts  3.72 us
  transfers between devices with their start and end apart: 8, of which 3 were waited for; matrix products, arithmetic and copies ran while one was open for 1% of the time, Pallas kernels for 49%

profile of v5, /device:TPU:1, one launch (start us, length us, event | category | flops | bytes accessed | tf_op | source)
XLA Modules:
  0.0 105.6 jit_solution(7507841684497144445)
XLA Ops:
  0.0 1.4 %collective-permute-start = (bf16[1024,1024]{1,0:T(8,128)(2,1)}, bf16[1024,1024]{1,0:T(8,128)(2,1)S(1)}, u32[]{:S(2)}, u32[]{:S(2)}) collective-permute-start(bf16[1024,1024]{1,0:T(8,128)(2,1)} %own_ref.1), channel_id=1, source_target_pairs={{0,1},{1,0},{2,3},{3,2},{4,5},{5,4},{6,7},{7,6},{8,9},{9,8},{10,11... | collective-permute-start | bytes 6291464 | tf_op jit(solution)/shard_map/ppermute | solution.py:489
  1.4 1.3 %broadcast_in_dim.3 = s32[64,2,16]{2,1,0:T(2,128)} broadcast(s32[2,16]{1,0:T(2,128)} %bitcast.16), dimensions={1,2} | broadcast | bytes 8320 | tf_op jit(solution)/shard_map/broadcast_in_dim | solution.py:488
  2.7 11.2 %all-to-all-start = ((s32[64,2,16]{2,1,0:T(2,128)}), s32[64,2,16]{2,1,0:T(2,128)S(1)}, u32[]{:S(2)}, u32[]{:S(2)}) async-start(s32[64,2,16]{2,1,0:T(2,128)} %broadcast_in_dim.3), calls=%async_computation | async-start | bytes 131072 | tf_op jit(solution)/shard_map/all_to_all | solution.py:488
  14.0 5.9 %project_store.1 = bf16[1024,512]{1,0:T(8,128)(2,1)S(1)} custom-call(bf16[1024,2048]{1,0:T(8,128)(2,1)} %bitcast.17, bf16[16,128]{1,0:T(8,128)(2,1)} %bitcast.18, bf16[2048,256]{1,0:T(8,128)(2,1)} %wk_hbm.1, bf16[2048,256]{1,0:T(8,128)(2,1)} %wv_hbm.1, bf16[2,128]{1,0:T(2,128)(2,1)} %bitcast.20), custom_call_target="tpu_custom_call" | custom-call | flops 2147483648 | bytes 8388608 | tf_op jit(solution)/shard_map/project_store/pallas_call | solution.py:129
  19.8 2.6 %all-to-all-done.ids_ref = s32[64,2,16]{2,1,0:T(2,128)S(1)} async-done(((s32[64,2,16]{2,1,0:T(2,128)}), s32[64,2,16]{2,1,0:T(2,128)S(1)}, u32[]{:S(2)}, u32[]{:S(2)}) %all-to-all-start) | async-done | bytes 8224 | tf_op jit(solution)/shard_map/all_to_all | solution.py:488
  22.4 3.4 %fill_slots.1 = bf16[64,64,512]{2,1,0:T(8,128)(2,1)} custom-call(s32[1]{0:T(128)} %bitcast.3.st_ref, s32[64,2,16]{2,1,0:T(2,128)S(1)} %all-to-all-done.ids_ref, bf16[16,64,512]{2,1,0:T(8,128)(2,1)S(1)} %bitcast.11), custom_call_target="tpu_custom_call" | custom-call | tf_op jit(solution)/shard_map/fill_slots/pallas_call | solution.py:169
  25.8 7.5 %all-to-all-start.1 = ((bf16[64,64,512]{2,1,0:T(8,128)(2,1)}), bf16[64,64,512]{2,1,0:T(8,128)(2,1)}, u32[]{:S(2)}, u32[]{:S(2)}) async-start(bf16[64,64,512]{2,1,0:T(8,128)(2,1)} %fill_slots.1), calls=%async_computation.1 | async-start | bytes 8388608 | tf_op jit(solution)/shard_map/all_to_all | solution.py:501
  33.3 0.9 collective-permute-start.5
  34.2 0.0 collective-permute-done.peer_ref
  34.2 0.0 copy-start.7
  34.2 1.3 %copy-done.7 = bf16[1024,1024]{1,0:T(8,128)(2,1)} copy-done((bf16[1024,1024]{1,0:T(8,128)(2,1)}, bf16[1024,1024]{1,0:T(8,128)(2,1)S(1)}, u32[]{:S(2)}) %copy-start.7) | copy-done | bytes 2097176
  35.6 24.9 %token_branch.1 = (f32[1024,768]{1,0:T(8,128)}, f32[1024,2]{1,0:T(8,128)}, bf16[1024,256]{1,0:T(8,128)(2,1)}) custom-call(s32[1]{0:T(128)} %bitcast.tp_ref.half_ref, bf16[1024,1024]{1,0:T(8,128)(2,1)} %own_ref.1, bf16[1024,1024]{1,0:T(8,128)(2,1)} %copy-done.7, bf16[2,8,128]{2,1,0:T(8,128)(2,1)} %bitcast.19, bf16[2048,768]{1,0:T(8,128)(2,1)} %wv_ref.1, ...), custom_call_target="tpu_custom_call" | custom-call | flops 32212254720 | bytes 16777216 | tf_op jit(solution)/shard_map/token_branch/pallas_call | solution.py:244
  60.4 0.0 copy-start.1
  60.4 0.0 copy-start.6
  60.4 0.1 collective-permute-start.3
  60.5 2.1 %collective-permute-done.3.refs_2_ = f32[1024,2]{1,0:T(8,128)S(1)} collective-permute-done((f32[1024,2]{1,0:T(8,128)}, f32[1024,2]{1,0:T(8,128)S(1)}, u32[]{:S(2)}, u32[]{:S(2)}) %collective-permute-start.3) | collective-permute-done | bytes 8224 | tf_op jit(solution)/shard_map/ppermute | solution.py:514
  62.6 0.0 copy-start.5
  62.6 0.8 copy-done.5
  63.4 2.7 %channel_swish.3 = bf16[512,768]{1,0:T(8,128)(2,1)} custom-call(s32[1]{0:T(128)S(6)} %sub.4.half_ref, f32[1024,768]{1,0:T(8,128)} %get-tuple-element.12.refs_0_, f32[1024,2]{1,0:T(8,128)} %get-tuple-element.18.refs_1_, f32[1024,2]{1,0:T(8,128)} %copy-done.5, bf16[6,128]{1,0:T(8,128)(2,1)} %bitcast.14), custom_call_target="tpu_custom_call" | custom-call | flops 805306368 | bytes 4194304 | tf_op jit(solution)/shard_map/channel_swish/pallas_call | solution.py:289
  66.1 0.0 copy-start.3
  66.1 0.0 copy-start.4
  66.1 0.3 collective-permute-start.4
  66.4 0.0 copy-done.1
  66.4 0.4 collective-permute-start.2
  66.8 0.0 copy-done.6
  66.8 0.1 copy.19
  66.8 0.1 shift_right_arithmetic.10.owner_ref
  66.9 2.7 %channel_swish.2.own_ref = bf16[512,768]{1,0:T(8,128)(2,1)} custom-call(s32[1]{0:T(128)} %bitcast.tp_ref.half_ref, f32[1024,768]{1,0:T(8,128)} %get-tuple-element.12.refs_0_, f32[1024,2]{1,0:T(8,128)} %get-tuple-element.18.refs_1_, f32[1024,2]{1,0:T(8,128)} %copy-done.5, bf16[6,128]{1,0:T(8,128)(2,1)} %bitcast.15), custom_call_target="tpu_custom_call" | custom-call | flops 805306368 | bytes 4194304 | tf_op jit(solution)/shard_map/channel_swish/pallas_call | solution.py:289
  69.6 0.0 copy-start.2
  69.6 17.9 %all-to-all-done.1.recv_hbm = bf16[64,64,512]{2,1,0:T(8,128)(2,1)} async-done(((bf16[64,64,512]{2,1,0:T(8,128)(2,1)}), bf16[64,64,512]{2,1,0:T(8,128)(2,1)}, u32[]{:S(2)}, u32[]{:S(2)}) %all-to-all-start.1) | async-done | bytes 4194336 | tf_op jit(solution)/shard_map/all_to_all | solution.py:501
  87.5 0.0 copy-done.3
  87.5 0.0 copy-done.4
  87.5 3.3 %attend_first.1 = (bf16[512,256]{1,0:T(8,128)(2,1)S(1)}, bf16[16,64,512]{2,1,0:T(8,128)(2,1)S(1)}, bf16[512,256]{1,0:T(8,128)(2,1)S(1)}) custom-call(s32[1]{0:T(128)S(6)} %sub.4.half_ref, s32[32]{0:T(128)S(1)} %shift_right_arithmetic.10.owner_ref, bf16[64,64,512]{2,1,0:T(8,128)(2,1)} %all-to-all-done.1.recv_hbm, bf16[1024,256]{1,0:T(8,128)(2,1)S(1)} %copy-done.3, ...), custom_call_target="tpu_custom_call" | custom-call | flops 268435456 | bytes 2097152 | tf_op jit(solution)/shard_map/attend_first/pallas_call | solution.py:401
  90.7 1.8 %collective-permute-start.1 = (bf16[512,256]{1,0:T(8,128)(2,1)S(1)}, bf16[512,256]{1,0:T(8,128)(2,1)S(1)}, u32[]{:S(2)}, u32[]{:S(2)}) collective-permute-start(bf16[512,256]{1,0:T(8,128)(2,1)S(1)} %get-tuple-element.17), channel_id=1, source_target_pairs={{0,1},{1,0},{2,3},{3,2},{4,5},{5,4},{6,7},{7,6},{8,9},{9,8},{10,11... | collective-permute-start | bytes 786440 | tf_op jit(solution)/shard_map/ppermute | solution.py:523
  92.6 0.0 collective-permute-done.4.peer_ref
  92.6 0.0 collective-permute-done.5.w_peer_hbm
  92.6 0.0 copy-done.2
  92.6 7.8 %conv_product.1.conv_ref = bf16[512,2048]{1,0:T(8,128)(2,1)} custom-call(bf16[512,768]{1,0:T(8,128)(2,1)S(1)} %copy-done.2, bf16[512,768]{1,0:T(8,128)(2,1)} %collective-permute-done.4.peer_ref, bf16[768,2048]{1,0:T(8,128)(2,1)} %w_own_hbm.1, bf16[768,2048]{1,0:T(8,128)(2,1)} %collective-permute-done.5.w_peer_hbm), custom_call_target="tpu_custom_call" | custom-call | flops 3221225472 | bytes 12582912 | tf_op jit(solution)/shard_map/conv_product/pallas_call | solution.py:322
  100.4 1.1 %attend_rest.1.own_ref = bf16[512,256]{1,0:T(8,128)(2,1)S(1)} custom-call(bf16[16,64,512]{2,1,0:T(8,128)(2,1)S(1)} %get-tuple-element.15.kv_ref, bf16[512,256]{1,0:T(8,128)(2,1)S(1)} %get-tuple-element.16.q_ref, bf16[2,128]{1,0:T(2,128)(2,1)S(1)} %bitcast.13), custom_call_target="tpu_custom_call" | custom-call | flops 268435456 | bytes 2097152 | tf_op jit(solution)/shard_map/attend_rest/pallas_call | solution.py:428
  101.6 0.0 collective-permute-done.2.w_peer_ref
  101.6 0.0 collective-permute-done.1.peer_ref
  101.6 0.0 copy-start
  101.6 1.6 %copy-done = bf16[512,2048]{1,0:T(8,128)(2,1)S(1)} copy-done((bf16[512,2048]{1,0:T(8,128)(2,1)S(1)}, bf16[512,2048]{1,0:T(8,128)(2,1)}, u32[]{:S(2)}) %copy-start) | copy-done | bytes 2097176
  103.2 2.2 %finish.1 = bf16[512,2048]{1,0:T(8,128)(2,1)} custom-call(bf16[512,256]{1,0:T(8,128)(2,1)S(1)} %attend_rest.1.own_ref, bf16[512,256]{1,0:T(8,128)(2,1)S(1)} %collective-permute-done.1.peer_ref, bf16[256,2048]{1,0:T(8,128)(2,1)S(1)} %copy-done.1, bf16[256,2048]{1,0:T(8,128)(2,1)S(1)} %collective-permute-done.2.w_peer_ref, bf16[512,2048]{1,0:T(8,128)(2,1)S(1)} %copy-done), custom_call_target="tpu_custom_call" | custom-call | flops 1073741824 | bytes 8388608 | tf_op jit(solution)/shard_map/finish/pallas_call | solution.py:453
  (1 shorter events, 0.0 us)
Async XLA Ops:
  0.0 34.2 %collective-permute-start = (bf16[1024,1024]{1,0:T(8,128)(2,1)}, bf16[1024,1024]{1,0:T(8,128)(2,1)S(1)}, u32[]{:S(2)}, u32[]{:S(2)}) collective-permute-start(bf16[1024,1024]{1,0:T(8,128)(2,1)} %own_ref.1), channel_id=1, source_target_pairs={{0,1},{1,0},{2,3},{3,2},{4,5},{5,4},{6,7},{7,6},{8,9},{9,8},{10,11... | collective-permute-start | bytes 6291464 | tf_op jit(solution)/shard_map/ppermute | solution.py:489
  2.7 19.7 %all-to-all-start = ((s32[64,2,16]{2,1,0:T(2,128)}), s32[64,2,16]{2,1,0:T(2,128)S(1)}, u32[]{:S(2)}, u32[]{:S(2)}) async-start(s32[64,2,16]{2,1,0:T(2,128)} %broadcast_in_dim.3), calls=%async_computation | async-start | bytes 131072 | tf_op jit(solution)/shard_map/all_to_all | solution.py:488
  25.8 61.7 %all-to-all-start.1 = ((bf16[64,64,512]{2,1,0:T(8,128)(2,1)}), bf16[64,64,512]{2,1,0:T(8,128)(2,1)}, u32[]{:S(2)}, u32[]{:S(2)}) async-start(bf16[64,64,512]{2,1,0:T(8,128)(2,1)} %fill_slots.1), calls=%async_computation.1 | async-start | bytes 8388608 | tf_op jit(solution)/shard_map/all_to_all | solution.py:501
  33.3 59.3 %collective-permute-start.5 = (bf16[768,2048]{1,0:T(8,128)(2,1)}, bf16[768,2048]{1,0:T(8,128)(2,1)}, u32[]{:S(2)}, u32[]{:S(2)}) collective-permute-start(bf16[768,2048]{1,0:T(8,128)(2,1)} %w_own_hbm.1), channel_id=1, source_target_pairs={{0,1},{1,0},{2,3},{3,2},{4,5},{5,4},{6,7},{7,6},{8,9},{9,8},{10,11... | collective-permute-start | bytes 9437192 | tf_op jit(solution)/shard_map/ppermute | solution.py:490
  34.2 1.3 %copy-start.7 = (bf16[1024,1024]{1,0:T(8,128)(2,1)}, bf16[1024,1024]{1,0:T(8,128)(2,1)S(1)}, u32[]{:S(2)}) copy-start(bf16[1024,1024]{1,0:T(8,128)(2,1)S(1)} %collective-permute-done.peer_ref) | copy-start | bytes 6291460
  60.4 6.0 %copy-start.1 = (bf16[256,2048]{1,0:T(8,128)(2,1)S(1)}, bf16[256,2048]{1,0:T(8,128)(2,1)}, u32[]{:S(2)}) copy-start(bf16[256,2048]{1,0:T(8,128)(2,1)} %w_own_ref.1) | copy-start | bytes 3145732
  60.4 6.3 %copy-start.6 = (s32[16,2]{0,1:T(2,128)S(1)}, s32[16,2]{0,1:T(2,128)}, u32[]{:S(2)}) copy-start(s32[16,2]{0,1:T(2,128)} %param.18) | copy-start | bytes 388
  60.4 2.2 %collective-permute-start.3 = (f32[1024,2]{1,0:T(8,128)}, f32[1024,2]{1,0:T(8,128)S(1)}, u32[]{:S(2)}, u32[]{:S(2)}) collective-permute-start(f32[1024,2]{1,0:T(8,128)} %get-tuple-element.18.refs_1_), channel_id=1, source_target_pairs={{0,1},{1,0},{2,3},{3,2},{4,5},{5,4},{6,7},{7,6},{8,9},{9,8},{10,11... | collective-permute-start | bytes 24584 | tf_op jit(solution)/shard_map/ppermute | solution.py:514
  62.6 0.8 copy-start.5
  66.1 21.4 %copy-start.3 = (bf16[1024,256]{1,0:T(8,128)(2,1)S(1)}, bf16[1024,256]{1,0:T(8,128)(2,1)}, u32[]{:S(2)}) copy-start(bf16[1024,256]{1,0:T(8,128)(2,1)} %get-tuple-element.14.q_ref) | copy-start | bytes 1572868
  66.1 21.4 %copy-start.4 = (bf16[256]{0:T(256)(128)(2,1)S(1)}, bf16[256]{0:T(256)(128)(2,1)}, u32[]{:S(2)}) copy-start(bf16[256]{0:T(256)(128)(2,1)} %param.31) | copy-start | bytes 1540
  66.1 26.5 %collective-permute-start.4 = (bf16[512,768]{1,0:T(8,128)(2,1)}, bf16[512,768]{1,0:T(8,128)(2,1)}, u32[]{:S(2)}, u32[]{:S(2)}) collective-permute-start(bf16[512,768]{1,0:T(8,128)(2,1)} %channel_swish.3), channel_id=1, source_target_pairs={{0,1},{1,0},{2,3},{3,2},{4,5},{5,4},{6,7},{7,6},{8,9},{9,8},{10,11... | collective-permute-start | bytes 2359304 | tf_op jit(solution)/shard_map/ppermute | solution.py:516
  66.4 35.2 %collective-permute-start.2 = (bf16[256,2048]{1,0:T(8,128)(2,1)S(1)}, bf16[256,2048]{1,0:T(8,128)(2,1)S(1)}, u32[]{:S(2)}, u32[]{:S(2)}) collective-permute-start(bf16[256,2048]{1,0:T(8,128)(2,1)S(1)} %copy-done.1), channel_id=1, source_target_pairs={{0,1},{1,0},{2,3},{3,2},{4,5},{5,4},{6,7},{7,6},{8,9},{9,8},{10,11... | collective-permute-start | bytes 3145736 | tf_op jit(solution)/shard_map/ppermute | solution.py:491
  69.6 23.0 %copy-start.2 = (bf16[512,768]{1,0:T(8,128)(2,1)S(1)}, bf16[512,768]{1,0:T(8,128)(2,1)}, u32[]{:S(2)}) copy-start(bf16[512,768]{1,0:T(8,128)(2,1)} %channel_swish.2.own_ref) | copy-start | bytes 2359300
  90.7 10.8 %collective-permute-start.1 = (bf16[512,256]{1,0:T(8,128)(2,1)S(1)}, bf16[512,256]{1,0:T(8,128)(2,1)S(1)}, u32[]{:S(2)}, u32[]{:S(2)}) collective-permute-start(bf16[512,256]{1,0:T(8,128)(2,1)S(1)} %get-tuple-element.17), channel_id=1, source_target_pairs={{0,1},{1,0},{2,3},{3,2},{4,5},{5,4},{6,7},{7,6},{8,9},{9,8},{10,11... | collective-permute-start | bytes 786440 | tf_op jit(solution)/shard_map/ppermute | solution.py:523
  101.6 1.6 %copy-start = (bf16[512,2048]{1,0:T(8,128)(2,1)S(1)}, bf16[512,2048]{1,0:T(8,128)(2,1)}, u32[]{:S(2)}) copy-start(bf16[512,2048]{1,0:T(8,128)(2,1)} %conv_product.1.conv_ref) | copy-start | bytes 6291460

commit v6 on v5

--- a/solution.py
+++ b/solution.py
@@ -147,9 +147,9 @@
     )(*offchip(rows, passage_gain, key_weight, value_weight, key_gain))
 
 
-def slots_kernel(st_ref, ids_ref, kv_ref, out_hbm, row_ref, table, table_sem, sem):
+def slots_kernel(ids_ref, kv_ref, out_hbm, row_ref, table, table_sem, sem):
     count = out_hbm.shape[0]
-    local = ids_ref[...] ^ (st_ref[0] * PASS_DEV)
+    local = ids_ref[...] ^ (lax.axis_index("st") * PASS_DEV)
     asked = jnp.where(local < PASS_DEV, local, 0)
     asked = jnp.sum(asked[:, 0, :] + asked[:, 1, :], axis=1, keepdims=True).astype(F32)
     square = jnp.concatenate([jnp.broadcast_to(asked, (count, LANES)), jnp.zeros((LANES - count, LANES), F32)], axis=0)
@@ -164,12 +164,12 @@
         c.wait()
 
 
-def fill_slots(st, ids, kv):
+def fill_slots(ids, kv):
     count = ids.shape[0]
     return pl.pallas_call(
         slots_kernel,
         out_shape=pltpu.HBM((count, PLEN, 2 * MEM_DEV), BF16),
-        in_specs=[pl.BlockSpec(memory_space=pltpu.SMEM), ONCHIP, ONCHIP],
+        in_specs=[ONCHIP, ONCHIP],
         out_specs=HBM,
         scratch_shapes=[
             pltpu.VMEM((8, LANES), jnp.int32),
@@ -179,7 +179,7 @@
         ],
         compiler_params=grant(2),
         name="fill_slots",
-    )(st, *onchip(ids, kv))
+    )(*onchip(ids, kv))
 
 
 def token_kernel(
@@ -497,7 +497,7 @@
         value_weight,
         key_gain.reshape(-1, LANES),
     ).reshape(PASS_DEV, PLEN, 2 * MEM_DEV)
-    sent = fill_slots(lax.axis_index("st").astype(jnp.int32).reshape(1), ids, kv)
+    sent = fill_slots(ids, kv)
     received = lax.all_to_all(sent, "st", 0, 0, tiled=True)
 
     filtered, own_stats, queries = token_branch(

time: 106 us -> 106 us (level)
  waiting for transfers between devices: 22.5 us -> 23.9 us
  local copies, waits for them, and re-layouts: 5.22 us -> 3.92 us
    all_to_all x1, waiting for transfers between devices: 17.9 us -> 19.2 us  [body(): received = lax.all_to_all(sent, 'st', 0, 0, tiled=True)]
    unnamed x16 -> x14, local copies, waits for them, and re-layouts: 3.72 us -> 2.42 us
where the time goes in v6:
time: 106 us
  Pallas kernels  53.9 us (51%)
  waiting for transfers between devices  23.9 us (23%)
  starting transfers between devices  23.7 us (22%)
  local copies, waits for them, and re-layouts  3.92 us (4%)
    pallas_call x1, Pallas kernels, token_branch(): pl.pallas_call(token_kernel, out_shape=(jax.ShapeDtypeStruct((n, C_DEV),...  24.8 us
    all_to_all x1, waiting for transfers between devices, body(): received = lax.all_to_all(sent, 'st', 0, 0, tiled=True)  19.2 us
    all_to_all x1, starting transfers between devices, body(): lax.all_to_all(jnp.broadcast_to(passage_ids.T, (owner_count, *passage_ids...  11.2 us
    pallas_call x1, Pallas kernels, conv_product(): pl.pallas_call(pair_kernel, out_shape=pltpu.HBM((n, D), BF16), in_specs=[...  7.84 us
    all_to_all x1, starting transfers between devices, body(): received = lax.all_to_all(sent, 'st', 0, 0, tiled=True)  7.51 us
    pallas_call x1, Pallas kernels, project_store(): pl.pallas_call(kv_kernel, out_shape=pltpu.VMEM((n, 2 * MEM_DEV), BF16), i...  5.87 us
    pallas_call x2, Pallas kernels, channel_swish(): pl.pallas_call(lambda half_ref, *refs: swish_kernel(*refs), out_shape=jax...  5.33 us
    pallas_call x1, Pallas kernels, fill_slots(): pl.pallas_call(slots_kernel, out_shape=pltpu.HBM((count, PLEN, 2 * MEM_DE...  3.37 us
  transfers between devices with their start and end apart: 8, of which 3 were waited for; matrix products, arithmetic and copies ran while one was open for 1% of the time, Pallas kernels for 49%

profile of v6, /device:TPU:1, one launch (start us, length us, event | category | flops | bytes accessed | tf_op | source)
XLA Modules:
  0.0 105.6 jit_solution(2238838149524053451)
XLA Ops:
  0.0 1.4 %collective-permute-start = (bf16[1024,1024]{1,0:T(8,128)(2,1)}, bf16[1024,1024]{1,0:T(8,128)(2,1)}, u32[]{:S(2)}, u32[]{:S(2)}) collective-permute-start(bf16[1024,1024]{1,0:T(8,128)(2,1)} %own_ref.1), channel_id=1, source_target_pairs={{0,1},{1,0},{2,3},{3,2},{4,5},{5,4},{6,7},{7,6},{8,9},{9,8},{10,11... | collective-permute-start | bytes 6291464 | tf_op jit(solution)/shard_map/ppermute | solution.py:489
  1.4 1.3 %broadcast_in_dim.3 = s32[64,2,16]{2,1,0:T(2,128)} broadcast(s32[2,16]{1,0:T(2,128)} %bitcast.15), dimensions={1,2} | broadcast | bytes 8320 | tf_op jit(solution)/shard_map/broadcast_in_dim | solution.py:488
  2.7 11.2 %all-to-all-start = ((s32[64,2,16]{2,1,0:T(2,128)}), s32[64,2,16]{2,1,0:T(2,128)S(1)}, u32[]{:S(2)}, u32[]{:S(2)}) async-start(s32[64,2,16]{2,1,0:T(2,128)} %broadcast_in_dim.3), calls=%async_computation | async-start | bytes 131072 | tf_op jit(solution)/shard_map/all_to_all | solution.py:488
  14.0 5.9 %project_store.1 = bf16[1024,512]{1,0:T(8,128)(2,1)S(1)} custom-call(bf16[1024,2048]{1,0:T(8,128)(2,1)} %bitcast.16, bf16[16,128]{1,0:T(8,128)(2,1)} %bitcast.17, bf16[2048,256]{1,0:T(8,128)(2,1)} %wk_hbm.1, bf16[2048,256]{1,0:T(8,128)(2,1)} %wv_hbm.1, bf16[2,128]{1,0:T(2,128)(2,1)} %bitcast.19), custom_call_target="tpu_custom_call" | custom-call | flops 2147483648 | bytes 8388608 | tf_op jit(solution)/shard_map/project_store/pallas_call | solution.py:129
  19.8 2.6 %all-to-all-done.ids_ref = s32[64,2,16]{2,1,0:T(2,128)S(1)} async-done(((s32[64,2,16]{2,1,0:T(2,128)}), s32[64,2,16]{2,1,0:T(2,128)S(1)}, u32[]{:S(2)}, u32[]{:S(2)}) %all-to-all-start) | async-done | bytes 8224 | tf_op jit(solution)/shard_map/all_to_all | solution.py:488
  22.4 3.4 %fill_slots.1 = bf16[64,64,512]{2,1,0:T(8,128)(2,1)} custom-call(s32[64,2,16]{2,1,0:T(2,128)S(1)} %all-to-all-done.ids_ref, bf16[16,64,512]{2,1,0:T(8,128)(2,1)S(1)} %bitcast.10), custom_call_target="tpu_custom_call" | custom-call | tf_op jit(solution)/shard_map/fill_slots/pallas_call | solution.py:169
  25.8 7.5 %all-to-all-start.1 = ((bf16[64,64,512]{2,1,0:T(8,128)(2,1)}), bf16[64,64,512]{2,1,0:T(8,128)(2,1)}, u32[]{:S(2)}, u32[]{:S(2)}) async-start(bf16[64,64,512]{2,1,0:T(8,128)(2,1)} %fill_slots.1), calls=%async_computation.1 | async-start | bytes 8388608 | tf_op jit(solution)/shard_map/all_to_all | solution.py:501
  33.3 0.9 collective-permute-start.5
  34.2 0.0 collective-permute-done.peer_ref
  34.2 24.8 %token_branch.1 = (f32[1024,768]{1,0:T(8,128)}, f32[1024,2]{1,0:T(8,128)}, bf16[1024,256]{1,0:T(8,128)(2,1)}) custom-call(s32[1]{0:T(128)} %bitcast.tp_ref.half_ref, bf16[1024,1024]{1,0:T(8,128)(2,1)} %own_ref.1, bf16[1024,1024]{1,0:T(8,128)(2,1)} %collective-permute-done.peer_ref, bf16[2,8,128]{2,1,0:T(8,128)(2,1)} %bitcast.18, bf16[2048,768]{1,0:T(8,128)(2,1)} %wv_ref.1, ...), custom_call_target="tpu_custom_call" | custom-call | flops 32212254720 | bytes 16777216 | tf_op jit(solution)/shard_map/token_branch/pallas_call | solution.py:244
  59.1 0.0 copy-start.1
  59.1 0.0 copy-start.6
  59.1 0.1 collective-permute-start.3
  59.2 2.1 %collective-permute-done.3.refs_2_ = f32[1024,2]{1,0:T(8,128)S(1)} collective-permute-done((f32[1024,2]{1,0:T(8,128)}, f32[1024,2]{1,0:T(8,128)S(1)}, u32[]{:S(2)}, u32[]{:S(2)}) %collective-permute-start.3) | collective-permute-done | bytes 8224 | tf_op jit(solution)/shard_map/ppermute | solution.py:514
  61.3 0.0 copy-start.5
  61.3 0.8 copy-done.5
  62.1 2.7 %channel_swish.3 = bf16[512,768]{1,0:T(8,128)(2,1)} custom-call(s32[1]{0:T(128)S(6)} %sub.4.half_ref, f32[1024,768]{1,0:T(8,128)} %get-tuple-element.12.refs_0_, f32[1024,2]{1,0:T(8,128)} %get-tuple-element.18.refs_1_, f32[1024,2]{1,0:T(8,128)} %copy-done.5, bf16[6,128]{1,0:T(8,128)(2,1)} %bitcast.13), custom_call_target="tpu_custom_call" | custom-call | flops 805306368 | bytes 4194304 | tf_op jit(solution)/shard_map/channel_swish/pallas_call | solution.py:289
  64.8 0.0 copy-start.3
  64.8 0.0 copy-start.4
  64.8 0.3 collective-permute-start.4
  65.1 0.0 copy-done.1
  65.1 0.4 collective-permute-start.2
  65.4 0.0 copy-done.6
  65.4 0.1 copy.19
  65.5 0.1 shift_right_arithmetic.10.owner_ref
  65.6 2.7 %channel_swish.2.own_ref = bf16[512,768]{1,0:T(8,128)(2,1)} custom-call(s32[1]{0:T(128)} %bitcast.tp_ref.half_ref, f32[1024,768]{1,0:T(8,128)} %get-tuple-element.12.refs_0_, f32[1024,2]{1,0:T(8,128)} %get-tuple-element.18.refs_1_, f32[1024,2]{1,0:T(8,128)} %copy-done.5, bf16[6,128]{1,0:T(8,128)(2,1)} %bitcast.14), custom_call_target="tpu_custom_call" | custom-call | flops 805306368 | bytes 4194304 | tf_op jit(solution)/shard_map/channel_swish/pallas_call | solution.py:289
  68.3 0.0 copy-start.2
  68.3 19.2 %all-to-all-done.1.recv_hbm = bf16[64,64,512]{2,1,0:T(8,128)(2,1)} async-done(((bf16[64,64,512]{2,1,0:T(8,128)(2,1)}), bf16[64,64,512]{2,1,0:T(8,128)(2,1)}, u32[]{:S(2)}, u32[]{:S(2)}) %all-to-all-start.1) | async-done | bytes 4194336 | tf_op jit(solution)/shard_map/all_to_all | solution.py:501
  87.5 0.0 copy-done.3
  87.5 0.0 copy-done.4
  87.5 3.3 %attend_first.1 = (bf16[512,256]{1,0:T(8,128)(2,1)S(1)}, bf16[16,64,512]{2,1,0:T(8,128)(2,1)S(1)}, bf16[512,256]{1,0:T(8,128)(2,1)S(1)}) custom-call(s32[1]{0:T(128)S(6)} %sub.4.half_ref, s32[32]{0:T(128)S(1)} %shift_right_arithmetic.10.owner_ref, bf16[64,64,512]{2,1,0:T(8,128)(2,1)} %all-to-all-done.1.recv_hbm, bf16[1024,256]{1,0:T(8,128)(2,1)S(1)} %copy-done.3, ...), custom_call_target="tpu_custom_call" | custom-call | flops 268435456 | bytes 2097152 | tf_op jit(solution)/shard_map/attend_first/pallas_call | solution.py:401
  90.8 1.8 %collective-permute-start.1 = (bf16[512,256]{1,0:T(8,128)(2,1)S(1)}, bf16[512,256]{1,0:T(8,128)(2,1)S(1)}, u32[]{:S(2)}, u32[]{:S(2)}) collective-permute-start(bf16[512,256]{1,0:T(8,128)(2,1)S(1)} %get-tuple-element.17), channel_id=1, source_target_pairs={{0,1},{1,0},{2,3},{3,2},{4,5},{5,4},{6,7},{7,6},{8,9},{9,8},{10,11... | collective-permute-start | bytes 786440 | tf_op jit(solution)/shard_map/ppermute | solution.py:523
  92.6 0.0 collective-permute-done.4.peer_ref
  92.6 0.0 collective-permute-done.5.w_peer_hbm
  92.6 0.0 copy-done.2
  92.6 7.8 %conv_product.1.conv_ref = bf16[512,2048]{1,0:T(8,128)(2,1)} custom-call(bf16[512,768]{1,0:T(8,128)(2,1)S(1)} %copy-done.2, bf16[512,768]{1,0:T(8,128)(2,1)} %collective-permute-done.4.peer_ref, bf16[768,2048]{1,0:T(8,128)(2,1)} %w_own_hbm.1, bf16[768,2048]{1,0:T(8,128)(2,1)} %collective-permute-done.5.w_peer_hbm), custom_call_target="tpu_custom_call" | custom-call | flops 3221225472 | bytes 12582912 | tf_op jit(solution)/shard_map/conv_product/pallas_call | solution.py:322
  100.5 1.1 %attend_rest.1.own_ref = bf16[512,256]{1,0:T(8,128)(2,1)S(1)} custom-call(bf16[16,64,512]{2,1,0:T(8,128)(2,1)S(1)} %get-tuple-element.15.kv_ref, bf16[512,256]{1,0:T(8,128)(2,1)S(1)} %get-tuple-element.16.q_ref, bf16[2,128]{1,0:T(2,128)(2,1)S(1)} %bitcast.12), custom_call_target="tpu_custom_call" | custom-call | flops 268435456 | bytes 2097152 | tf_op jit(solution)/shard_map/attend_rest/pallas_call | solution.py:428
  101.6 0.0 collective-permute-done.2.w_peer_ref
  101.6 0.0 collective-permute-done.1.peer_ref
  101.6 0.0 copy-start
  101.6 1.6 %copy-done = bf16[512,2048]{1,0:T(8,128)(2,1)S(1)} copy-done((bf16[512,2048]{1,0:T(8,128)(2,1)S(1)}, bf16[512,2048]{1,0:T(8,128)(2,1)}, u32[]{:S(2)}) %copy-start) | copy-done | bytes 2097176
  103.2 2.2 %finish.1 = bf16[512,2048]{1,0:T(8,128)(2,1)} custom-call(bf16[512,256]{1,0:T(8,128)(2,1)S(1)} %attend_rest.1.own_ref, bf16[512,256]{1,0:T(8,128)(2,1)S(1)} %collective-permute-done.1.peer_ref, bf16[256,2048]{1,0:T(8,128)(2,1)S(1)} %copy-done.1, bf16[256,2048]{1,0:T(8,128)(2,1)S(1)} %collective-permute-done.2.w_peer_ref, bf16[512,2048]{1,0:T(8,128)(2,1)S(1)} %copy-done), custom_call_target="tpu_custom_call" | custom-call | flops 1073741824 | bytes 8388608 | tf_op jit(solution)/shard_map/finish/pallas_call | solution.py:453
  (1 shorter events, 0.0 us)
Async XLA Ops:
  0.0 34.2 %collective-permute-start = (bf16[1024,1024]{1,0:T(8,128)(2,1)}, bf16[1024,1024]{1,0:T(8,128)(2,1)}, u32[]{:S(2)}, u32[]{:S(2)}) collective-permute-start(bf16[1024,1024]{1,0:T(8,128)(2,1)} %own_ref.1), channel_id=1, source_target_pairs={{0,1},{1,0},{2,3},{3,2},{4,5},{5,4},{6,7},{7,6},{8,9},{9,8},{10,11... | collective-permute-start | bytes 6291464 | tf_op jit(solution)/shard_map/ppermute | solution.py:489
  2.7 19.7 %all-to-all-start = ((s32[64,2,16]{2,1,0:T(2,128)}), s32[64,2,16]{2,1,0:T(2,128)S(1)}, u32[]{:S(2)}, u32[]{:S(2)}) async-start(s32[64,2,16]{2,1,0:T(2,128)} %broadcast_in_dim.3), calls=%async_computation | async-start | bytes 131072 | tf_op jit(solution)/shard_map/all_to_all | solution.py:488
  25.8 61.7 %all-to-all-start.1 = ((bf16[64,64,512]{2,1,0:T(8,128)(2,1)}), bf16[64,64,512]{2,1,0:T(8,128)(2,1)}, u32[]{:S(2)}, u32[]{:S(2)}) async-start(bf16[64,64,512]{2,1,0:T(8,128)(2,1)} %fill_slots.1), calls=%async_computation.1 | async-start | bytes 8388608 | tf_op jit(solution)/shard_map/all_to_all | solution.py:501
  33.3 59.3 %collective-permute-start.5 = (bf16[768,2048]{1,0:T(8,128)(2,1)}, bf16[768,2048]{1,0:T(8,128)(2,1)}, u32[]{:S(2)}, u32[]{:S(2)}) collective-permute-start(bf16[768,2048]{1,0:T(8,128)(2,1)} %w_own_hbm.1), channel_id=1, source_target_pairs={{0,1},{1,0},{2,3},{3,2},{4,5},{5,4},{6,7},{7,6},{8,9},{9,8},{10,11... | collective-permute-start | bytes 9437192 | tf_op jit(solution)/shard_map/ppermute | solution.py:490
  59.1 6.0 %copy-start.1 = (bf16[256,2048]{1,0:T(8,128)(2,1)S(1)}, bf16[256,2048]{1,0:T(8,128)(2,1)}, u32[]{:S(2)}) copy-start(bf16[256,2048]{1,0:T(8,128)(2,1)} %w_own_ref.1) | copy-start | bytes 3145732
  59.1 6.4 %copy-start.6 = (s32[16,2]{0,1:T(2,128)S(1)}, s32[16,2]{0,1:T(2,128)}, u32[]{:S(2)}) copy-start(s32[16,2]{0,1:T(2,128)} %param.18) | copy-start | bytes 388
  59.1 2.2 %collective-permute-start.3 = (f32[1024,2]{1,0:T(8,128)}, f32[1024,2]{1,0:T(8,128)S(1)}, u32[]{:S(2)}, u32[]{:S(2)}) collective-permute-start(f32[1024,2]{1,0:T(8,128)} %get-tuple-element.18.refs_1_), channel_id=1, source_target_pairs={{0,1},{1,0},{2,3},{3,2},{4,5},{5,4},{6,7},{7,6},{8,9},{9,8},{10,11... | collective-permute-start | bytes 24584 | tf_op jit(solution)/shard_map/ppermute | solution.py:514
  61.3 0.8 copy-start.5
  64.8 22.7 %copy-start.3 = (bf16[1024,256]{1,0:T(8,128)(2,1)S(1)}, bf16[1024,256]{1,0:T(8,128)(2,1)}, u32[]{:S(2)}) copy-start(bf16[1024,256]{1,0:T(8,128)(2,1)} %get-tuple-element.14.q_ref) | copy-start | bytes 1572868
  64.8 22.7 %copy-start.4 = (bf16[256]{0:T(256)(128)(2,1)S(1)}, bf16[256]{0:T(256)(128)(2,1)}, u32[]{:S(2)}) copy-start(bf16[256]{0:T(256)(128)(2,1)} %param.31) | copy-start | bytes 1540
  64.8 27.9 %collective-permute-start.4 = (bf16[512,768]{1,0:T(8,128)(2,1)}, bf16[512,768]{1,0:T(8,128)(2,1)}, u32[]{:S(2)}, u32[]{:S(2)}) collective-permute-start(bf16[512,768]{1,0:T(8,128)(2,1)} %channel_swish.3), channel_id=1, source_target_pairs={{0,1},{1,0},{2,3},{3,2},{4,5},{5,4},{6,7},{7,6},{8,9},{9,8},{10,11... | collective-permute-start | bytes 2359304 | tf_op jit(solution)/shard_map/ppermute | solution.py:516
  65.1 36.5 %collective-permute-start.2 = (bf16[256,2048]{1,0:T(8,128)(2,1)S(1)}, bf16[256,2048]{1,0:T(8,128)(2,1)S(1)}, u32[]{:S(2)}, u32[]{:S(2)}) collective-permute-start(bf16[256,2048]{1,0:T(8,128)(2,1)S(1)} %copy-done.1), channel_id=1, source_target_pairs={{0,1},{1,0},{2,3},{3,2},{4,5},{5,4},{6,7},{7,6},{8,9},{9,8},{10,11... | collective-permute-start | bytes 3145736 | tf_op jit(solution)/shard_map/ppermute | solution.py:491
  68.3 24.3 %copy-start.2 = (bf16[512,768]{1,0:T(8,128)(2,1)S(1)}, bf16[512,768]{1,0:T(8,128)(2,1)}, u32[]{:S(2)}) copy-start(bf16[512,768]{1,0:T(8,128)(2,1)} %channel_swish.2.own_ref) | copy-start | bytes 2359300
  90.8 10.8 %collective-permute-start.1 = (bf16[512,256]{1,0:T(8,128)(2,1)S(1)}, bf16[512,256]{1,0:T(8,128)(2,1)S(1)}, u32[]{:S(2)}, u32[]{:S(2)}) collective-permute-start(bf16[512,256]{1,0:T(8,128)(2,1)S(1)} %get-tuple-element.17), channel_id=1, source_target_pairs={{0,1},{1,0},{2,3},{3,2},{4,5},{5,4},{6,7},{7,6},{8,9},{9,8},{10,11... | collective-permute-start | bytes 786440 | tf_op jit(solution)/shard_map/ppermute | solution.py:523
  101.6 1.6 %copy-start = (bf16[512,2048]{1,0:T(8,128)(2,1)S(1)}, bf16[512,2048]{1,0:T(8,128)(2,1)}, u32[]{:S(2)}) copy-start(bf16[512,2048]{1,0:T(8,128)(2,1)} %conv_product.1.conv_ref) | copy-start | bytes 6291460
